TPU v7x, 512 devices: a whole 4x4x16 slice. The times are simulated.
512 devices in a mesh: ep: 32 (over z, core), tp: 16 (over y, x).
Axes of the slice: x: 4, y: 4, z: 16, core: 2. Of those that a mesh axis runs over, the one named last changes fastest.
Arguments:
- tokens: bfloat16 [512, 2048], P('ep'), may hold values from -6 to 6
- mix_gain: float32 [2048], replicated, may hold values from 0.1 to 1.9
- gate_weight: bfloat16 [2048, 1024], P('ep', 'tp'), may hold values from -0.125 to 0.125
- inner_weight: bfloat16 [2048, 1024], P('ep', 'tp'), may hold values from -0.125 to 0.125
- write_weight: bfloat16 [2048, 512], P('ep'), may hold values from -0.125 to 0.125
- read_weight: bfloat16 [2048, 512], P('ep'), may hold values from -0.125 to 0.125
- step_weight: bfloat16 [2048, 16], P('ep'), may hold values from -0.125 to 0.125
- step_bias: float32 [16], replicated, may hold values from -2 to 1
- decay_log: float32 [16], replicated, may hold values from -1 to 1.5
- skip_scale: float32 [16], replicated, may hold values from 0.5 to 2
- inner_taps: bfloat16 [4, 1024], P(None, 'tp'), may hold values from -3 to 3
- access_taps: bfloat16 [2, 4, 512], replicated, may hold values from -3 to 3
- inner_history: bfloat16 [512, 3, 1024], P('ep', None, 'tp'), may hold values from -6 to 6
- access_history: bfloat16 [512, 2, 3, 512], P('ep'), may hold values from -6 to 6
- recurrent: float32 [512, 16, 64, 128], P('ep', 'tp'), may hold values from -3 to 3
- head_gain: float32 [1024], P('tp'), may hold values from 0.1 to 1.9
- mixer_out: bfloat16 [1024, 2048], P('tp'), may hold values from -0.1875 to 0.1875
- moe_gain: float32 [2048], replicated, may hold values from 0.1 to 1.9
- expert_ids: int32 [512, 2], P('ep'), may hold values from 0 to 31, all different within a row; in each aligned block of 16 rows (0 to 15, 16 to 31, ...) at most 2 rows name the same one
- route_scores: float32 [512, 2], P('ep'), may hold values from -6 to 6
- expert_gate: bfloat16 [32, 2048, 4096], P('ep', None, 'tp'), may hold values from -0.125 to 0.125
- expert_up: bfloat16 [32, 2048, 4096], P('ep', None, 'tp'), may hold values from -0.125 to 0.125
- expert_down: bfloat16 [32, 4096, 2048], P('ep', 'tp'), may hold values from -0.1875 to 0.1875
- blend_vector: bfloat16 [2048], replicated, may hold values from -0.125 to 0.125
- dense_gate: bfloat16 [2048, 7168], P('tp', 'ep'), may hold values from -0.125 to 0.125
- dense_up: bfloat16 [2048, 7168], P('tp', 'ep'), may hold values from -0.125 to 0.125
- dense_down: bfloat16 [7168, 2048], P('ep', 'tp'), may hold values from -0.125 to 0.125
Outputs:
- output: float32 [512, 2048], P('ep', 'tp')
- new_recurrent: float32 [512, 16, 64, 128], P('ep', 'tp')
- new_inner_history: bfloat16 [512, 3, 1024], P('ep', None, 'tp')
- new_access_history: bfloat16 [512, 2, 3, 512], P('ep')
Inputs may be any that keep to these rules, and one draw needn't show every extreme that they name: `expert_ids`: each row names 2 different experts; among the rows of one device no expert is named by more than 2 rows, and in some aligned blocks of 16 rows one expert is named by exactly 2.
All inputs are finite; a program needn't handle non-finite values.
Results may differ from a plain program's by a relative error of at most 0.009.
Values may be sent and summed in bfloat16 or wider, within the bound.
No kernel may reach another device: no remote copies, remote signals or barrier semaphores. Data moves between devices by JAX's collectives and lax.ppermute only.
A program may use at most 64 MiB of HBM per device.

v0:
```python
import jax
import jax.numpy as jnp
from jax import lax
from jax.sharding import PartitionSpec as P

HEADS = 16
HEAD_DIM = 64
GROUPS = 4
STATE = 128
TOP = 2


EPS = 1e-06


def from_everyone(shard, axis):
    copies = jnp.broadcast_to(shard, (lax.axis_size(axis), *shard.shape))
    return lax.all_to_all(copies, axis, split_axis=0, concat_axis=0, tiled=True)


def over_copies(shard, axis):
    return from_everyone(shard, axis).sum(axis=0)


def in_order(pieces, dim):
    pieces = jnp.moveaxis(pieces, 0, dim)
    shape = pieces.shape
    return pieces.reshape(*shape[:dim], shape[dim] * shape[dim + 1], *shape[dim + 2 :])


def gathered_copies(shard, axis, dim):
    pieces = from_everyone(shard, axis)
    return in_order(pieces, dim)


def rows_for(lines, peers):
    spare = -lines.shape[0] % peers
    if not spare:
        return lines
    return jnp.concatenate([lines, jnp.zeros((spare, *lines.shape[1:]), lines.dtype)])


def total_of(shard, axis):
    lines = shard.reshape(-1, *shard.shape[1:][-1:])
    own = lax.psum_scatter(
        rows_for(lines, lax.axis_size(axis)), axis, scatter_dimension=0, tiled=True
    )
    whole = lax.all_gather(own, axis).reshape(-1, *lines.shape[1:])
    return lax.slice_in_dim(whole, 0, len(lines)).reshape(shard.shape)


def cut_along(shard, dim, peers):
    before, after = (shard.shape[:dim], shard.shape[dim + 1 :])
    return jnp.moveaxis(shard.reshape(*before, peers, -1, *after), dim, 0)


def sent_and_summed(shard, axis, dim):
    pieces = cut_along(shard, dim, lax.axis_size(axis))
    arrived = lax.all_to_all(pieces, axis, split_axis=0, concat_axis=0, tiled=True)
    return arrived.sum(axis=0)


def rms_scale(values, gain):
    mean_square = jnp.mean(values * values, axis=-1, keepdims=True)
    return values * lax.rsqrt(mean_square + EPS) * gain


def local(
    tokens,
    mix_gain,
    gate_weight,
    inner_weight,
    write_weight,
    read_weight,
    step_weight,
    step_bias,
    decay_log,
    skip_scale,
    inner_taps,
    access_taps,
    inner_history,
    access_history,
    recurrent,
    head_gain,
    mixer_out,
    moe_gain,
    expert_ids,
    route_scores,
    expert_gate,
    expert_up,
    expert_down,
    blend_vector,
    dense_gate,
    dense_up,
    dense_down,
):
    seq_count = tokens.shape[0]
    width = tokens.shape[1]
    heads_here = recurrent.shape[1]
    tp_index = lax.axis_index("tp")
    head_start = tp_index * heads_here
    normed = rms_scale(tokens.astype(jnp.float32), mix_gain).astype(jnp.bfloat16)
    stacked = jnp.concatenate(
        [gate_weight, inner_weight, write_weight, read_weight, step_weight], axis=1
    )
    projected = jnp.dot(
        normed,
        lax.all_gather(stacked, "ep", axis=0, tiled=True),
        preferred_element_type=jnp.float32,
    )
    inner_cols = inner_weight.shape[1]
    map_cols = write_weight.shape[1]
    offset = 2 * inner_cols
    gate_part = projected[:, :inner_cols].astype(jnp.bfloat16)
    inner_part = projected[:, inner_cols:offset].astype(jnp.bfloat16)
    write_part = projected[:, offset : offset + map_cols].astype(jnp.bfloat16)
    read_part = projected[:, offset + map_cols : offset + 2 * map_cols].astype(jnp.bfloat16)
    step_raw = projected[:, offset + 2 * map_cols :]
    inner_window = jnp.concatenate([inner_history, inner_part[:, None, :]], axis=1)
    inner_conv = jax.nn.silu(
        jnp.sum(inner_window.astype(jnp.float32) * inner_taps.astype(jnp.float32)[None], axis=1)
    )
    access_window = jnp.concatenate(
        [access_history, jnp.stack([write_part, read_part], axis=1)[:, :, None, :]], axis=2
    )
    access_conv = jax.nn.silu(
        jnp.sum(access_window.astype(jnp.float32) * access_taps.astype(jnp.float32)[None], axis=2)
    )
    per_group = HEADS // GROUPS
    write_all = jnp.repeat(access_conv[:, 0].reshape(seq_count, GROUPS, STATE), per_group, axis=1)
    read_all = jnp.repeat(access_conv[:, 1].reshape(seq_count, GROUPS, STATE), per_group, axis=1)
    write_heads = lax.dynamic_slice_in_dim(write_all, head_start, heads_here, 1)
    read_heads = lax.dynamic_slice_in_dim(read_all, head_start, heads_here, 1)
    step_own = lax.dynamic_slice_in_dim(step_raw, head_start, heads_here, 1)
    bias_own = lax.dynamic_slice_in_dim(step_bias, head_start, heads_here, 0)
    rate_own = lax.dynamic_slice_in_dim(decay_log, head_start, heads_here, 0)
    skip_own = lax.dynamic_slice_in_dim(skip_scale, head_start, heads_here, 0)
    step = jax.nn.softplus(step_own + bias_own[None, :])
    decay = jnp.exp(-step * jnp.exp(rate_own)[None, :])
    inner_heads = inner_conv.reshape(seq_count, heads_here, HEAD_DIM)
    new_recurrent = (
        decay[:, :, None, None] * recurrent
        + (step[:, :, None] * inner_heads)[..., None] * write_heads[:, :, None, :]
    )
    readout = (
        jnp.sum(new_recurrent * read_heads[:, :, None, :], axis=-1)
        + skip_own[None, :, None] * inner_heads
    )
    gated = readout * jax.nn.silu(
        gate_part.astype(jnp.float32).reshape(seq_count, heads_here, HEAD_DIM)
    )
    head_out = (
        rms_scale(gated, head_gain.reshape(heads_here, HEAD_DIM))
        .reshape(seq_count, heads_here * HEAD_DIM)
        .astype(jnp.bfloat16)
    )
    partial_mix = jnp.dot(head_out, mixer_out, preferred_element_type=jnp.float32)
    mixed = over_copies(partial_mix, "tp").astype(jnp.bfloat16)
    resid = tokens.astype(jnp.float32) + mixed.astype(jnp.float32)
    hidden = rms_scale(resid, moe_gain).astype(jnp.bfloat16)
    blend = jax.nn.sigmoid(jnp.dot(hidden, blend_vector, preferred_element_type=jnp.float32))
    slice_width = width // lax.axis_size("tp")
    own_cols = lax.dynamic_slice_in_dim(hidden, tp_index * slice_width, slice_width, 1)
    both_dense = jnp.concatenate([dense_gate, dense_up], axis=1)
    dense_partial = jnp.dot(
        gathered_copies(own_cols, "ep", 0), both_dense, preferred_element_type=jnp.float32
    )
    dense_inner = total_of(dense_partial, "tp")
    hidden_units = dense_gate.shape[1]
    dense_act = (jax.nn.silu(dense_inner[:, :hidden_units]) * dense_inner[:, hidden_units:]).astype(
        jnp.bfloat16
    )
    rows = dense_act
    dense_out = sent_and_summed(
        jnp.dot(rows, dense_down, preferred_element_type=jnp.float32), "ep", 0
    )
    experts = lax.axis_size("ep")
    capacity = max(2, 2 * seq_count * TOP // experts)
    flat_ids = expert_ids.reshape(-1)
    chosen = (flat_ids[:, None] == jnp.arange(experts)[None, :]).astype(jnp.int32)
    ranks = jnp.sum((jnp.cumsum(chosen, axis=0) - chosen) * chosen, axis=1)
    slots = flat_ids * capacity + ranks
    placing = (jnp.arange(experts * capacity)[:, None] == slots[None, :]).astype(jnp.bfloat16)
    repeated = jnp.repeat(hidden, TOP, axis=0)
    dispatch = (
        jnp.dot(placing, repeated, preferred_element_type=jnp.float32)
        .astype(jnp.bfloat16)
        .reshape(experts, capacity, width)
    )
    received = lax.all_to_all(dispatch, "ep", split_axis=0, concat_axis=0, tiled=True)
    rows = received.reshape(-1, width)
    gate_vals = jnp.dot(rows, expert_gate[0], preferred_element_type=jnp.float32)
    up_vals = jnp.dot(rows, expert_up[0], preferred_element_type=jnp.float32)
    act = (jax.nn.silu(gate_vals) * up_vals).astype(jnp.bfloat16)
    partial_out = jnp.dot(act, expert_down[0], preferred_element_type=jnp.float32)
    partial_out = partial_out.reshape(received.shape[0], received.shape[1], width)
    summed = sent_and_summed(partial_out, "tp", 2)
    returned = lax.all_to_all(
        summed.astype(jnp.bfloat16), "ep", split_axis=0, concat_axis=0, tiled=True
    )
    picked_back = jnp.dot(
        placing.T,
        returned.reshape(experts * capacity, slice_width),
        preferred_element_type=jnp.float32,
    )
    first = jax.nn.sigmoid(route_scores[:, 0] - route_scores[:, 1])
    weights = jnp.stack([first, 1.0 - first], axis=1).reshape(-1)
    routed = jnp.sum((picked_back * weights[:, None]).reshape(seq_count, TOP, slice_width), axis=1)
    resid_part = lax.dynamic_slice_in_dim(resid, tp_index * slice_width, slice_width, 1)
    output = resid_part + routed + blend[:, None] * dense_out
    return (output, new_recurrent, inner_window[:, 1:], access_window[:, :, 1:])


def solution(mesh):
    in_specs = (
        P("ep", None),
        P(),
        P("ep", "tp"),
        P("ep", "tp"),
        P("ep", None),
        P("ep", None),
        P("ep", None),
        P(),
        P(),
        P(),
        P(None, "tp"),
        P(),
        P("ep", None, "tp"),
        P("ep", None, None, None),
        P("ep", "tp", None, None),
        P("tp"),
        P("tp", None),
        P(),
        P("ep", None),
        P("ep", None),
        P("ep", None, "tp"),
        P("ep", None, "tp"),
        P("ep", "tp", None),
        P(),
        P("tp", "ep"),
        P("tp", "ep"),
        P("ep", "tp"),
    )
    out_specs = (
        P("ep", "tp"),
        P("ep", "tp", None, None),
        P("ep", None, "tp"),
        P("ep", None, None, None),
    )
    return jax.shard_map(local, mesh=mesh, in_specs=in_specs, out_specs=out_specs, check_vma=False)
```

profile of v0, /device:TPU:1, one launch (start us, length us, event | category | flops | bytes accessed | tf_op | source)
XLA Modules:
  0.0 332.0 jit_solution(13312532237748975122)
XLA Ops:
  7.3 0.9 copy.82
  8.2 1.7 concatenate.12
  9.9 0.7 copy.84
  10.6 1.2 dynamic_slice.26
  12.5 1.2 dynamic_slice.25
  13.7 0.7 convert_element_type.57
  14.4 1.3 dynamic_slice.29
  15.7 1.0 constant_dynamic-update-slice_fusion
  16.6 1.0 fusion.11
  17.6 73.8 %all-gather.3.cloned.1.call-done = bf16[2048,1168]{1,0:T(8,128)(2,1)} async-done(((bf16[64,1168]{1,0:T(8,128)(2,1)}), bf16[2048,1168]{1,0:T(8,128)(2,1)}) %all-gather.3.cloned.1.call-update) | async-done | bytes 4784144 | tf_op jit(solution)/shard_map/all_gather | solution.py:108
  91.4 3.4 %fusion.39 = (bf16[16,1168]{1,0:T(8,128)(2,1)S(1)}, f32[16,1168]{1,0:T(8,128)S(1)}) fusion(bf16[2048,1168]{1,0:T(8,128)(2,1)} %all-gather.3.cloned.1.call-done, bf16[16,2048]{1,0:T(8,128)(2,1)} %param.27, f32[2048]{0:T(1024)} %param.28, f32[16]{0:T(128)S(1)} %add_rsqrt_fusion.2), kind=kOutput, calls=%fused_computation.83 | convolution fusion | flops 76695808 | bytes 4970048 | tf_op jit(solution)/shard_map/dot_general | solution.py:106
  94.8 0.1 slice_bitcast_fusion.2
  94.9 0.2 multiply_reduce_fusion.1
  95.1 0.1 divide_multiply_fusion
  95.2 0.1 fusion.38
  95.3 0.9 exponential_reduce_fusion
  96.2 0.1 broadcast_multiply_fusion
  96.3 1.0 multiply_reduce_fusion
  97.3 0.8 multiply_reduce_fusion.4
  98.1 0.2 fusion.31
  98.3 1.6 broadcast_in_dim.18
  99.9 6.5 %all-to-all-start = ((f32[16,16,2048]{2,1,0:T(8,128)}), f32[16,16,2048]{2,1,0:T(8,128)S(1)}, u32[]{:S(2)}, u32[]{:S(2)}) async-start(f32[16,16,2048]{2,1,0:T(8,128)} %broadcast_in_dim.18), calls=%async_computation | async-start | bytes 4194304 | tf_op jit(solution)/shard_map/all_to_all | solution.py:18
  106.5 0.1 copy.87
  106.5 0.1 reshape.162
  106.6 0.1 fusion.25
  106.7 0.1 reduce_window_sum.11
  106.8 0.4 copy-done.12
  107.1 31.8 %all-to-all-done = f32[16,16,2048]{2,1,0:T(8,128)S(1)} async-done(((f32[16,16,2048]{2,1,0:T(8,128)}), f32[16,16,2048]{2,1,0:T(8,128)S(1)}, u32[]{:S(2)}, u32[]{:S(2)}) %all-to-all-start) | async-done | bytes 2097184 | tf_op jit(solution)/shard_map/all_to_all | solution.py:18
  139.0 0.1 reduce_sum.104
  139.1 0.1 multiply_reduce_fusion.2
  139.3 0.9 multiply_convert_fusion
  140.2 0.7 broadcast_in_dim.20
  140.9 9.0 %all-to-all-start.4 = ((bf16[32,16,128]{2,1,0:T(8,128)(2,1)}), bf16[32,16,128]{2,1,0:T(8,128)(2,1)S(1)}, u32[]{:S(2)}, u32[]{:S(2)}) async-start(bf16[32,16,128]{2,1,0:T(8,128)(2,1)} %broadcast_in_dim.20), calls=%async_computation.4 | async-start | bytes 262144 | tf_op jit(solution)/shard_map/all_to_all | solution.py:18
  149.8 0.8 select_reduce_fusion
  150.7 0.7 multiply_add_fusion.2
  151.3 0.1 broadcast_in_dim.19
  151.4 0.1 reshape.163
  151.5 0.2 convolution_convert_fusion
  151.7 0.9 reshape.164
  152.6 13.1 %all-to-all-done.4 = bf16[32,16,128]{2,1,0:T(8,128)(2,1)S(1)} async-done(((bf16[32,16,128]{2,1,0:T(8,128)(2,1)}), bf16[32,16,128]{2,1,0:T(8,128)(2,1)S(1)}, u32[]{:S(2)}, u32[]{:S(2)}) %all-to-all-start.4) | async-done | bytes 131104 | tf_op jit(solution)/shard_map/all_to_all | solution.py:18
  165.7 5.1 %all-to-all-start.1 = ((bf16[32,2,2048]{2,1,0:T(2,128)(2,1)}), bf16[32,2,2048]{2,1,0:T(2,128)(2,1)S(1)}, u32[]{:S(2)}, u32[]{:S(2)}) async-start(bf16[32,2,2048]{2,1,0:T(2,128)(2,1)} %reshape.164), calls=%async_computation.1 | async-start | bytes 524288 | tf_op jit(solution)/shard_map/all_to_all | solution.py:190
  170.9 2.1 fusion.14
  173.0 0.5 copy.97
  173.6 18.9 %all-to-all-done.1 = bf16[32,2,2048]{2,1,0:T(2,128)(2,1)S(1)} async-done(((bf16[32,2,2048]{2,1,0:T(2,128)(2,1)}), bf16[32,2,2048]{2,1,0:T(2,128)(2,1)S(1)}, u32[]{:S(2)}, u32[]{:S(2)}) %all-to-all-start.1) | async-done | bytes 262176 | tf_op jit(solution)/shard_map/all_to_all | solution.py:190
  192.4 0.1 reshape.165
  192.6 0.3 fusion.6
  192.9 1.6 fusion
  194.5 0.4 convolution_bitcast_fusion
  195.0 13.6 %all_to_all.30 = f32[16,32,2,128]{3,1,2,0:T(8,128)S(1)} all-to-all(f32[16,32,2,128]{3,1,2,0:T(8,128)S(1)} %copy.90), channel_id=1, replica_groups=mesh['ep'=32,'tp'=16] {'tp'}, dimensions={0} | all-to-all | bytes 1048576 | tf_op jit(solution)/shard_map/all_to_all | solution.py:59
  208.6 0.6 copy.92
  209.2 5.9 %all-to-all-start.3 = ((bf16[32,2,128]{2,1,0:T(2,128)(2,1)}), bf16[32,2,128]{2,1,0:T(2,128)(2,1)S(1)}, u32[]{:S(2)}, u32[]{:S(2)}) async-start(bf16[32,2,128]{2,1,0:T(2,128)(2,1)} %copy.92), calls=%async_computation.3 | async-start | bytes 32768 | tf_op jit(solution)/shard_map/all_to_all | solution.py:198
  215.1 46.5 %reduce-scatter.2.cloned.1.call-done = f32[32,448]{1,0:T(8,128)} async-done(((f32[512,448]{1,0:T(8,128)}), f32[32,448]{1,0:T(8,128)}) %reduce-scatter.2.cloned.1.call-update) | async-done | bytes 57360 | tf_op jit(solution)/shard_map/reduce_scatter | solution.py:45
  261.7 18.3 %all-gather = f32[512,448]{1,0:T(8,128)S(1)} all-gather(f32[32,448]{1,0:T(8,128)} %reduce-scatter.2.cloned.1.call-done), channel_id=2, replica_groups=mesh['ep'=32,'tp'=16] {'tp'}, dimensions={0}, use_global_device_ids=true | all-gather | bytes 974848 | tf_op jit(solution)/shard_map/all_gather | solution.py:48
  279.9 1.0 fusion.9
  280.9 20.5 %all-to-all-start.5 = ((f32[32,16,128]{2,1,0:T(8,128)}), f32[32,16,128]{2,1,0:T(8,128)S(1)}, u32[]{:S(2)}, u32[]{:S(2)}) async-start(f32[32,16,128]{2,1,0:T(8,128)} %bitcast.25), calls=%async_computation.6 | async-start | bytes 524288 | tf_op jit(solution)/shard_map/all_to_all | solution.py:59
  301.5 0.1 copy.93
  301.6 0.1 mul.275
  301.7 0.7 slice.67
  302.5 0.6 fusion.26
  303.1 0.1 fusion.4
  303.2 0.1 convolution_multiply_fusion.1
  303.3 0.1 reduce_sum.108
  303.4 20.3 %all-to-all-done.5 = f32[32,16,128]{2,1,0:T(8,128)S(1)} async-done(((f32[32,16,128]{2,1,0:T(8,128)}), f32[32,16,128]{2,1,0:T(8,128)S(1)}, u32[]{:S(2)}, u32[]{:S(2)}) %all-to-all-start.5) | async-done | bytes 262176 | tf_op jit(solution)/shard_map/all_to_all | solution.py:59
  323.8 1.4 multiply_add_fusion.1
  (61 shorter events, 0.5 us)
Async XLA Ops:
  7.2 185.4 %copy-start = (bf16[1,2048,256]{2,1,0:T(8,128)(2,1)S(1)}, bf16[1,2048,256]{2,1,0:T(8,128)(2,1)}, u32[]{:S(2)}) copy-start(bf16[1,2048,256]{2,1,0:T(8,128)(2,1)} %param.47) | copy-start | bytes 3145732
  7.2 89.0 %copy-start.8 = (bf16[16,3,64]{2,0,1:T(8,128)(2,1)S(1)}, bf16[16,3,64]{2,0,1:T(8,128)(2,1)}, u32[]{:S(2)}) copy-start(bf16[16,3,64]{2,0,1:T(8,128)(2,1)} %param.39) | copy-start | bytes 18436
  7.2 89.1 %copy-start.4 = (f32[16,1,64,128]{3,2,1,0:T(8,128)S(1)}, f32[16,1,64,128]{3,2,1,0:T(8,128)}, u32[]{:S(2)}) copy-start(f32[16,1,64,128]{3,2,1,0:T(8,128)} %param.41) | copy-start | bytes 1572868
  7.2 90.9 %copy-start.7 = (bf16[64,2048]{1,0:T(8,128)(2,1)S(1)}, bf16[64,2048]{1,0:T(8,128)(2,1)}, u32[]{:S(2)}) copy-start(bf16[64,2048]{1,0:T(8,128)(2,1)} %param.43) | copy-start | bytes 786436
  7.2 90.9 %copy-start.16 = (f32[64]{0:T(128)S(1)}, f32[64]{0:T(128)}, u32[]{:S(2)}) copy-start(f32[64]{0:T(128)} %param.42) | copy-start | bytes 772
  7.2 84.2 %all-gather.3.cloned.1.call-start = ((), (), s32[]{:S(2)}) async-start(), calls=%async_computation.7 | async-start | bytes 5406720 | tf_op jit(solution)/shard_map/all_gather | solution.py:108
  94.8 11.7 %copy-start.14 = (s32[16,2]{0,1:T(2,128)S(1)}, s32[16,2]{0,1:T(2,128)}, u32[]{:S(2)}) copy-start(s32[16,2]{0,1:T(2,128)} %param.45) | copy-start | bytes 388
  94.9 11.9 %copy-start.10 = (bf16[16,1,64]{2,0,1:T(8,128)(2,1)}, bf16[16,1,64]{2,0,1:T(8,128)(2,1)S(1)}, u32[]{:S(2)}) copy-start(bf16[16,1,64]{2,0,1:T(8,128)(2,1)S(1)} %slice_bitcast_fusion.2) | copy-start | bytes 6148
  95.3 43.8 %copy-start.2 = (bf16[16,2048]{1,0:T(8,128)(2,1)S(1)}, bf16[16,2048]{1,0:T(8,128)(2,1)}, u32[]{:S(2)}) copy-start(bf16[16,2048]{1,0:T(8,128)(2,1)} %param.27) | copy-start | bytes 196612
  99.9 39.1 %all-to-all-start = ((f32[16,16,2048]{2,1,0:T(8,128)}), f32[16,16,2048]{2,1,0:T(8,128)S(1)}, u32[]{:S(2)}, u32[]{:S(2)}) async-start(f32[16,16,2048]{2,1,0:T(8,128)} %broadcast_in_dim.18), calls=%async_computation | async-start | bytes 4194304 | tf_op jit(solution)/shard_map/all_to_all | solution.py:18
  106.6 0.5 copy-start.12
  139.1 33.9 %copy-start.1 = (bf16[1,256,2048]{2,1,0:T(8,128)(2,1)S(1)}, bf16[1,256,2048]{2,1,0:T(8,128)(2,1)}, u32[]{:S(2)}) copy-start(bf16[1,256,2048]{2,1,0:T(8,128)(2,1)} %param.49) | copy-start | bytes 3145732
  139.3 26.4 %copy-start.3 = (f32[16,2048]{1,0:T(8,128)}, f32[16,2048]{1,0:T(8,128)S(1)}, u32[]{:S(2)}) copy-start(f32[16,2048]{1,0:T(8,128)S(1)} %get-tuple-element.9) | copy-start | bytes 393220
  140.2 25.5 %copy-start.5 = (bf16[16,2048]{1,0:T(8,128)(2,1)}, bf16[16,2048]{1,0:T(8,128)(2,1)S(1)}, u32[]{:S(2)}) copy-start(bf16[16,2048]{1,0:T(8,128)(2,1)S(1)} %multiply_convert_fusion) | copy-start | bytes 196612
  140.9 24.8 %all-to-all-start.4 = ((bf16[32,16,128]{2,1,0:T(8,128)(2,1)}), bf16[32,16,128]{2,1,0:T(8,128)(2,1)S(1)}, u32[]{:S(2)}, u32[]{:S(2)}) async-start(bf16[32,16,128]{2,1,0:T(8,128)(2,1)} %broadcast_in_dim.20), calls=%async_computation.4 | async-start | bytes 262144 | tf_op jit(solution)/shard_map/all_to_all | solution.py:18
  165.7 26.7 %all-to-all-start.1 = ((bf16[32,2,2048]{2,1,0:T(2,128)(2,1)}), bf16[32,2,2048]{2,1,0:T(2,128)(2,1)S(1)}, u32[]{:S(2)}, u32[]{:S(2)}) async-start(bf16[32,2,2048]{2,1,0:T(2,128)(2,1)} %reshape.164), calls=%async_computation.1 | async-start | bytes 524288 | tf_op jit(solution)/shard_map/all_to_all | solution.py:190
  170.8 90.8 %reduce-scatter.2.cloned.1.call-start = ((), (), s32[]{:S(2)}) async-start(), calls=%async_computation.8 | async-start | bytes 1114112 | tf_op jit(solution)/shard_map/reduce_scatter | solution.py:45
  173.6 106.4 %copy-start.17 = (bf16[224,128]{1,0:T(8,128)(2,1)S(1)}, bf16[224,128]{1,0:T(8,128)(2,1)}, u32[]{:S(2)}) copy-start(bf16[224,128]{1,0:T(8,128)(2,1)} %param.53) | copy-start | bytes 172036
  192.9 108.6 %copy-start.15 = (f32[16,2]{0,1:T(2,128)S(1)}, f32[16,2]{0,1:T(2,128)}, u32[]{:S(2)}) copy-start(f32[16,2]{0,1:T(2,128)} %param.46) | copy-start | bytes 388
  192.9 108.8 %copy-start.13 = (bf16[2048]{0:T(1024)(128)(2,1)S(1)}, bf16[2048]{0:T(1024)(128)(2,1)}, u32[]{:S(2)}) copy-start(bf16[2048]{0:T(1024)(128)(2,1)} %param.50) | copy-start | bytes 12292
  192.9 109.6 %copy-start.9 = (bf16[16,3,64]{2,0,1:T(8,128)(2,1)S(1)}, bf16[16,3,64]{2,0,1:T(8,128)(2,1)}, u32[]{:S(2)}) copy-start(bf16[16,3,64]{2,0,1:T(8,128)(2,1)} %param.39) | copy-start | bytes 18436
  192.9 109.6 %copy-start.11 = (bf16[16,1,64]{2,0,1:T(8,128)(2,1)S(1)}, bf16[16,1,64]{2,0,1:T(8,128)(2,1)}, u32[]{:S(2)}) copy-start(bf16[16,1,64]{2,0,1:T(8,128)(2,1)} %copy-done.10) | copy-start | bytes 6148
  192.9 110.2 %copy-start.6 = (bf16[16,2048]{1,0:T(8,128)(2,1)S(1)}, bf16[16,2048]{1,0:T(8,128)(2,1)}, u32[]{:S(2)}) copy-start(bf16[16,2048]{1,0:T(8,128)(2,1)} %copy-done.5) | copy-start | bytes 196612
  209.2 71.7 %all-to-all-start.3 = ((bf16[32,2,128]{2,1,0:T(2,128)(2,1)}), bf16[32,2,128]{2,1,0:T(2,128)(2,1)S(1)}, u32[]{:S(2)}, u32[]{:S(2)}) async-start(bf16[32,2,128]{2,1,0:T(2,128)(2,1)} %copy.92), calls=%async_computation.3 | async-start | bytes 32768 | tf_op jit(solution)/shard_map/all_to_all | solution.py:198
  280.9 42.8 %all-to-all-start.5 = ((f32[32,16,128]{2,1,0:T(8,128)}), f32[32,16,128]{2,1,0:T(8,128)S(1)}, u32[]{:S(2)}, u32[]{:S(2)}) async-start(f32[32,16,128]{2,1,0:T(8,128)} %bitcast.25), calls=%async_computation.6 | async-start | bytes 524288 | tf_op jit(solution)/shard_map/all_to_all | solution.py:59
Sparse Core Ops, SparseCore 0:
  10.7 80.6 all-gather.2
  175.7 85.9 reduce-scatter.1
where the time goes:
time: 333 us; the launch traced here: 332 us
  waiting for transfers between devices  204 us (61%)
  starting transfers between devices  47.1 us (14%)
  blocking collectives  31.8 us (10%)
  between operations  15.2 us (5%)
  local copies, waits for them, and re-layouts  14.3 us (4%)
  other arithmetic  9.57 us (3%)
  matrix products  9.5 us (3%)
    all_gather x1, waiting for transfers between devices, local(): lax.all_gather(stacked, 'ep', axis=0, tiled=True)  73.8 us
    reduce_scatter x1, waiting for transfers between devices, total_of(): lax.psum_scatter(rows_for(lines, lax.axis_size(axis)), axis, scatter_dime...  46.5 us
    all_to_all x2, waiting for transfers between devices, from_everyone(): return lax.all_to_all(copies, axis, split_axis=0, concat_axis=0, tiled=True)  44.9 us
    all_to_all x1, starting transfers between devices, sent_and_summed(): lax.all_to_all(pieces, axis, split_axis=0, concat_axis=0, tiled=True)  20.5 us
    all_to_all x1, waiting for transfers between devices, sent_and_summed(): lax.all_to_all(pieces, axis, split_axis=0, concat_axis=0, tiled=True)  20.3 us
    all_to_all x1, waiting for transfers between devices, local(): lax.all_to_all(dispatch, 'ep', split_axis=0, concat_axis=0, tiled=True)  18.9 us
    all_gather x1, blocking collectives, total_of(): whole = lax.all_gather(own, axis).reshape(-1, *lines.shape[1:])  18.3 us
    all_to_all x2, starting transfers between devices, from_everyone(): return lax.all_to_all(copies, axis, split_axis=0, concat_axis=0, tiled=True)  15.5 us
  transfers between devices with their start and end apart: 7, of which 6 were waited for; matrix products, arithmetic and copies ran while one was open for 6% of the time, Pallas kernels for 0%

commit v1 on v0

v1 whole, which is shorter than its diff:
```python
import jax
import jax.numpy as jnp
from jax import lax
from jax.sharding import PartitionSpec as P

HEADS = 16
HEAD_DIM = 64
GROUPS = 4
STATE = 128
TOP = 2
PER_GROUP = HEADS // GROUPS
EPS = 1e-06
BF = jnp.bfloat16
F32 = jnp.float32
CORES = 2


def exchange(pieces, axis, groups=None):
    return lax.all_to_all(
        pieces, axis, split_axis=0, concat_axis=0, tiled=True, axis_index_groups=groups
    )


def to_everyone(shard, peers):
    return jnp.broadcast_to(shard[None], (peers, *shard.shape))


def rms_scale(values, gain):
    mean_square = jnp.mean(values * values, axis=-1, keepdims=True)
    return values * lax.rsqrt(mean_square + EPS) * gain


def dot32(left, right):
    return jnp.dot(left, right, preferred_element_type=F32)


def slice_at(array, start, size, dim):
    return lax.dynamic_slice_in_dim(array, start, size, dim)


def local(
    tokens,
    mix_gain,
    gate_weight,
    inner_weight,
    write_weight,
    read_weight,
    step_weight,
    step_bias,
    decay_log,
    skip_scale,
    inner_taps,
    access_taps,
    inner_history,
    access_history,
    recurrent,
    head_gain,
    mixer_out,
    moe_gain,
    expert_ids,
    route_scores,
    expert_gate,
    expert_up,
    expert_down,
    blend_vector,
    dense_gate,
    dense_up,
    dense_down,
):
    seqs, width = tokens.shape
    n_ep = lax.axis_size("ep")
    n_tp = lax.axis_size("tp")
    chips = n_ep // CORES
    ep = lax.axis_index("ep")
    tp = lax.axis_index("tp")
    core = ep % CORES
    group = tp // PER_GROUP
    rows_k = gate_weight.shape[0]
    cols = width // n_tp
    same_core = [[CORES * z + c for z in range(chips)] for c in range(CORES)]
    swap = [(i, i ^ 1) for i in range(n_ep)]

    write_own = slice_at(write_weight, group * STATE, STATE, 1)
    read_own = slice_at(read_weight, group * STATE, STATE, 1)
    main = jnp.concatenate([gate_weight, inner_weight, write_own, read_own], axis=1)
    pack_cols = main.shape[1]
    head_pick = (jnp.arange(HEADS) == tp).astype(BF)[None]
    step_row = lax.dot_general(
        head_pick, step_weight, (((1,), (1,)), ((), ())), preferred_element_type=F32
    ).astype(BF)
    first = jax.nn.sigmoid(route_scores[:, 0] - route_scores[:, 1])
    first_high = first.astype(BF).astype(F32)
    first_low = first - first_high
    lane = jnp.arange(4 * seqs)[None]
    spread = jnp.where(
        lane < seqs,
        expert_ids[:, 0:1].astype(F32),
        jnp.where(
            lane < 2 * seqs,
            expert_ids[:, 1:2].astype(F32),
            jnp.where(lane < 3 * seqs, first_high[:, None], first_low[:, None]),
        ),
    )
    route_row = jnp.sum(
        jnp.where(lane % seqs == jnp.arange(seqs)[:, None], spread, 0.0), axis=0, keepdims=True
    ).astype(BF)
    extra = jnp.concatenate([step_row, route_row, jnp.zeros((6, rows_k), BF)], axis=0)
    extra = jnp.pad(extra, ((0, 0), (0, pack_cols - rows_k)))
    pack = jnp.concatenate([main, extra], axis=0)
    own_pack = exchange(to_everyone(pack, chips), "ep", same_core)
    other_pack = lax.ppermute(own_pack, "ep", swap)

    normed = rms_scale(tokens.astype(F32), mix_gain).astype(BF)
    by_core = normed.reshape(seqs, chips, CORES, rows_k)
    own_k = jnp.where(core == 0, by_core[:, :, 0], by_core[:, :, 1])
    other_k = jnp.where(core == 0, by_core[:, :, 1], by_core[:, :, 0])

    def projected_by(keys, packed):
        padded = jnp.pad(keys, ((0, 0), (0, 0), (0, packed.shape[1] - rows_k)))
        main_part = dot32(padded.reshape(seqs, -1), packed.reshape(-1, pack_cols))
        weights = packed[:, rows_k, :rows_k].astype(F32)
        step_part = jnp.sum(keys.astype(F32) * weights[None], axis=(1, 2))
        return main_part, step_part

    main_a, step_a = projected_by(own_k, own_pack)
    main_b, step_b = projected_by(other_k, other_pack)
    projected = main_a + main_b
    step_raw = step_a + step_b
    gate_part = projected[:, :HEAD_DIM].astype(BF)
    inner_part = projected[:, HEAD_DIM : 2 * HEAD_DIM].astype(BF)
    write_part = projected[:, 2 * HEAD_DIM : 2 * HEAD_DIM + STATE].astype(BF)
    read_part = projected[:, 2 * HEAD_DIM + STATE :].astype(BF)

    inner_window = jnp.concatenate([inner_history, inner_part[:, None, :]], axis=1)
    inner_conv = jax.nn.silu(
        jnp.sum(inner_window.astype(F32) * inner_taps.astype(F32)[None], axis=1)
    )
    history_own = slice_at(access_history, group * STATE, STATE, 3).astype(F32)
    taps_own = slice_at(access_taps, group * STATE, STATE, 2).astype(F32)

    def access_conv(which, part):
        taps = taps_own[which]
        past = jnp.sum(history_own[:, which] * taps[None, :3], axis=1)
        return jax.nn.silu(past + part.astype(F32) * taps[3][None])

    write_conv = access_conv(0, write_part)
    read_conv = access_conv(1, read_part)
    bias_own = slice_at(step_bias, tp, 1, 0)
    rate_own = slice_at(decay_log, tp, 1, 0)
    skip_own = slice_at(skip_scale, tp, 1, 0)
    step = jax.nn.softplus(step_raw + bias_own)
    decay = jnp.exp(-step * jnp.exp(rate_own))
    new_recurrent = (
        decay[:, None, None] * recurrent[:, 0]
        + (step[:, None] * inner_conv)[..., None] * write_conv[:, None, :]
    )
    readout = jnp.sum(new_recurrent * read_conv[:, None, :], axis=-1) + skip_own * inner_conv
    gated = readout * jax.nn.silu(gate_part.astype(F32))
    head_out = rms_scale(gated, head_gain).astype(BF)

    partial_mix = dot32(head_out, mixer_out)
    mix_pieces = partial_mix.reshape(seqs, n_tp, cols).transpose(1, 0, 2)
    parts_sent = jnp.where(tp % 2 == 0, write_part, read_part).astype(F32)
    arrived = exchange(
        jnp.concatenate([mix_pieces, to_everyone(parts_sent, n_tp)], axis=1), "tp"
    )
    mixed = jnp.sum(arrived[:, :seqs], axis=0).astype(BF)
    parts_all = arrived[:, seqs:].astype(BF).reshape(GROUPS, PER_GROUP, seqs, STATE)[:, :2]
    parts_all = parts_all.transpose(2, 1, 0, 3).reshape(seqs, 2, 1, GROUPS * STATE)
    new_access = jnp.concatenate([access_history[:, :, 1:], parts_all], axis=2)

    resid = slice_at(tokens, tp * cols, cols, 1).astype(F32) + mixed.astype(F32)
    gain_own = slice_at(moe_gain, tp * cols, cols, 0)
    scaled = (resid * gain_own).astype(BF)
    scaled_all = exchange(to_everyone(scaled, n_ep), "ep").reshape(n_ep * seqs, cols)

    own_routes = own_pack[:, rows_k + 1, : 4 * seqs].astype(F32)
    other_routes = other_pack[:, rows_k + 1, : 4 * seqs].astype(F32)
    routes = jnp.where(
        core == 0,
        jnp.stack([own_routes, other_routes], axis=1),
        jnp.stack([other_routes, own_routes], axis=1),
    ).reshape(n_ep, 4 * seqs)
    mine = ep.astype(F32)
    is_first = routes[:, :seqs] == mine
    is_second = routes[:, seqs : 2 * seqs] == mine
    first_all = routes[:, 2 * seqs : 3 * seqs] + routes[:, 3 * seqs :]
    weight = jnp.where(is_first, first_all, 1.0 - first_all)
    named = is_first | is_second
    earlier = (jnp.arange(seqs)[:, None] < jnp.arange(seqs)[None]).astype(BF)
    rank = dot32(named.astype(BF), earlier)
    key = jnp.where(named, rank, -1.0)
    total = n_ep * seqs
    place = jnp.arange(total)[None]
    tiled = (place % seqs == jnp.arange(seqs)[:, None]).astype(F32)
    own_block = place // seqs == jnp.arange(n_ep)[:, None]
    spread = jnp.dot(
        jnp.concatenate([key, weight], axis=0), tiled, precision=lax.Precision.HIGHEST
    )
    key_row = jnp.sum(jnp.where(own_block, spread[:n_ep], 0.0), axis=0, keepdims=True)
    weight_row = jnp.sum(jnp.where(own_block, spread[n_ep:], 0.0), axis=0, keepdims=True)
    slots = TOP * n_ep
    slot = jnp.arange(slots)[:, None]
    chosen = (slot // TOP == place // seqs) & (key_row == (slot % TOP).astype(F32))
    slot_weight = jnp.sum(jnp.where(chosen, weight_row, 0.0), axis=1, keepdims=True)
    chosen = chosen.astype(BF)

    units = dense_gate.shape[1]
    half = -(-(units + 2) // 128) * 128
    blend_col = slice_at(blend_vector, tp * cols, cols, 0)[:, None]
    both_dense = jnp.concatenate(
        [
            dense_gate,
            blend_col,
            jnp.zeros((cols, half - units - 1), BF),
            dense_up,
            jnp.zeros((cols, half - units), BF),
        ],
        axis=1,
    )
    plain = scaled_all.astype(F32) / gain_own
    square_sum = jnp.sum(plain * plain, axis=1, keepdims=True)
    dense_partial = dot32(scaled_all, both_dense)
    dense_partial = jnp.where(
        jnp.arange(2 * half)[None] == units + 1, square_sum, dense_partial
    ).astype(BF)
    expert_rows = dot32(chosen, scaled_all).astype(BF)
    quarter = slots * cols // (2 * half)
    expert_block = (
        expert_rows.reshape(slots // quarter, quarter, cols)
        .transpose(1, 0, 2)
        .reshape(quarter, 2 * half)
    )
    share = total // n_tp
    arrived = exchange(
        jnp.concatenate(
            [dense_partial.reshape(n_tp, share, 2 * half), to_everyone(expert_block, n_tp)],
            axis=1,
        ),
        "tp",
    )
    dense_inner = jnp.sum(arrived[:, :share].astype(F32), axis=0)
    rows = (
        arrived[:, share:]
        .reshape(n_tp, quarter, slots // quarter, cols)
        .transpose(2, 1, 0, 3)
        .reshape(slots, width)
    )
    plain_rows = rows.astype(F32) / moe_gain
    row_scale = lax.rsqrt(jnp.mean(plain_rows * plain_rows, axis=1, keepdims=True) + EPS)
    gate_vals = dot32(rows, expert_gate[0]) * row_scale
    up_vals = dot32(rows, expert_up[0]) * row_scale
    act = (jax.nn.silu(gate_vals) * up_vals).astype(BF)
    partial_out = dot32(act, expert_down[0]).astype(BF)
    out_pieces = partial_out.reshape(slots, n_tp, cols).transpose(1, 0, 2)
    scale = lax.rsqrt(dense_inner[:, units + 1 : units + 2] / width + EPS)
    blend = jax.nn.sigmoid(dense_inner[:, units : units + 1] * scale)
    dense_act = (
        blend * jax.nn.silu(dense_inner[:, :half] * scale) * (dense_inner[:, half:] * scale)
    ).astype(BF)
    act_block = jnp.concatenate([dense_act[:, :128], dense_act[:, 128:]], axis=0)
    arrived = exchange(
        jnp.concatenate([out_pieces, to_everyone(act_block, n_tp)], axis=1), "tp"
    )
    expert_out = jnp.sum(arrived[:, :slots].astype(F32), axis=0) * slot_weight
    down = jnp.pad(dense_down, ((0, half - units), (0, 0)))
    summed = (
        dot32(arrived[:, slots : slots + share].reshape(total, 128), down[:128])
        + dot32(arrived[:, slots + share :].reshape(total, 128), down[128:])
        + lax.dot_general(
            chosen, expert_out.astype(BF), (((0,), (0,)), ((), ())), preferred_element_type=F32
        )
    )
    final = exchange(summed.astype(BF).reshape(n_ep, seqs, cols), "ep")
    output = resid + jnp.sum(final.astype(F32), axis=0)
    return (output, new_recurrent[:, None], inner_window[:, 1:], new_access)


def solution(mesh):
    in_specs = (
        P("ep", None),
        P(),
        P("ep", "tp"),
        P("ep", "tp"),
        P("ep", None),
        P("ep", None),
        P("ep", None),
        P(),
        P(),
        P(),
        P(None, "tp"),
        P(),
        P("ep", None, "tp"),
        P("ep", None, None, None),
        P("ep", "tp", None, None),
        P("tp"),
        P("tp", None),
        P(),
        P("ep", None),
        P("ep", None),
        P("ep", None, "tp"),
        P("ep", None, "tp"),
        P("ep", "tp", None),
        P(),
        P("tp", "ep"),
        P("tp", "ep"),
        P("ep", "tp"),
    )
    out_specs = (
        P("ep", "tp"),
        P("ep", "tp", None, None),
        P("ep", None, "tp"),
        P("ep", None, None, None),
    )
    return jax.shard_map(local, mesh=mesh, in_specs=in_specs, out_specs=out_specs, check_vma=False)
```

time: 333 us -> 176 us (0.53)
  waiting for transfers between devices: 204 us -> 80.4 us
  blocking collectives: 31.8 us -> 15.1 us
  between operations: 15.2 us -> 1.99 us
  local copies, waits for them, and re-layouts: 14.3 us -> 7.13 us
  starting transfers between devices: 47.1 us -> 52.5 us
    all_gather x1 -> x0, waiting for transfers between devices: 73.8 us -> none  [local(): lax.all_gather(stacked, 'ep', axis=0, tiled=True)]
    reduce_scatter x1 -> x0, waiting for transfers between devices: 46.5 us -> none  [total_of(): lax.psum_scatter(rows_for(lines, lax.axis_size(axis)), axis, scatter_dime...]
    all_gather x1 -> x0, blocking collectives: 18.3 us -> none  [total_of(): whole = lax.all_gather(own, axis).reshape(-1, *lines.shape[1:])]
    ppermute x0 -> x1, starting transfers between devices: none -> 7.09 us  [local(): other_pack = lax.ppermute(own_pack, 'ep', swap)]
    all_to_all x5, waiting for transfers between devices: 84.1 us -> 78.6 us  [exchange(): lax.all_to_all(pieces, axis, split_axis=0, concat_axis=0, tiled=True, axi...]
    dot_general x10 -> x13, matrix products: 9.5 us -> 6.28 us  [the longest x10 4.83 us: dot32(): return jnp.dot(left, right, preferred_element_type=F32)]
  transfers between devices with their start and end apart: 7 -> 6, of which waited for: 6 -> 6; matrix products, arithmetic and copies ran while one was open for 6% -> 4% of each run, Pallas kernels for 0% -> 0%
where the time goes in v1:
time: 176 us; the launch traced here: 175 us
  waiting for transfers between devices  80.4 us (46%)
  starting transfers between devices  52.5 us (30%)
  blocking collectives  15.1 us (9%)
  other arithmetic  11.5 us (7%)
  local copies, waits for them, and re-layouts  7.13 us (4%)
  matrix products  6.28 us (4%)
  between operations  1.99 us (1%)
    all_to_all x5, waiting for transfers between devices, exchange(): lax.all_to_all(pieces, axis, split_axis=0, concat_axis=0, tiled=True, axi...  78.6 us
    all_to_all x5, starting transfers between devices, exchange(): lax.all_to_all(pieces, axis, split_axis=0, concat_axis=0, tiled=True, axi...  45.5 us
    all_to_all x1, blocking collectives, exchange(): lax.all_to_all(pieces, axis, split_axis=0, concat_axis=0, tiled=True, axi...  15.1 us
    ppermute x1, starting transfers between devices, local(): other_pack = lax.ppermute(own_pack, 'ep', swap)  7.09 us
    dot_general x10, matrix products, dot32(): return jnp.dot(left, right, preferred_element_type=F32)  4.83 us
  transfers between devices with their start and end apart: 6, of which 6 were waited for; matrix products, arithmetic and copies ran while one was open for 4% of the time, Pallas kernels for 0%

profile of v1, /device:TPU:1, one launch (start us, length us, event | category | flops | bytes accessed | tf_op | source)
XLA Modules:
  0.0 175.0 jit_solution(6227822275324334819)
XLA Ops:
  0.7 0.8 convert_bitcast_fusion.1
  1.5 0.8 convert_bitcast_fusion.3
  2.2 0.8 fusion.9
  3.1 0.1 pad.44.clone
  3.1 0.1 select_reduce_fusion.1
  3.3 0.7 constant_dynamic-slice_fusion.1
  4.0 0.8 fusion.46
  4.9 1.0 broadcast_in_dim.197
  6.0 15.9 %all-to-all-start = ((bf16[16,72,384]{2,1,0:T(8,128)(2,1)}), bf16[16,72,384]{2,1,0:T(8,128)(2,1)S(1)}, u32[]{:S(2)}, u32[]{:S(2)}) async-start(bf16[16,72,384]{2,1,0:T(8,128)(2,1)} %broadcast_in_dim.197), calls=%async_computation | async-start | bytes 1769472 | tf_op jit(solution)/shard_map/all_to_all | solution.py:19
  21.9 0.1 fusion.24
  22.0 0.1 fusion.26
  22.1 0.2 reshape.353
  22.3 0.6 dynamic_slice.34
  23.6 0.6 dynamic_slice.33
  24.2 0.6 dynamic_slice.37
  24.9 0.8 dynamic-slice_bitcast_fusion
  25.6 0.2 concatenate.38
  25.8 0.7 dynamic-slice_convert_fusion
  26.6 33.5 %all-to-all-done = bf16[16,72,384]{2,1,0:T(8,128)(2,1)S(1)} async-done(((bf16[16,72,384]{2,1,0:T(8,128)(2,1)}), bf16[16,72,384]{2,1,0:T(8,128)(2,1)S(1)}, u32[]{:S(2)}, u32[]{:S(2)}) %all-to-all-start) | async-done | bytes 884768 | tf_op jit(solution)/shard_map/all_to_all | solution.py:19
  60.1 7.1 %collective-permute-start = (bf16[16,72,384]{2,1,0:T(8,128)(2,1)S(1)}, bf16[16,72,384]{2,1,0:T(8,128)(2,1)S(1)}, u32[]{:S(2)}, u32[]{:S(2)}) collective-permute-start(bf16[16,72,384]{2,1,0:T(8,128)(2,1)S(1)} %all-to-all-done), channel_id=1, source_target_pairs={{0,16},{16,0},{32,48},{48,32},{64,80},{80,64},{96,112},{112,96},{1... | collective-permute-start | bytes 2654216 | tf_op jit(solution)/shard_map/ppermute | solution.py:111
  67.2 0.2 fusion.101
  67.4 1.8 %collective-permute-done = bf16[16,72,384]{2,1,0:T(8,128)(2,1)S(1)} collective-permute-done((bf16[16,72,384]{2,1,0:T(8,128)(2,1)S(1)}, bf16[16,72,384]{2,1,0:T(8,128)(2,1)S(1)}, u32[]{:S(2)}, u32[]{:S(2)}) %collective-permute-start) | collective-permute-done | bytes 884768 | tf_op jit(solution)/shard_map/ppermute | solution.py:111
  69.2 0.2 multiply_reduce_fusion.1
  69.5 0.3 convolution_bitcast_fusion.2
  69.8 0.3 fusion.7
  70.2 0.7 multiply_exponential_fusion
  71.0 0.4 fusion.16
  71.4 0.8 multiply_reduce_fusion.4
  72.2 0.2 convolution_bitcast_fusion
  72.5 0.7 pad_maximum_fusion.2
  73.2 6.8 %all-to-all-start.1 = ((f32[16,32,128]{2,1,0:T(8,128)}), f32[16,32,128]{2,1,0:T(8,128)S(1)}, u32[]{:S(2)}, u32[]{:S(2)}) async-start(f32[16,32,128]{2,1,0:T(8,128)} %pad_maximum_fusion.2), calls=%async_computation.1 | async-start | bytes 524288 | tf_op jit(solution)/shard_map/all_to_all | solution.py:19
  80.4 7.7 %all-to-all-done.1 = f32[16,32,128]{2,1,0:T(8,128)S(1)} async-done(((f32[16,32,128]{2,1,0:T(8,128)}), f32[16,32,128]{2,1,0:T(8,128)S(1)}, u32[]{:S(2)}, u32[]{:S(2)}) %all-to-all-start.1) | async-done | bytes 262176 | tf_op jit(solution)/shard_map/all_to_all | solution.py:19
  88.2 0.7 broadcast_in_dim.201
  88.8 9.9 %all-to-all-start.2 = ((bf16[32,16,128]{2,1,0:T(8,128)(2,1)}), bf16[32,16,128]{2,1,0:T(8,128)(2,1)S(1)}, u32[]{:S(2)}, u32[]{:S(2)}) async-start(bf16[32,16,128]{2,1,0:T(8,128)(2,1)} %broadcast_in_dim.201), calls=%async_computation.2 | async-start | bytes 262144 | tf_op jit(solution)/shard_map/all_to_all | solution.py:19
  98.7 0.2 convolution_select_fusion.1
  98.9 0.3 fusion.53
  99.3 15.3 %all-to-all-done.2 = bf16[32,16,128]{2,1,0:T(8,128)(2,1)S(1)} async-done(((bf16[32,16,128]{2,1,0:T(8,128)(2,1)}), bf16[32,16,128]{2,1,0:T(8,128)(2,1)S(1)}, u32[]{:S(2)}, u32[]{:S(2)}) %all-to-all-start.2) | async-done | bytes 131104 | tf_op jit(solution)/shard_map/all_to_all | solution.py:19
  114.6 0.2 convolution_convert_fusion.1
  114.8 0.2 multiply_reduce_fusion
  115.0 0.1 broadcast_in_dim.202
  115.1 0.3 fusion
  115.5 15.1 %all_to_all.30 = bf16[16,48,512]{2,1,0:T(8,128)(2,1)S(1)} all-to-all(bf16[16,48,512]{2,1,0:T(8,128)(2,1)S(1)} %pad_maximum_fusion), channel_id=1, replica_groups=mesh['ep'=32,'tp'=16] {'tp'}, dimensions={0} | all-to-all | bytes 1572864 | tf_op jit(solution)/shard_map/all_to_all | solution.py:19
  130.6 0.2 fusion.66
  130.8 0.1 fusion.48
  131.1 0.2 copy.100
  131.2 0.3 fusion.17
  131.5 0.1 copy.115
  131.6 0.1 rsqrt.33
  131.7 0.2 copy-done.2
  131.9 0.3 convolution_multiply_fusion.1
  132.2 2.0 %fusion.1 = bf16[8,16,8,128]{3,2,1,0:T(8,128)(2,1)S(1)} fusion(bf16[1,256,2048]{2,1,0:T(8,128)(2,1)S(1)} %copy-done, bf16[1,2048,256]{2,1,0:T(8,128)(2,1)} %param.48, bf16[8,8,16,128]{3,2,1,0:T(8,128)(2,1)S(1)} %bitcast.135, f32[64,256]{1,0:T(8,128)S(1)} %convolution_multiply_fusion.1, f32[64]{0:T(128)S(1)} %rsqrt.33), kind=kOutput, calls=%fused_computation.3 | convolution fusion | flops 134463488 | bytes 2687232 | tf_op jit(solution)/shard_map/dot_general | solution.py:34
  134.3 0.8 pad_maximum_fusion.1
  135.2 3.7 %all-to-all-start.4 = ((bf16[16,128,128]{2,1,0:T(8,128)(2,1)}), bf16[16,128,128]{2,1,0:T(8,128)(2,1)S(1)}, u32[]{:S(2)}, u32[]{:S(2)}) async-start(bf16[16,128,128]{2,1,0:T(8,128)(2,1)} %pad_maximum_fusion.1), calls=%async_computation.4 | async-start | bytes 1048576 | tf_op jit(solution)/shard_map/all_to_all | solution.py:19
  138.9 0.2 select_reduce_fusion
  139.1 8.8 %all-to-all-done.4 = bf16[16,128,128]{2,1,0:T(8,128)(2,1)S(1)} async-done(((bf16[16,128,128]{2,1,0:T(8,128)(2,1)}), bf16[16,128,128]{2,1,0:T(8,128)(2,1)S(1)}, u32[]{:S(2)}, u32[]{:S(2)}) %all-to-all-start.4) | async-done | bytes 524320 | tf_op jit(solution)/shard_map/all_to_all | solution.py:19
  147.9 0.3 fusion.28
  148.2 0.2 fusion.49
  148.4 0.8 fusion.3
  149.2 9.2 %all-to-all-start.5 = ((bf16[32,16,128]{2,1,0:T(8,128)(2,1)}), bf16[32,16,128]{2,1,0:T(8,128)(2,1)S(1)}, u32[]{:S(2)}, u32[]{:S(2)}) async-start(bf16[32,16,128]{2,1,0:T(8,128)(2,1)} %bitcast.40), calls=%async_computation.5 | async-start | bytes 262144 | tf_op jit(solution)/shard_map/all_to_all | solution.py:19
  158.5 1.0 multiply_add_fusion
  159.5 0.6 fusion.68
  160.2 0.8 pad_maximum_fusion.3
  160.9 13.4 %all-to-all-done.5 = bf16[32,16,128]{2,1,0:T(8,128)(2,1)S(1)} async-done(((bf16[32,16,128]{2,1,0:T(8,128)(2,1)}), bf16[32,16,128]{2,1,0:T(8,128)(2,1)S(1)}, u32[]{:S(2)}, u32[]{:S(2)}) %all-to-all-start.5) | async-done | bytes 131104 | tf_op jit(solution)/shard_map/all_to_all | solution.py:19
  174.3 0.6 fusion.78
  (98 shorter events, 1.6 us)
Async XLA Ops:
  0.6 131.5 %copy-start = (bf16[1,256,2048]{2,1,0:T(8,128)(2,1)S(1)}, bf16[1,256,2048]{2,1,0:T(8,128)(2,1)}, u32[]{:S(2)}) copy-start(bf16[1,256,2048]{2,1,0:T(8,128)(2,1)} %param.49) | copy-start | bytes 3145732
  5.9 16.0 %copy-start.3 = (bf16[16,2048]{1,0:T(8,128)(2,1)S(1)}, bf16[16,2048]{1,0:T(8,128)(2,1)}, u32[]{:S(2)}) copy-start(bf16[16,2048]{1,0:T(8,128)(2,1)} %param.27) | copy-start | bytes 196612
  5.9 16.1 %copy-start.10 = (f32[2048]{0:T(1024)S(1)}, f32[2048]{0:T(1024)}, u32[]{:S(2)}) copy-start(f32[2048]{0:T(1024)} %param.28) | copy-start | bytes 24580
  5.9 16.4 %copy-start.16 = (f32[16]{0:T(128)S(1)}, f32[16]{0:T(128)}, u32[]{:S(2)}) copy-start(f32[16]{0:T(128)} %param.35) | copy-start | bytes 196
  5.9 17.7 %copy-start.17 = (f32[16]{0:T(128)S(1)}, f32[16]{0:T(128)}, u32[]{:S(2)}) copy-start(f32[16]{0:T(128)} %param.34) | copy-start | bytes 196
  5.9 18.3 %copy-start.14 = (bf16[4,64]{1,0:T(4,128)(2,1)S(1)}, bf16[4,64]{1,0:T(4,128)(2,1)}, u32[]{:S(2)}) copy-start(bf16[4,64]{1,0:T(4,128)(2,1)} %param.37) | copy-start | bytes 1540
  5.9 18.3 %copy-start.18 = (f32[16]{0:T(128)S(1)}, f32[16]{0:T(128)}, u32[]{:S(2)}) copy-start(f32[16]{0:T(128)} %param.36) | copy-start | bytes 196
  5.9 18.9 %copy-start.11 = (f32[2048]{0:T(1024)S(1)}, f32[2048]{0:T(1024)}, u32[]{:S(2)}) copy-start(f32[2048]{0:T(1024)} %param.44) | copy-start | bytes 24580
  5.9 19.7 %copy-start.7 = (bf16[128,224]{0,1:T(8,128)(2,1)S(1)}, bf16[128,224]{0,1:T(8,128)(2,1)}, u32[]{:S(2)}) copy-start(bf16[128,224]{0,1:T(8,128)(2,1)} %param.51) | copy-start | bytes 172036
  5.9 19.7 %copy-start.8 = (bf16[128,224]{0,1:T(8,128)(2,1)S(1)}, bf16[128,224]{0,1:T(8,128)(2,1)}, u32[]{:S(2)}) copy-start(bf16[128,224]{0,1:T(8,128)(2,1)} %param.52) | copy-start | bytes 172036
  5.9 20.6 %copy-start.4 = (bf16[16,2,3,512]{3,1,2,0:T(2,128)(2,1)S(1)}, bf16[16,2,3,512]{3,1,2,0:T(2,128)(2,1)}, u32[]{:S(2)}) copy-start(bf16[16,2,3,512]{3,1,2,0:T(2,128)(2,1)} %param.40) | copy-start | bytes 294916
  6.0 54.1 %all-to-all-start = ((bf16[16,72,384]{2,1,0:T(8,128)(2,1)}), bf16[16,72,384]{2,1,0:T(8,128)(2,1)S(1)}, u32[]{:S(2)}, u32[]{:S(2)}) async-start(bf16[16,72,384]{2,1,0:T(8,128)(2,1)} %broadcast_in_dim.197), calls=%async_computation | async-start | bytes 1769472 | tf_op jit(solution)/shard_map/all_to_all | solution.py:19
  25.8 88.8 %copy-start.12 = (f32[64]{0:T(128)}, f32[64]{0:T(128)S(1)}, u32[]{:S(2)}) copy-start(f32[64]{0:T(128)S(1)} %get-tuple-element.47) | copy-start | bytes 772
  60.1 9.1 %collective-permute-start = (bf16[16,72,384]{2,1,0:T(8,128)(2,1)S(1)}, bf16[16,72,384]{2,1,0:T(8,128)(2,1)S(1)}, u32[]{:S(2)}, u32[]{:S(2)}) collective-permute-start(bf16[16,72,384]{2,1,0:T(8,128)(2,1)S(1)} %all-to-all-done), channel_id=1, source_target_pairs={{0,16},{16,0},{32,48},{48,32},{64,80},{80,64},{96,112},{112,96},{1... | collective-permute-start | bytes 2654216 | tf_op jit(solution)/shard_map/ppermute | solution.py:111
  69.5 0.7 copy-start.9
  69.5 1.5 copy-start.1
  69.8 2.4 %copy-start.5 = (bf16[64,2048]{1,0:T(8,128)(2,1)S(1)}, bf16[64,2048]{1,0:T(8,128)(2,1)}, u32[]{:S(2)}) copy-start(bf16[64,2048]{1,0:T(8,128)(2,1)} %param.43) | copy-start | bytes 786436
  69.8 2.5 %copy-start.15 = (f32[64]{0:T(128)S(1)}, f32[64]{0:T(128)}, u32[]{:S(2)}) copy-start(f32[64]{0:T(128)} %param.42) | copy-start | bytes 772
  73.2 14.9 %all-to-all-start.1 = ((f32[16,32,128]{2,1,0:T(8,128)}), f32[16,32,128]{2,1,0:T(8,128)S(1)}, u32[]{:S(2)}, u32[]{:S(2)}) async-start(f32[16,32,128]{2,1,0:T(8,128)} %pad_maximum_fusion.2), calls=%async_computation.1 | async-start | bytes 524288 | tf_op jit(solution)/shard_map/all_to_all | solution.py:19
  88.8 25.8 %all-to-all-start.2 = ((bf16[32,16,128]{2,1,0:T(8,128)(2,1)}), bf16[32,16,128]{2,1,0:T(8,128)(2,1)S(1)}, u32[]{:S(2)}, u32[]{:S(2)}) async-start(bf16[32,16,128]{2,1,0:T(8,128)(2,1)} %broadcast_in_dim.201), calls=%async_computation.2 | async-start | bytes 262144 | tf_op jit(solution)/shard_map/all_to_all | solution.py:19
  130.6 1.2 copy-start.2
  134.3 4.6 %copy-start.13 = (f32[64]{0:T(128)S(1)}, f32[64]{0:T(128)}, u32[]{:S(2)}) copy-start(f32[64]{0:T(128)} %copy-done.12) | copy-start | bytes 772
  135.2 13.1 %copy-start.6 = (bf16[224,128]{1,0:T(8,128)(2,1)S(1)}, bf16[224,128]{1,0:T(8,128)(2,1)}, u32[]{:S(2)}) copy-start(bf16[224,128]{1,0:T(8,128)(2,1)} %param.53) | copy-start | bytes 172036
  135.2 12.7 %all-to-all-start.4 = ((bf16[16,128,128]{2,1,0:T(8,128)(2,1)}), bf16[16,128,128]{2,1,0:T(8,128)(2,1)S(1)}, u32[]{:S(2)}, u32[]{:S(2)}) async-start(bf16[16,128,128]{2,1,0:T(8,128)(2,1)} %pad_maximum_fusion.1), calls=%async_computation.4 | async-start | bytes 1048576 | tf_op jit(solution)/shard_map/all_to_all | solution.py:19
  149.2 10.9 %slice-start = ((bf16[16,2,3,512]{3,1,2,0:T(2,128)(2,1)}), bf16[16,2,2,512]{3,1,2,0:T(2,128)(2,1)S(1)}, s32[]{:S(2)}) async-start(bf16[16,2,3,512]{3,1,2,0:T(2,128)(2,1)} %param.40), calls=%async_computation.6 | async-start | bytes 131072 | tf_op jit(solution)/shard_map/slice | solution.py:170
  149.2 25.1 %all-to-all-start.5 = ((bf16[32,16,128]{2,1,0:T(8,128)(2,1)}), bf16[32,16,128]{2,1,0:T(8,128)(2,1)S(1)}, u32[]{:S(2)}, u32[]{:S(2)}) async-start(bf16[32,16,128]{2,1,0:T(8,128)(2,1)} %bitcast.40), calls=%async_computation.5 | async-start | bytes 262144 | tf_op jit(solution)/shard_map/all_to_all | solution.py:19

commit v2 on v1

--- a/solution.py
+++ b/solution.py
@@ -75,14 +75,19 @@
     tp = lax.axis_index("tp")
     core = ep % CORES
     group = tp // PER_GROUP
+    member = tp % PER_GROUP
     rows_k = gate_weight.shape[0]
     cols = width // n_tp
     same_core = [[CORES * z + c for z in range(chips)] for c in range(CORES)]
     swap = [(i, i ^ 1) for i in range(n_ep)]
+    same_group = [[PER_GROUP * g + m for m in range(PER_GROUP)] for g in range(GROUPS)]
+    part = 2 * STATE // PER_GROUP
 
     write_own = slice_at(write_weight, group * STATE, STATE, 1)
     read_own = slice_at(read_weight, group * STATE, STATE, 1)
-    main = jnp.concatenate([gate_weight, inner_weight, write_own, read_own], axis=1)
+    either = jnp.where(member < PER_GROUP // 2, write_own, read_own)
+    either = jnp.where(member % 2 == 0, either[:, :part], either[:, part:])
+    main = jnp.concatenate([gate_weight, inner_weight, either], axis=1)
     pack_cols = main.shape[1]
     head_pick = (jnp.arange(HEADS) == tp).astype(BF)[None]
     step_row = lax.dot_general(
@@ -128,8 +133,16 @@
     step_raw = step_a + step_b
     gate_part = projected[:, :HEAD_DIM].astype(BF)
     inner_part = projected[:, HEAD_DIM : 2 * HEAD_DIM].astype(BF)
-    write_part = projected[:, 2 * HEAD_DIM : 2 * HEAD_DIM + STATE].astype(BF)
-    read_part = projected[:, 2 * HEAD_DIM + STATE :].astype(BF)
+    share_part = projected[:, 2 * HEAD_DIM :].astype(BF)
+    none = jnp.zeros_like(share_part)
+    placed = jnp.where(
+        member % 2 == 0,
+        jnp.concatenate([share_part, none], axis=1),
+        jnp.concatenate([none, share_part], axis=1),
+    )
+    quarters = exchange(to_everyone(placed, PER_GROUP), "tp", same_group)
+    write_part = quarters[0] + quarters[1]
+    read_part = quarters[2] + quarters[3]
 
     inner_window = jnp.concatenate([inner_history, inner_part[:, None, :]], axis=1)
     inner_conv = jax.nn.silu(
@@ -159,28 +172,27 @@
     head_out = rms_scale(gated, head_gain).astype(BF)
 
     partial_mix = dot32(head_out, mixer_out)
-    mix_pieces = partial_mix.reshape(seqs, n_tp, cols).transpose(1, 0, 2)
-    parts_sent = jnp.where(tp % 2 == 0, write_part, read_part).astype(F32)
+    mix_pieces = partial_mix.astype(BF).reshape(seqs, n_tp, cols).transpose(1, 0, 2)
+    parts_sent = jnp.where(tp % 2 == 0, write_part, read_part)
     arrived = exchange(
         jnp.concatenate([mix_pieces, to_everyone(parts_sent, n_tp)], axis=1), "tp"
     )
-    mixed = jnp.sum(arrived[:, :seqs], axis=0).astype(BF)
-    parts_all = arrived[:, seqs:].astype(BF).reshape(GROUPS, PER_GROUP, seqs, STATE)[:, :2]
+    mixed = jnp.sum(arrived[:, :seqs].astype(F32), axis=0).astype(BF)
+    parts_all = arrived[:, seqs:].reshape(GROUPS, PER_GROUP, seqs, STATE)[:, :2]
     parts_all = parts_all.transpose(2, 1, 0, 3).reshape(seqs, 2, 1, GROUPS * STATE)
     new_access = jnp.concatenate([access_history[:, :, 1:], parts_all], axis=2)
 
     resid = slice_at(tokens, tp * cols, cols, 1).astype(F32) + mixed.astype(F32)
     gain_own = slice_at(moe_gain, tp * cols, cols, 0)
     scaled = (resid * gain_own).astype(BF)
-    scaled_all = exchange(to_everyone(scaled, n_ep), "ep").reshape(n_ep * seqs, cols)
+    scaled_own = exchange(to_everyone(scaled, chips), "ep", same_core)
+    scaled_own = scaled_own.reshape(chips * seqs, cols)
+    scaled_other = lax.ppermute(scaled_own, "ep", swap)
+    scaled_all = jnp.concatenate([scaled_own, scaled_other], axis=0)
 
     own_routes = own_pack[:, rows_k + 1, : 4 * seqs].astype(F32)
     other_routes = other_pack[:, rows_k + 1, : 4 * seqs].astype(F32)
-    routes = jnp.where(
-        core == 0,
-        jnp.stack([own_routes, other_routes], axis=1),
-        jnp.stack([other_routes, own_routes], axis=1),
-    ).reshape(n_ep, 4 * seqs)
+    routes = jnp.concatenate([own_routes, other_routes], axis=0)
     mine = ep.astype(F32)
     is_first = routes[:, :seqs] == mine
     is_second = routes[:, seqs : 2 * seqs] == mine
@@ -263,15 +275,25 @@
         jnp.concatenate([out_pieces, to_everyone(act_block, n_tp)], axis=1), "tp"
     )
     expert_out = jnp.sum(arrived[:, :slots].astype(F32), axis=0) * slot_weight
+    expert_out = expert_out.astype(BF)
     down = jnp.pad(dense_down, ((0, half - units), (0, 0)))
-    summed = (
-        dot32(arrived[:, slots : slots + share].reshape(total, 128), down[:128])
-        + dot32(arrived[:, slots + share :].reshape(total, 128), down[128:])
-        + lax.dot_general(
-            chosen, expert_out.astype(BF), (((0,), (0,)), ((), ())), preferred_element_type=F32
+
+    def outputs_of(core_rank):
+        acts = arrived[core_rank * n_tp // CORES : (core_rank + 1) * n_tp // CORES, slots:]
+        tokens_of = total // CORES
+        slots_of = slice(core_rank * slots // CORES, (core_rank + 1) * slots // CORES)
+        picks = chosen[slots_of, core_rank * tokens_of : (core_rank + 1) * tokens_of]
+        return (
+            dot32(acts[:, :share].reshape(tokens_of, 128), down[:128])
+            + dot32(acts[:, share:].reshape(tokens_of, 128), down[128:])
+            + lax.dot_general(
+                picks, expert_out[slots_of], (((0,), (0,)), ((), ())), preferred_element_type=F32
+            )
         )
-    )
-    final = exchange(summed.astype(BF).reshape(n_ep, seqs, cols), "ep")
+
+    swapped = lax.ppermute(outputs_of(1), "ep", swap)
+    summed = outputs_of(0) + swapped
+    final = exchange(summed.astype(BF).reshape(chips, seqs, cols), "ep", same_core)
     output = resid + jnp.sum(final.astype(F32), axis=0)
     return (output, new_recurrent[:, None], inner_window[:, 1:], new_access)
 

time: 176 us -> 170 us (0.966)
  blocking collectives: 15.1 us -> 0 us
  starting transfers between devices: 52.5 us -> 61.8 us
  waiting for transfers between devices: 80.4 us -> 77.7 us
  other arithmetic: 11.5 us -> 13.4 us
    all_to_all x1 -> x0, blocking collectives: 15.1 us -> none  [exchange(): lax.all_to_all(pieces, axis, split_axis=0, concat_axis=0, tiled=True, axi...]
    ppermute x0 -> x2, starting transfers between devices: none -> 10.6 us  [the longest x1 6.48 us: local(): scaled_other = lax.ppermute(scaled_own, 'ep', swap)]
    all_to_all x5 -> x7, waiting for transfers between devices: 78.6 us -> 74.5 us  [exchange(): lax.all_to_all(pieces, axis, split_axis=0, concat_axis=0, tiled=True, axi...]
    all_to_all x5 -> x7, starting transfers between devices: 45.5 us -> 42.9 us  [exchange(): lax.all_to_all(pieces, axis, split_axis=0, concat_axis=0, tiled=True, axi...]
    dot_general x10 -> x12, matrix products: 4.83 us -> 5.51 us  [dot32(): return jnp.dot(left, right, preferred_element_type=F32)]
  transfers between devices with their start and end apart: 6 -> 10, of which waited for: 6 -> 10; matrix products, arithmetic and copies ran while one was open for 4% -> 5% of each run, Pallas kernels for 0% -> 0%
where the time goes in v2:
time: 170 us; the launch traced here: 169 us
  waiting for transfers between devices  77.7 us (46%)
  starting transfers between devices  61.8 us (36%)
  other arithmetic  13.4 us (8%)
  matrix products  7.79 us (5%)
  local copies, waits for them, and re-layouts  6.4 us (4%)
  between operations  2.07 us (1%)
    all_to_all x7, waiting for transfers between devices, exchange(): lax.all_to_all(pieces, axis, split_axis=0, concat_axis=0, tiled=True, axi...  74.5 us
    all_to_all x7, starting transfers between devices, exchange(): lax.all_to_all(pieces, axis, split_axis=0, concat_axis=0, tiled=True, axi...  42.9 us
    ppermute x1, starting transfers between devices, local(): other_pack = lax.ppermute(own_pack, 'ep', swap)  8.32 us
    ppermute x1, starting transfers between devices, local(): scaled_other = lax.ppermute(scaled_own, 'ep', swap)  6.48 us
    dot_general x12, matrix products, dot32(): return jnp.dot(left, right, preferred_element_type=F32)  5.51 us
    ppermute x1, starting transfers between devices, local(): swapped = lax.ppermute(outputs_of(1), 'ep', swap)  4.07 us
  transfers between devices with their start and end apart: 10, of which 10 were waited for; matrix products, arithmetic and copies ran while one was open for 5% of the time, Pallas kernels for 0%

profile of v2, /device:TPU:1, one launch (start us, length us, event | category | flops | bytes accessed | tf_op | source)
XLA Modules:
  0.0 169.1 jit_solution(13337492225014606414)
XLA Ops:
  0.8 0.9 fusion.10
  1.6 0.8 convert_bitcast_fusion.1
  2.4 0.8 convert_bitcast_fusion.3
  3.2 0.7 dynamic-slice_select_fusion
  4.2 0.8 fusion.38
  5.2 0.8 broadcast_in_dim.204
  6.0 15.9 %all-to-all-start = ((bf16[16,72,192]{2,1,0:T(8,128)(2,1)}), bf16[16,72,192]{2,1,0:T(8,128)(2,1)S(1)}, u32[]{:S(2)}, u32[]{:S(2)}) async-start(bf16[16,72,192]{2,1,0:T(8,128)(2,1)} %broadcast_in_dim.204), calls=%async_computation | async-start | bytes 1179648 | tf_op jit(solution)/shard_map/all_to_all | solution.py:19
  22.1 0.2 reshape.420
  22.3 0.6 dynamic_slice.34
  23.6 0.6 dynamic_slice.33
  24.2 0.6 dynamic_slice.37
  24.9 0.8 dynamic-slice_bitcast_fusion
  25.7 0.2 concatenate.56
  25.9 0.7 dynamic-slice_convert_fusion
  26.6 0.2 fusion.106
  26.8 20.4 %all-to-all-done = bf16[16,72,192]{2,1,0:T(8,128)(2,1)S(1)} async-done(((bf16[16,72,192]{2,1,0:T(8,128)(2,1)}), bf16[16,72,192]{2,1,0:T(8,128)(2,1)S(1)}, u32[]{:S(2)}, u32[]{:S(2)}) %all-to-all-start) | async-done | bytes 442400 | tf_op jit(solution)/shard_map/all_to_all | solution.py:19
  47.2 8.3 %collective-permute-start = (bf16[16,72,192]{2,1,0:T(8,128)(2,1)S(1)}, bf16[16,72,192]{2,1,0:T(8,128)(2,1)S(1)}, u32[]{:S(2)}, u32[]{:S(2)}) collective-permute-start(bf16[16,72,192]{2,1,0:T(8,128)(2,1)S(1)} %all-to-all-done), channel_id=1, source_target_pairs={{0,16},{16,0},{32,48},{48,32},{64,80},{80,64},{96,112},{112,96},{1... | collective-permute-start | bytes 1327112 | tf_op jit(solution)/shard_map/ppermute | solution.py:116
  55.7 1.5 collective-permute-done
  57.2 0.2 multiply_reduce_fusion.1
  57.4 0.2 convolution_bitcast_fusion.1
  57.6 0.2 fusion.8
  58.0 0.6 broadcast_in_dim.206
  58.7 4.0 %all-to-all-start.1 = ((bf16[4,16,128]{2,1,0:T(8,128)(2,1)}), bf16[4,16,128]{2,1,0:T(8,128)(2,1)S(1)}, u32[]{:S(2)}, u32[]{:S(2)}) async-start(bf16[4,16,128]{2,1,0:T(8,128)(2,1)} %broadcast_in_dim.206), calls=%async_computation.1 | async-start | bytes 32768 | tf_op jit(solution)/shard_map/all_to_all | solution.py:19
  62.8 0.7 multiply_exponential_fusion
  63.6 3.3 %all-to-all-done.1 = bf16[4,16,128]{2,1,0:T(8,128)(2,1)S(1)} async-done(((bf16[4,16,128]{2,1,0:T(8,128)(2,1)}), bf16[4,16,128]{2,1,0:T(8,128)(2,1)S(1)}, u32[]{:S(2)}, u32[]{:S(2)}) %all-to-all-start.1) | async-done | bytes 16416 | tf_op jit(solution)/shard_map/all_to_all | solution.py:19
  66.9 0.4 fusion.17
  67.4 0.8 multiply_reduce_fusion.4
  68.2 0.2 fusion.4
  68.4 0.7 pad_maximum_fusion.2
  69.1 5.1 %all-to-all-start.2 = ((bf16[16,32,128]{2,1,0:T(8,128)(2,1)}), bf16[16,32,128]{2,1,0:T(8,128)(2,1)S(1)}, u32[]{:S(2)}, u32[]{:S(2)}) async-start(bf16[16,32,128]{2,1,0:T(8,128)(2,1)} %pad_maximum_fusion.2), calls=%async_computation.2 | async-start | bytes 262144 | tf_op jit(solution)/shard_map/all_to_all | solution.py:19
  74.3 6.8 %all-to-all-done.2 = bf16[16,32,128]{2,1,0:T(8,128)(2,1)S(1)} async-done(((bf16[16,32,128]{2,1,0:T(8,128)(2,1)}), bf16[16,32,128]{2,1,0:T(8,128)(2,1)S(1)}, u32[]{:S(2)}, u32[]{:S(2)}) %all-to-all-start.2) | async-done | bytes 131104 | tf_op jit(solution)/shard_map/all_to_all | solution.py:19
  81.1 0.6 broadcast_in_dim.210
  81.8 7.1 %all-to-all-start.3 = ((bf16[16,16,128]{2,1,0:T(8,128)(2,1)}), bf16[16,16,128]{2,1,0:T(8,128)(2,1)S(1)}, u32[]{:S(2)}, u32[]{:S(2)}) async-start(bf16[16,16,128]{2,1,0:T(8,128)(2,1)} %broadcast_in_dim.210), calls=%async_computation.3 | async-start | bytes 131072 | tf_op jit(solution)/shard_map/all_to_all | solution.py:19
  88.9 0.2 convolution_select_fusion.1
  89.1 0.3 fusion.43
  89.4 11.0 %all-to-all-done.3 = bf16[16,16,128]{2,1,0:T(8,128)(2,1)S(1)} async-done(((bf16[16,16,128]{2,1,0:T(8,128)(2,1)}), bf16[16,16,128]{2,1,0:T(8,128)(2,1)S(1)}, u32[]{:S(2)}, u32[]{:S(2)}) %all-to-all-start.3) | async-done | bytes 65568 | tf_op jit(solution)/shard_map/all_to_all | solution.py:19
  100.5 6.5 %collective-permute-start.1 = (bf16[256,128]{1,0:T(8,128)(2,1)S(1)}, bf16[256,128]{1,0:T(8,128)(2,1)S(1)}, u32[]{:S(2)}, u32[]{:S(2)}) collective-permute-start(bf16[256,128]{1,0:T(8,128)(2,1)S(1)} %bitcast.150), channel_id=1, source_target_pairs={{0,16},{16,0},{32,48},{48,32},{64,80},{80,64},{96,112},{112,96},{1... | collective-permute-start | bytes 196616 | tf_op jit(solution)/shard_map/ppermute | solution.py:190
  107.0 0.8 collective-permute-done.1
  107.8 0.2 convolution_convert_fusion.2
  108.1 0.1 multiply_reduce_fusion
  108.2 0.3 fusion
  108.6 0.9 pad_maximum_fusion
  109.5 3.6 %all-to-all-start.4 = ((bf16[16,48,512]{2,1,0:T(8,128)(2,1)}), bf16[16,48,512]{2,1,0:T(8,128)(2,1)S(1)}, u32[]{:S(2)}, u32[]{:S(2)}) async-start(bf16[16,48,512]{2,1,0:T(8,128)(2,1)} %pad_maximum_fusion), calls=%async_computation.4 | async-start | bytes 1572864 | tf_op jit(solution)/shard_map/all_to_all | solution.py:19
  113.1 0.2 select_reduce_fusion
  113.3 13.6 %all-to-all-done.4 = bf16[16,48,512]{2,1,0:T(8,128)(2,1)S(1)} async-done(((bf16[16,48,512]{2,1,0:T(8,128)(2,1)}), bf16[16,48,512]{2,1,0:T(8,128)(2,1)S(1)}, u32[]{:S(2)}, u32[]{:S(2)}) %all-to-all-start.4) | async-done | bytes 786464 | tf_op jit(solution)/shard_map/all_to_all | solution.py:19
  127.0 0.2 copy.92
  127.2 0.3 fusion.18
  127.6 1.5 convolution_multiply_fusion.1
  129.1 2.0 %fusion.1 = bf16[8,16,8,128]{3,2,1,0:T(8,128)(2,1)S(1)} fusion(bf16[1,256,2048]{2,1,0:T(8,128)(2,1)S(1)} %copy-done, bf16[1,2048,256]{2,1,0:T(8,128)(2,1)} %param.48, bf16[8,8,16,128]{3,2,1,0:T(8,128)(2,1)S(1)} %bitcast.146, f32[64,256]{1,0:T(8,128)S(1)} %convolution_multiply_fusion.1, f32[64]{0:T(128)S(1)} %rsqrt.33), kind=kOutput, calls=%fused_computation.4 | convolution fusion | flops 134463488 | bytes 2687232 | tf_op jit(solution)/shard_map/dot_general | solution.py:34
  131.3 0.2 fusion.61
  131.7 0.8 pad_maximum_fusion.1
  132.5 3.7 %all-to-all-start.5 = ((bf16[16,128,128]{2,1,0:T(8,128)(2,1)}), bf16[16,128,128]{2,1,0:T(8,128)(2,1)S(1)}, u32[]{:S(2)}, u32[]{:S(2)}) async-start(bf16[16,128,128]{2,1,0:T(8,128)(2,1)} %pad_maximum_fusion.1), calls=%async_computation.5 | async-start | bytes 1048576 | tf_op jit(solution)/shard_map/all_to_all | solution.py:19
  136.2 0.6 fusion.63
  136.9 1.0 multiply_add_fusion
  138.0 8.6 %all-to-all-done.5 = bf16[16,128,128]{2,1,0:T(8,128)(2,1)S(1)} async-done(((bf16[16,128,128]{2,1,0:T(8,128)(2,1)}), bf16[16,128,128]{2,1,0:T(8,128)(2,1)S(1)}, u32[]{:S(2)}, u32[]{:S(2)}) %all-to-all-start.5) | async-done | bytes 524320 | tf_op jit(solution)/shard_map/all_to_all | solution.py:19
  146.7 0.1 fusion.46
  147.2 0.2 convolution_add_fusion
  147.4 4.1 %collective-permute-start.2 = (f32[256,128]{1,0:T(8,128)S(1)}, f32[256,128]{1,0:T(8,128)S(1)}, u32[]{:S(2)}, u32[]{:S(2)}) collective-permute-start(f32[256,128]{1,0:T(8,128)S(1)} %convolution_add_fusion), channel_id=1, source_target_pairs={{0,16},{16,0},{32,48},{48,32},{64,80},{80,64},{96,112},{112,96},{1... | collective-permute-start | bytes 393224 | tf_op jit(solution)/shard_map/ppermute | solution.py:294
  151.6 0.8 collective-permute-done.2
  152.4 0.8 fusion.3
  153.3 3.5 %all-to-all-start.6 = ((bf16[16,16,128]{2,1,0:T(8,128)(2,1)}), bf16[16,16,128]{2,1,0:T(8,128)(2,1)S(1)}, u32[]{:S(2)}, u32[]{:S(2)}) async-start(bf16[16,16,128]{2,1,0:T(8,128)(2,1)} %bitcast.46), calls=%async_computation.6 | async-start | bytes 131072 | tf_op jit(solution)/shard_map/all_to_all | solution.py:19
  156.9 0.8 pad_maximum_fusion.4
  157.6 10.9 %all-to-all-done.6 = bf16[16,16,128]{2,1,0:T(8,128)(2,1)S(1)} async-done(((bf16[16,16,128]{2,1,0:T(8,128)(2,1)}), bf16[16,16,128]{2,1,0:T(8,128)(2,1)S(1)}, u32[]{:S(2)}, u32[]{:S(2)}) %all-to-all-start.6) | async-done | bytes 65568 | tf_op jit(solution)/shard_map/all_to_all | solution.py:19
  168.5 0.6 fusion.77
  (102 shorter events, 2.8 us)
Async XLA Ops:
  0.6 128.5 %copy-start = (bf16[1,256,2048]{2,1,0:T(8,128)(2,1)S(1)}, bf16[1,256,2048]{2,1,0:T(8,128)(2,1)}, u32[]{:S(2)}) copy-start(bf16[1,256,2048]{2,1,0:T(8,128)(2,1)} %param.49) | copy-start | bytes 3145732
  0.7 21.2 %copy-start.3 = (bf16[16,2048]{1,0:T(8,128)(2,1)S(1)}, bf16[16,2048]{1,0:T(8,128)(2,1)}, u32[]{:S(2)}) copy-start(bf16[16,2048]{1,0:T(8,128)(2,1)} %param.27) | copy-start | bytes 196612
  1.6 20.4 %copy-start.9 = (f32[2048]{0:T(1024)S(1)}, f32[2048]{0:T(1024)}, u32[]{:S(2)}) copy-start(f32[2048]{0:T(1024)} %param.28) | copy-start | bytes 24580
  5.1 17.3 %copy-start.13 = (f32[16]{0:T(128)S(1)}, f32[16]{0:T(128)}, u32[]{:S(2)}) copy-start(f32[16]{0:T(128)} %param.35) | copy-start | bytes 196
  5.1 18.5 %copy-start.14 = (f32[16]{0:T(128)S(1)}, f32[16]{0:T(128)}, u32[]{:S(2)}) copy-start(f32[16]{0:T(128)} %param.34) | copy-start | bytes 196
  5.1 19.1 %copy-start.11 = (bf16[4,64]{1,0:T(4,128)(2,1)S(1)}, bf16[4,64]{1,0:T(4,128)(2,1)}, u32[]{:S(2)}) copy-start(bf16[4,64]{1,0:T(4,128)(2,1)} %param.37) | copy-start | bytes 1540
  5.1 19.1 %copy-start.15 = (f32[16]{0:T(128)S(1)}, f32[16]{0:T(128)}, u32[]{:S(2)}) copy-start(f32[16]{0:T(128)} %param.36) | copy-start | bytes 196
  5.1 19.7 %copy-start.10 = (f32[2048]{0:T(1024)S(1)}, f32[2048]{0:T(1024)}, u32[]{:S(2)}) copy-start(f32[2048]{0:T(1024)} %param.44) | copy-start | bytes 24580
  5.1 20.5 %copy-start.6 = (bf16[128,224]{0,1:T(8,128)(2,1)S(1)}, bf16[128,224]{0,1:T(8,128)(2,1)}, u32[]{:S(2)}) copy-start(bf16[128,224]{0,1:T(8,128)(2,1)} %param.51) | copy-start | bytes 172036
  5.1 20.5 %copy-start.7 = (bf16[128,224]{0,1:T(8,128)(2,1)S(1)}, bf16[128,224]{0,1:T(8,128)(2,1)}, u32[]{:S(2)}) copy-start(bf16[128,224]{0,1:T(8,128)(2,1)} %param.52) | copy-start | bytes 172036
  6.0 20.6 %copy-start.4 = (bf16[16,2,3,512]{3,1,2,0:T(2,128)(2,1)S(1)}, bf16[16,2,3,512]{3,1,2,0:T(2,128)(2,1)}, u32[]{:S(2)}) copy-start(bf16[16,2,3,512]{3,1,2,0:T(2,128)(2,1)} %param.40) | copy-start | bytes 294916
  6.0 41.2 %all-to-all-start = ((bf16[16,72,192]{2,1,0:T(8,128)(2,1)}), bf16[16,72,192]{2,1,0:T(8,128)(2,1)S(1)}, u32[]{:S(2)}, u32[]{:S(2)}) async-start(bf16[16,72,192]{2,1,0:T(8,128)(2,1)} %broadcast_in_dim.204), calls=%async_computation | async-start | bytes 1179648 | tf_op jit(solution)/shard_map/all_to_all | solution.py:19
  26.8 36.0 %copy-start.8 = (bf16[16,3,64]{2,0,1:T(8,128)(2,1)S(1)}, bf16[16,3,64]{2,0,1:T(8,128)(2,1)}, u32[]{:S(2)}) copy-start(bf16[16,3,64]{2,0,1:T(8,128)(2,1)} %param.39) | copy-start | bytes 18436
  47.2 9.9 %collective-permute-start = (bf16[16,72,192]{2,1,0:T(8,128)(2,1)S(1)}, bf16[16,72,192]{2,1,0:T(8,128)(2,1)S(1)}, u32[]{:S(2)}, u32[]{:S(2)}) collective-permute-start(bf16[16,72,192]{2,1,0:T(8,128)(2,1)S(1)} %all-to-all-done), channel_id=1, source_target_pairs={{0,16},{16,0},{32,48},{48,32},{64,80},{80,64},{96,112},{112,96},{1... | collective-permute-start | bytes 1327112 | tf_op jit(solution)/shard_map/ppermute | solution.py:116
  55.7 11.2 %copy-start.1 = (f32[16,1,64,128]{3,2,1,0:T(8,128)S(1)}, f32[16,1,64,128]{3,2,1,0:T(8,128)}, u32[]{:S(2)}) copy-start(f32[16,1,64,128]{3,2,1,0:T(8,128)} %param.41) | copy-start | bytes 1572868
  57.4 10.8 %copy-start.5 = (bf16[64,2048]{1,0:T(8,128)(2,1)S(1)}, bf16[64,2048]{1,0:T(8,128)(2,1)}, u32[]{:S(2)}) copy-start(bf16[64,2048]{1,0:T(8,128)(2,1)} %param.43) | copy-start | bytes 786436
  57.4 10.8 %copy-start.12 = (f32[64]{0:T(128)S(1)}, f32[64]{0:T(128)}, u32[]{:S(2)}) copy-start(f32[64]{0:T(128)} %param.42) | copy-start | bytes 772
  58.7 8.2 %all-to-all-start.1 = ((bf16[4,16,128]{2,1,0:T(8,128)(2,1)}), bf16[4,16,128]{2,1,0:T(8,128)(2,1)S(1)}, u32[]{:S(2)}, u32[]{:S(2)}) async-start(bf16[4,16,128]{2,1,0:T(8,128)(2,1)} %broadcast_in_dim.206), calls=%async_computation.1 | async-start | bytes 32768 | tf_op jit(solution)/shard_map/all_to_all | solution.py:19
  69.1 12.0 %all-to-all-start.2 = ((bf16[16,32,128]{2,1,0:T(8,128)(2,1)}), bf16[16,32,128]{2,1,0:T(8,128)(2,1)S(1)}, u32[]{:S(2)}, u32[]{:S(2)}) async-start(bf16[16,32,128]{2,1,0:T(8,128)(2,1)} %pad_maximum_fusion.2), calls=%async_computation.2 | async-start | bytes 262144 | tf_op jit(solution)/shard_map/all_to_all | solution.py:19
  81.8 18.7 %all-to-all-start.3 = ((bf16[16,16,128]{2,1,0:T(8,128)(2,1)}), bf16[16,16,128]{2,1,0:T(8,128)(2,1)S(1)}, u32[]{:S(2)}, u32[]{:S(2)}) async-start(bf16[16,16,128]{2,1,0:T(8,128)(2,1)} %broadcast_in_dim.210), calls=%async_computation.3 | async-start | bytes 131072 | tf_op jit(solution)/shard_map/all_to_all | solution.py:19
  100.5 7.4 %collective-permute-start.1 = (bf16[256,128]{1,0:T(8,128)(2,1)S(1)}, bf16[256,128]{1,0:T(8,128)(2,1)S(1)}, u32[]{:S(2)}, u32[]{:S(2)}) collective-permute-start(bf16[256,128]{1,0:T(8,128)(2,1)S(1)} %bitcast.150), channel_id=1, source_target_pairs={{0,16},{16,0},{32,48},{48,32},{64,80},{80,64},{96,112},{112,96},{1... | collective-permute-start | bytes 196616 | tf_op jit(solution)/shard_map/ppermute | solution.py:190
  109.5 17.4 %all-to-all-start.4 = ((bf16[16,48,512]{2,1,0:T(8,128)(2,1)}), bf16[16,48,512]{2,1,0:T(8,128)(2,1)S(1)}, u32[]{:S(2)}, u32[]{:S(2)}) async-start(bf16[16,48,512]{2,1,0:T(8,128)(2,1)} %pad_maximum_fusion), calls=%async_computation.4 | async-start | bytes 1572864 | tf_op jit(solution)/shard_map/all_to_all | solution.py:19
  132.5 14.0 %all-to-all-start.5 = ((bf16[16,128,128]{2,1,0:T(8,128)(2,1)}), bf16[16,128,128]{2,1,0:T(8,128)(2,1)S(1)}, u32[]{:S(2)}, u32[]{:S(2)}) async-start(bf16[16,128,128]{2,1,0:T(8,128)(2,1)} %pad_maximum_fusion.1), calls=%async_computation.5 | async-start | bytes 1048576 | tf_op jit(solution)/shard_map/all_to_all | solution.py:19
  136.2 10.4 %copy-start.2 = (bf16[224,128]{1,0:T(8,128)(2,1)S(1)}, bf16[224,128]{1,0:T(8,128)(2,1)}, u32[]{:S(2)}) copy-start(bf16[224,128]{1,0:T(8,128)(2,1)} %param.53) | copy-start | bytes 172036
  146.9 10.0 %slice-start = ((bf16[16,2,3,512]{3,1,2,0:T(2,128)(2,1)}), bf16[16,2,2,512]{3,1,2,0:T(2,128)(2,1)S(1)}, s32[]{:S(2)}) async-start(bf16[16,2,3,512]{3,1,2,0:T(2,128)(2,1)} %param.40), calls=%async_computation.7 | async-start | bytes 131072 | tf_op jit(solution)/shard_map/slice | solution.py:183
  147.4 5.0 %collective-permute-start.2 = (f32[256,128]{1,0:T(8,128)S(1)}, f32[256,128]{1,0:T(8,128)S(1)}, u32[]{:S(2)}, u32[]{:S(2)}) collective-permute-start(f32[256,128]{1,0:T(8,128)S(1)} %convolution_add_fusion), channel_id=1, source_target_pairs={{0,16},{16,0},{32,48},{48,32},{64,80},{80,64},{96,112},{112,96},{1... | collective-permute-start | bytes 393224 | tf_op jit(solution)/shard_map/ppermute | solution.py:294
  153.3 15.2 %all-to-all-start.6 = ((bf16[16,16,128]{2,1,0:T(8,128)(2,1)}), bf16[16,16,128]{2,1,0:T(8,128)(2,1)S(1)}, u32[]{:S(2)}, u32[]{:S(2)}) async-start(bf16[16,16,128]{2,1,0:T(8,128)(2,1)} %bitcast.46), calls=%async_computation.6 | async-start | bytes 131072 | tf_op jit(solution)/shard_map/all_to_all | solution.py:19

commit v3 on v2

--- a/solution.py
+++ b/solution.py
@@ -79,7 +79,10 @@
     rows_k = gate_weight.shape[0]
     cols = width // n_tp
     same_core = [[CORES * z + c for z in range(chips)] for c in range(CORES)]
-    swap = [(i, i ^ 1) for i in range(n_ep)]
+
+    def from_other_core(shard):
+        return lax.ppermute(shard, "ep", [(i, i ^ 1) for i in range(n_ep)])
+
     same_group = [[PER_GROUP * g + m for m in range(PER_GROUP)] for g in range(GROUPS)]
     part = 2 * STATE // PER_GROUP
 
@@ -94,7 +97,7 @@
         head_pick, step_weight, (((1,), (1,)), ((), ())), preferred_element_type=F32
     ).astype(BF)
     first = jax.nn.sigmoid(route_scores[:, 0] - route_scores[:, 1])
-    first_high = first.astype(BF).astype(F32)
+    first_high = lax.reduce_precision(first, 8, 7)
     first_low = first - first_high
     lane = jnp.arange(4 * seqs)[None]
     spread = jnp.where(
@@ -113,7 +116,7 @@
     extra = jnp.pad(extra, ((0, 0), (0, pack_cols - rows_k)))
     pack = jnp.concatenate([main, extra], axis=0)
     own_pack = exchange(to_everyone(pack, chips), "ep", same_core)
-    other_pack = lax.ppermute(own_pack, "ep", swap)
+    other_pack = from_other_core(own_pack)
 
     normed = rms_scale(tokens.astype(F32), mix_gain).astype(BF)
     by_core = normed.reshape(seqs, chips, CORES, rows_k)
@@ -171,6 +174,31 @@
     gated = readout * jax.nn.silu(gate_part.astype(F32))
     head_out = rms_scale(gated, head_gain).astype(BF)
 
+    total = chips * seqs
+    at = jnp.arange(total)[:, None]
+    by_source = (at // seqs == jnp.arange(chips)[None]).astype(BF)
+    route_rows = dot32(by_source, own_pack[:, gate_weight.shape[0] + 1, : 4 * seqs])
+    route_lane = jnp.arange(4 * seqs)[None]
+    class_routes = jnp.concatenate(
+        [
+            jnp.sum(
+                jnp.where(route_lane == which * seqs + at % seqs, route_rows, 0.0),
+                axis=1,
+                keepdims=True,
+            )
+            for which in range(4)
+        ],
+        axis=1,
+    )
+
+    units = CORES * dense_gate.shape[1]
+    gate_pair = [expert_gate[0], from_other_core(expert_gate[0])]
+    up_pair = [expert_up[0], from_other_core(expert_up[0])]
+    down_pair = [expert_down[0], from_other_core(expert_down[0])]
+    own_dense = jnp.concatenate([dense_gate, dense_up], axis=1)
+    other_dense = from_other_core(own_dense)
+    chip_down = jnp.concatenate([dense_down, from_other_core(dense_down)], axis=0)
+
     partial_mix = dot32(head_out, mixer_out)
     mix_pieces = partial_mix.astype(BF).reshape(seqs, n_tp, cols).transpose(1, 0, 2)
     parts_sent = jnp.where(tp % 2 == 0, write_part, read_part)
@@ -185,63 +213,65 @@
     resid = slice_at(tokens, tp * cols, cols, 1).astype(F32) + mixed.astype(F32)
     gain_own = slice_at(moe_gain, tp * cols, cols, 0)
     scaled = (resid * gain_own).astype(BF)
-    scaled_own = exchange(to_everyone(scaled, chips), "ep", same_core)
-    scaled_own = scaled_own.reshape(chips * seqs, cols)
-    scaled_other = lax.ppermute(scaled_own, "ep", swap)
-    scaled_all = jnp.concatenate([scaled_own, scaled_other], axis=0)
-
-    own_routes = own_pack[:, rows_k + 1, : 4 * seqs].astype(F32)
-    other_routes = other_pack[:, rows_k + 1, : 4 * seqs].astype(F32)
-    routes = jnp.concatenate([own_routes, other_routes], axis=0)
-    mine = ep.astype(F32)
-    is_first = routes[:, :seqs] == mine
-    is_second = routes[:, seqs : 2 * seqs] == mine
-    first_all = routes[:, 2 * seqs : 3 * seqs] + routes[:, 3 * seqs :]
+    class_scaled = exchange(to_everyone(scaled, chips), "ep", same_core).reshape(total, cols)
+
+    first_all = class_routes[:, 2:3] + class_routes[:, 3:4]
+    place = jnp.arange(total)
+    block = place // seqs
+    earlier = ((block[:, None] == block[None]) & (place[None] < place[:, None])).astype(BF)
+    mine = jnp.stack([ep, ep + 1 - 2 * core]).astype(F32)[None]
+    is_first = class_routes[:, 0:1] == mine
+    named = is_first | (class_routes[:, 1:2] == mine)
     weight = jnp.where(is_first, first_all, 1.0 - first_all)
-    named = is_first | is_second
-    earlier = (jnp.arange(seqs)[:, None] < jnp.arange(seqs)[None]).astype(BF)
-    rank = dot32(named.astype(BF), earlier)
-    key = jnp.where(named, rank, -1.0)
-    total = n_ep * seqs
-    place = jnp.arange(total)[None]
-    tiled = (place % seqs == jnp.arange(seqs)[:, None]).astype(F32)
-    own_block = place // seqs == jnp.arange(n_ep)[:, None]
-    spread = jnp.dot(
-        jnp.concatenate([key, weight], axis=0), tiled, precision=lax.Precision.HIGHEST
-    )
-    key_row = jnp.sum(jnp.where(own_block, spread[:n_ep], 0.0), axis=0, keepdims=True)
-    weight_row = jnp.sum(jnp.where(own_block, spread[n_ep:], 0.0), axis=0, keepdims=True)
-    slots = TOP * n_ep
-    slot = jnp.arange(slots)[:, None]
-    chosen = (slot // TOP == place // seqs) & (key_row == (slot % TOP).astype(F32))
-    slot_weight = jnp.sum(jnp.where(chosen, weight_row, 0.0), axis=1, keepdims=True)
+    weight_high = lax.reduce_precision(weight, 8, 7)
+    weight_low = (weight - weight_high).astype(BF)
+    rank = jnp.where(named, dot32(earlier, named.astype(BF)), -1.0)
+    per_expert = TOP * chips
+    slots = CORES * per_expert
+    slot = jnp.arange(slots)[None]
+    key = jnp.where(slot < per_expert, rank[:, 0:1], rank[:, 1:2])
+    chosen = (slot % per_expert // TOP == block[:, None]) & (key == (slot % TOP).astype(F32))
     chosen = chosen.astype(BF)
-
-    units = dense_gate.shape[1]
+    by_slot = lax.dot_general(
+        chosen,
+        jnp.concatenate([weight_high.astype(BF), weight_low], axis=1),
+        (((0,), (0,)), ((), ())),
+        preferred_element_type=F32,
+    )
+    slot_weight = jnp.where(
+        jnp.arange(slots)[:, None] < per_expert,
+        by_slot[:, 0:1] + by_slot[:, 2:3],
+        by_slot[:, 1:2] + by_slot[:, 3:4],
+    )
+
     half = -(-(units + 2) // 128) * 128
+    own_units = units // CORES
     blend_col = slice_at(blend_vector, tp * cols, cols, 0)[:, None]
     both_dense = jnp.concatenate(
         [
-            dense_gate,
+            own_dense[:, :own_units],
+            other_dense[:, :own_units],
             blend_col,
             jnp.zeros((cols, half - units - 1), BF),
-            dense_up,
+            own_dense[:, own_units:],
+            other_dense[:, own_units:],
             jnp.zeros((cols, half - units), BF),
         ],
         axis=1,
     )
-    plain = scaled_all.astype(F32) / gain_own
+    plain = class_scaled.astype(F32) / gain_own
     square_sum = jnp.sum(plain * plain, axis=1, keepdims=True)
-    dense_partial = dot32(scaled_all, both_dense)
+    dense_partial = dot32(class_scaled, both_dense)
     dense_partial = jnp.where(
         jnp.arange(2 * half)[None] == units + 1, square_sum, dense_partial
     ).astype(BF)
-    expert_rows = dot32(chosen, scaled_all).astype(BF)
-    quarter = slots * cols // (2 * half)
+    expert_rows = lax.dot_general(
+        chosen, class_scaled, (((0,), (0,)), ((), ())), preferred_element_type=F32
+    ).astype(BF)
+    wide = 2 * half // cols
+    deep = slots // wide
     expert_block = (
-        expert_rows.reshape(slots // quarter, quarter, cols)
-        .transpose(1, 0, 2)
-        .reshape(quarter, 2 * half)
+        expert_rows.reshape(wide, deep, cols).transpose(1, 0, 2).reshape(deep, 2 * half)
     )
     share = total // n_tp
     arrived = exchange(
@@ -254,45 +284,41 @@
     dense_inner = jnp.sum(arrived[:, :share].astype(F32), axis=0)
     rows = (
         arrived[:, share:]
-        .reshape(n_tp, quarter, slots // quarter, cols)
+        .reshape(n_tp, deep, wide, cols)
         .transpose(2, 1, 0, 3)
         .reshape(slots, width)
     )
     plain_rows = rows.astype(F32) / moe_gain
     row_scale = lax.rsqrt(jnp.mean(plain_rows * plain_rows, axis=1, keepdims=True) + EPS)
-    gate_vals = dot32(rows, expert_gate[0]) * row_scale
-    up_vals = dot32(rows, expert_up[0]) * row_scale
-    act = (jax.nn.silu(gate_vals) * up_vals).astype(BF)
-    partial_out = dot32(act, expert_down[0]).astype(BF)
+
+    def expert_share(which):
+        here = slice(which * per_expert, (which + 1) * per_expert)
+        gate_vals = dot32(rows[here], gate_pair[which]) * row_scale[here]
+        up_vals = dot32(rows[here], up_pair[which]) * row_scale[here]
+        act = (jax.nn.silu(gate_vals) * up_vals).astype(BF)
+        return dot32(act, down_pair[which]).astype(BF)
+
+    partial_out = jnp.concatenate([expert_share(0), expert_share(1)], axis=0)
     out_pieces = partial_out.reshape(slots, n_tp, cols).transpose(1, 0, 2)
     scale = lax.rsqrt(dense_inner[:, units + 1 : units + 2] / width + EPS)
     blend = jax.nn.sigmoid(dense_inner[:, units : units + 1] * scale)
     dense_act = (
         blend * jax.nn.silu(dense_inner[:, :half] * scale) * (dense_inner[:, half:] * scale)
     ).astype(BF)
-    act_block = jnp.concatenate([dense_act[:, :128], dense_act[:, 128:]], axis=0)
+    tiles = half // 128
+    act_block = dense_act.reshape(share, tiles, 128).transpose(1, 0, 2).reshape(tiles * share, 128)
     arrived = exchange(
         jnp.concatenate([out_pieces, to_everyone(act_block, n_tp)], axis=1), "tp"
     )
     expert_out = jnp.sum(arrived[:, :slots].astype(F32), axis=0) * slot_weight
-    expert_out = expert_out.astype(BF)
-    down = jnp.pad(dense_down, ((0, half - units), (0, 0)))
-
-    def outputs_of(core_rank):
-        acts = arrived[core_rank * n_tp // CORES : (core_rank + 1) * n_tp // CORES, slots:]
-        tokens_of = total // CORES
-        slots_of = slice(core_rank * slots // CORES, (core_rank + 1) * slots // CORES)
-        picks = chosen[slots_of, core_rank * tokens_of : (core_rank + 1) * tokens_of]
-        return (
-            dot32(acts[:, :share].reshape(tokens_of, 128), down[:128])
-            + dot32(acts[:, share:].reshape(tokens_of, 128), down[128:])
-            + lax.dot_general(
-                picks, expert_out[slots_of], (((0,), (0,)), ((), ())), preferred_element_type=F32
-            )
-        )
-
-    swapped = lax.ppermute(outputs_of(1), "ep", swap)
-    summed = outputs_of(0) + swapped
+    act_all = (
+        arrived[:, slots:]
+        .reshape(n_tp, tiles, share, 128)
+        .transpose(0, 2, 1, 3)
+        .reshape(total, half)
+    )
+    down = jnp.pad(chip_down, ((0, half - units), (0, 0)))
+    summed = dot32(act_all, down) + dot32(chosen, expert_out.astype(BF))
     final = exchange(summed.astype(BF).reshape(chips, seqs, cols), "ep", same_core)
     output = resid + jnp.sum(final.astype(F32), axis=0)
     return (output, new_recurrent[:, None], inner_window[:, 1:], new_access)

time: 170 us -> 166 us (0.976)
  waiting for transfers between devices: 77.7 us -> 59.9 us
  starting transfers between devices: 61.8 us -> 70.2 us
  matrix products: 7.79 us -> 11.5 us
    all_to_all x7, waiting for transfers between devices: 74.5 us -> 58.3 us  [exchange(): lax.all_to_all(pieces, axis, split_axis=0, concat_axis=0, tiled=True, axi...]
    ppermute x3 -> x6, starting transfers between devices: 18.9 us -> 23.9 us  [from_other_core(): return lax.ppermute(shard, 'ep', [(i, i ^ 1) for i in range(n_ep)])]
    dot_general x12, matrix products: 5.51 us -> 9.49 us  [dot32(): return jnp.dot(left, right, preferred_element_type=F32)]
    all_to_all x7, starting transfers between devices: 42.9 us -> 46.2 us  [exchange(): lax.all_to_all(pieces, axis, split_axis=0, concat_axis=0, tiled=True, axi...]
  transfers between devices with their start and end apart: 10 -> 13, of which waited for: 10 -> 7; matrix products, arithmetic and copies ran while one was open for 5% -> 13% of each run, Pallas kernels for 0% -> 0%
where the time goes in v3:
time: 166 us; the launch traced here: 164 us
  starting transfers between devices  70.2 us (42%)
  waiting for transfers between devices  59.9 us (36%)
  other arithmetic  12.4 us (7%)
  matrix products  11.5 us (7%)
  local copies, waits for them, and re-layouts  7.7 us (5%)
  between operations  2.28 us (1%)
    all_to_all x7, waiting for transfers between devices, exchange(): lax.all_to_all(pieces, axis, split_axis=0, concat_axis=0, tiled=True, axi...  58.3 us
    all_to_all x7, starting transfers between devices, exchange(): lax.all_to_all(pieces, axis, split_axis=0, concat_axis=0, tiled=True, axi...  46.2 us
    ppermute x6, starting transfers between devices, from_other_core(): return lax.ppermute(shard, 'ep', [(i, i ^ 1) for i in range(n_ep)])  23.9 us
    dot_general x12, matrix products, dot32(): return jnp.dot(left, right, preferred_element_type=F32)  9.49 us
  transfers between devices with their start and end apart: 13, of which 7 were waited for; matrix products, arithmetic and copies ran while one was open for 13% of the time, Pallas kernels for 0%

profile of v3, /device:TPU:1, one launch (start us, length us, event | category | flops | bytes accessed | tf_op | source)
XLA Modules:
  0.0 164.0 jit_solution(430037031304738857)
XLA Ops:
  0.8 0.8 fusion.131
  1.7 0.8 convert_bitcast_fusion.2
  2.5 0.8 fusion.9
  3.3 0.7 dynamic-slice_select_fusion
  4.5 0.8 fusion.48
  5.3 0.9 broadcast_in_dim.247
  6.2 15.9 %all-to-all-start = ((bf16[16,72,192]{2,1,0:T(8,128)(2,1)}), bf16[16,72,192]{2,1,0:T(8,128)(2,1)S(1)}, u32[]{:S(2)}, u32[]{:S(2)}) async-start(bf16[16,72,192]{2,1,0:T(8,128)(2,1)} %broadcast_in_dim.247), calls=%async_computation | async-start | bytes 1179648 | tf_op jit(solution)/shard_map/all_to_all | solution.py:19
  22.1 2.9 %collective-permute-start.1 = (bf16[128,448]{0,1:T(8,128)(2,1)S(1)}, bf16[128,448]{0,1:T(8,128)(2,1)S(1)}, u32[]{:S(2)}, u32[]{:S(2)}) collective-permute-start(bf16[128,448]{0,1:T(8,128)(2,1)S(1)} %pad_maximum_fusion.3), channel_id=1, source_target_pairs={{0,16},{16,0},{32,48},{48,32},{64,80},{80,64},{96,112},{112,96},{1... | collective-permute-start | bytes 344072 | tf_op jit(solution)/shard_map/ppermute | solution.py:84
  25.0 0.1 fusion.20
  25.3 0.2 reshape.502
  25.5 0.6 dynamic_slice.34
  26.8 0.6 dynamic_slice.33
  27.4 0.6 dynamic_slice.37
  28.0 0.8 dynamic-slice_bitcast_fusion
  28.9 0.7 dynamic-slice_convert_fusion
  29.7 0.2 fusion.127
  29.9 17.5 %all-to-all-done = bf16[16,72,192]{2,1,0:T(8,128)(2,1)S(1)} async-done(((bf16[16,72,192]{2,1,0:T(8,128)(2,1)}), bf16[16,72,192]{2,1,0:T(8,128)(2,1)S(1)}, u32[]{:S(2)}, u32[]{:S(2)}) %all-to-all-start) | async-done | bytes 442400 | tf_op jit(solution)/shard_map/all_to_all | solution.py:19
  47.4 8.3 %collective-permute-start = (bf16[16,72,192]{2,1,0:T(8,128)(2,1)S(1)}, bf16[16,72,192]{2,1,0:T(8,128)(2,1)S(1)}, u32[]{:S(2)}, u32[]{:S(2)}) collective-permute-start(bf16[16,72,192]{2,1,0:T(8,128)(2,1)S(1)} %all-to-all-done), channel_id=1, source_target_pairs={{0,16},{16,0},{32,48},{48,32},{64,80},{80,64},{96,112},{112,96},{1... | collective-permute-start | bytes 1327112 | tf_op jit(solution)/shard_map/ppermute | solution.py:84
  55.8 1.6 collective-permute-done
  57.4 0.2 multiply_reduce_fusion.2
  57.6 0.2 convolution_bitcast_fusion.1
  57.8 0.2 fusion.7
  58.2 0.6 broadcast_in_dim.249
  58.9 4.0 %all-to-all-start.1 = ((bf16[4,16,128]{2,1,0:T(8,128)(2,1)}), bf16[4,16,128]{2,1,0:T(8,128)(2,1)S(1)}, u32[]{:S(2)}, u32[]{:S(2)}) async-start(bf16[4,16,128]{2,1,0:T(8,128)(2,1)} %broadcast_in_dim.249), calls=%async_computation.1 | async-start | bytes 32768 | tf_op jit(solution)/shard_map/all_to_all | solution.py:19
  62.9 0.7 multiply_exponential_fusion
  63.6 3.5 %all-to-all-done.1 = bf16[4,16,128]{2,1,0:T(8,128)(2,1)S(1)} async-done(((bf16[4,16,128]{2,1,0:T(8,128)(2,1)}), bf16[4,16,128]{2,1,0:T(8,128)(2,1)S(1)}, u32[]{:S(2)}, u32[]{:S(2)}) %all-to-all-start.1) | async-done | bytes 16416 | tf_op jit(solution)/shard_map/all_to_all | solution.py:19
  67.1 0.4 fusion.12
  67.6 0.8 multiply_reduce_fusion.5
  68.4 0.2 fusion.2
  68.6 0.7 pad_maximum_fusion.2
  69.3 5.1 %all-to-all-start.2 = ((bf16[16,32,128]{2,1,0:T(8,128)(2,1)}), bf16[16,32,128]{2,1,0:T(8,128)(2,1)S(1)}, u32[]{:S(2)}, u32[]{:S(2)}) async-start(bf16[16,32,128]{2,1,0:T(8,128)(2,1)} %pad_maximum_fusion.2), calls=%async_computation.2 | async-start | bytes 262144 | tf_op jit(solution)/shard_map/all_to_all | solution.py:19
  74.5 0.3 concatenate.57
  74.8 0.3 select_reduce_fusion
  75.0 6.3 %all-to-all-done.2 = bf16[16,32,128]{2,1,0:T(8,128)(2,1)S(1)} async-done(((bf16[16,32,128]{2,1,0:T(8,128)(2,1)}), bf16[16,32,128]{2,1,0:T(8,128)(2,1)S(1)}, u32[]{:S(2)}, u32[]{:S(2)}) %all-to-all-start.2) | async-done | bytes 131104 | tf_op jit(solution)/shard_map/all_to_all | solution.py:19
  81.3 0.6 broadcast_in_dim.253
  82.0 7.1 %all-to-all-start.3 = ((bf16[16,16,128]{2,1,0:T(8,128)(2,1)}), bf16[16,16,128]{2,1,0:T(8,128)(2,1)S(1)}, u32[]{:S(2)}, u32[]{:S(2)}) async-start(bf16[16,16,128]{2,1,0:T(8,128)(2,1)} %broadcast_in_dim.253), calls=%async_computation.3 | async-start | bytes 131072 | tf_op jit(solution)/shard_map/all_to_all | solution.py:19
  89.1 0.2 convolution_select_fusion.1
  89.3 11.3 %all-to-all-done.3 = bf16[16,16,128]{2,1,0:T(8,128)(2,1)S(1)} async-done(((bf16[16,16,128]{2,1,0:T(8,128)(2,1)}), bf16[16,16,128]{2,1,0:T(8,128)(2,1)S(1)}, u32[]{:S(2)}, u32[]{:S(2)}) %all-to-all-start.3) | async-done | bytes 65568 | tf_op jit(solution)/shard_map/all_to_all | solution.py:19
  100.9 0.3 fusion
  101.2 0.3 fusion.5
  101.5 1.0 pad_maximum_fusion
  102.5 3.7 %all-to-all-start.4 = ((bf16[16,24,1024]{2,1,0:T(8,128)(2,1)}), bf16[16,24,1024]{2,1,0:T(8,128)(2,1)S(1)}, u32[]{:S(2)}, u32[]{:S(2)}) async-start(bf16[16,24,1024]{2,1,0:T(8,128)(2,1)} %pad_maximum_fusion), calls=%async_computation.4 | async-start | bytes 1572864 | tf_op jit(solution)/shard_map/all_to_all | solution.py:19
  106.2 6.5 %collective-permute-start.3 = (bf16[2048,256]{1,0:T(8,128)(2,1)}, bf16[2048,256]{1,0:T(8,128)(2,1)}, u32[]{:S(2)}, u32[]{:S(2)}) collective-permute-start(bf16[2048,256]{1,0:T(8,128)(2,1)} %bitcast.186), channel_id=1, source_target_pairs={{0,16},{16,0},{32,48},{48,32},{64,80},{80,64},{96,112},{112,96},{1... | collective-permute-start | bytes 3145736 | tf_op jit(solution)/shard_map/ppermute | solution.py:84
  112.8 1.9 %collective-permute-start.2 = (bf16[2048,256]{1,0:T(8,128)(2,1)S(1)}, bf16[2048,256]{1,0:T(8,128)(2,1)}, u32[]{:S(2)}, u32[]{:S(2)}) collective-permute-start(bf16[2048,256]{1,0:T(8,128)(2,1)S(1)} %bitcast.183), channel_id=1, source_target_pairs={{0,16},{16,0},{32,48},{48,32},{64,80},{80,64},{96,112},{112,96},{1... | collective-permute-start | bytes 3145736 | tf_op jit(solution)/shard_map/ppermute | solution.py:84
  114.7 2.4 %collective-permute-start.4 = (bf16[256,2048]{1,0:T(8,128)(2,1)}, bf16[256,2048]{1,0:T(8,128)(2,1)}, u32[]{:S(2)}, u32[]{:S(2)}) collective-permute-start(bf16[256,2048]{1,0:T(8,128)(2,1)} %bitcast.187), channel_id=1, source_target_pairs={{0,16},{16,0},{32,48},{48,32},{64,80},{80,64},{96,112},{112,96},{1... | collective-permute-start | bytes 3145736 | tf_op jit(solution)/shard_map/ppermute | solution.py:84
  117.1 1.9 %collective-permute-start.5 = (bf16[224,128]{1,0:T(8,128)(2,1)}, bf16[224,128]{1,0:T(8,128)(2,1)}, u32[]{:S(2)}, u32[]{:S(2)}) collective-permute-start(bf16[224,128]{1,0:T(8,128)(2,1)} %param.53), channel_id=1, source_target_pairs={{0,16},{16,0},{32,48},{48,32},{64,80},{80,64},{96,112},{112,96},{1... | collective-permute-start | bytes 172040 | tf_op jit(solution)/shard_map/ppermute | solution.py:84
  119.2 0.9 fusion.93
  120.1 0.2 multiply_reduce_fusion
  120.5 0.2 fusion.84
  121.3 0.2 convolution_multiply_fusion.3
  121.6 1.5 convolution_multiply_fusion
  123.2 2.0 %convolution_convert_fusion.1 = bf16[32,2048]{1,0:T(8,128)(2,1)S(1)} fusion(bf16[4,8,16,128]{3,2,1,0:T(8,128)(2,1)S(1)} %copy.147, f32[32,256]{1,0:T(8,128)S(1)} %convolution_multiply_fusion.3, f32[32]{0:T(128)S(1)} %mul.398, bf16[1,256,2048]{2,1,0:T(8,128)(2,1)} %param.49, bf16[1,2048,256]{2,1,0:T(8,128)(2,1)S(1)} %copy-done.3), kind=kOutput, calls=%fused_computation.1 | convolution fusion | flops 67231744 | bytes 2392192 | tf_op jit(solution)/shard_map/dot_general | solution.py:34
  125.1 2.3 %convolution_convert_fusion = bf16[32,2048]{1,0:T(8,128)(2,1)S(1)} fusion(bf16[256,2048]{1,0:T(8,128)(2,1)} %collective-permute-done.4, f32[32,256]{1,0:T(8,128)S(1)} %convolution_multiply_fusion, bf16[2048,256]{1,0:T(8,128)(2,1)} %collective-permute-done.2, bf16[4,8,16,128]{3,2,1,0:T(8,128)(2,1)S(1)} %copy.146, f32[32]{0:T(128)S(1)} %mul.404), kind=kOutput, calls=%fused_computation | convolution fusion | flops 67231744 | bytes 2392192 | tf_op jit(solution)/shard_map/dot_general | solution.py:34
  127.6 0.8 pad_maximum_fusion.1
  128.5 6.9 %all-to-all-start.5 = ((bf16[16,128,128]{2,1,0:T(8,128)(2,1)}), bf16[16,128,128]{2,1,0:T(8,128)(2,1)S(1)}, u32[]{:S(2)}, u32[]{:S(2)}) async-start(bf16[16,128,128]{2,1,0:T(8,128)(2,1)} %pad_maximum_fusion.1), calls=%async_computation.5 | async-start | bytes 1048576 | tf_op jit(solution)/shard_map/all_to_all | solution.py:19
  135.4 0.6 fusion.70
  136.0 1.0 multiply_add_fusion
  137.0 9.0 %all-to-all-done.5 = bf16[16,128,128]{2,1,0:T(8,128)(2,1)S(1)} async-done(((bf16[16,128,128]{2,1,0:T(8,128)(2,1)}), bf16[16,128,128]{2,1,0:T(8,128)(2,1)S(1)}, u32[]{:S(2)}, u32[]{:S(2)}) %all-to-all-start.5) | async-done | bytes 524320 | tf_op jit(solution)/shard_map/all_to_all | solution.py:19
  146.0 0.3 fusion.64
  146.5 1.7 %fusion.1 = bf16[256,128]{1,0:T(8,128)(2,1)} fusion(f32[256,128]{1,0:T(8,128)S(1)} %fusion.64, bf16[32,8,4,128]{3,2,1,0:T(4,128)(2,1)S(1)} %bitcast.189, bf16[224,128]{1,0:T(8,128)(2,1)} %collective-permute-done.5, bf16[224,128]{1,0:T(8,128)(2,1)} %param.53), kind=kOutput, calls=%fused_computation.6 | convolution fusion | flops 34078720 | bytes 573440 | tf_op jit(solution)/shard_map/dot_general | solution.py:34
  148.2 3.5 %all-to-all-start.6 = ((bf16[16,16,128]{2,1,0:T(8,128)(2,1)}), bf16[16,16,128]{2,1,0:T(8,128)(2,1)S(1)}, u32[]{:S(2)}, u32[]{:S(2)}) async-start(bf16[16,16,128]{2,1,0:T(8,128)(2,1)} %bitcast.48), calls=%async_computation.6 | async-start | bytes 131072 | tf_op jit(solution)/shard_map/all_to_all | solution.py:19
  151.8 0.8 pad_maximum_fusion.4
  152.6 10.8 %all-to-all-done.6 = bf16[16,16,128]{2,1,0:T(8,128)(2,1)S(1)} async-done(((bf16[16,16,128]{2,1,0:T(8,128)(2,1)}), bf16[16,16,128]{2,1,0:T(8,128)(2,1)S(1)}, u32[]{:S(2)}, u32[]{:S(2)}) %all-to-all-start.6) | async-done | bytes 65568 | tf_op jit(solution)/shard_map/all_to_all | solution.py:19
  163.4 0.6 fusion.85
  (140 shorter events, 3.1 us)
Async XLA Ops:
  0.6 67.7 %copy-start = (bf16[64,2048]{1,0:T(8,128)(2,1)S(1)}, bf16[64,2048]{1,0:T(8,128)(2,1)}, u32[]{:S(2)}) copy-start(bf16[64,2048]{1,0:T(8,128)(2,1)} %param.43) | copy-start | bytes 786436
  0.7 118.4 %copy-start.18 = (pred[64]{0:T(512)(128)(4,1)}, pred[64]{0:T(512)(128)(4,1)S(1)}, u32[]{:S(2)}) copy-start(pred[64]{0:T(512)(128)(4,1)S(1)} %iota_compare_fusion.12) | copy-start | bytes 196
  0.7 21.4 %copy-start.6 = (bf16[128,224]{0,1:T(8,128)(2,1)S(1)}, bf16[128,224]{0,1:T(8,128)(2,1)}, u32[]{:S(2)}) copy-start(bf16[128,224]{0,1:T(8,128)(2,1)} %param.51) | copy-start | bytes 172036
  0.7 21.4 %copy-start.7 = (bf16[128,224]{0,1:T(8,128)(2,1)S(1)}, bf16[128,224]{0,1:T(8,128)(2,1)}, u32[]{:S(2)}) copy-start(bf16[128,224]{0,1:T(8,128)(2,1)} %param.52) | copy-start | bytes 172036
  5.3 19.7 %copy-start.4 = (bf16[16,2048]{1,0:T(8,128)(2,1)S(1)}, bf16[16,2048]{1,0:T(8,128)(2,1)}, u32[]{:S(2)}) copy-start(bf16[16,2048]{1,0:T(8,128)(2,1)} %param.27) | copy-start | bytes 196612
  5.3 19.9 %copy-start.9 = (f32[2048]{0:T(1024)S(1)}, f32[2048]{0:T(1024)}, u32[]{:S(2)}) copy-start(f32[2048]{0:T(1024)} %param.28) | copy-start | bytes 24580
  6.2 19.3 %copy-start.20 = (f32[16]{0:T(128)S(1)}, f32[16]{0:T(128)}, u32[]{:S(2)}) copy-start(f32[16]{0:T(128)} %param.35) | copy-start | bytes 196
  6.2 20.6 %copy-start.21 = (f32[16]{0:T(128)S(1)}, f32[16]{0:T(128)}, u32[]{:S(2)}) copy-start(f32[16]{0:T(128)} %param.34) | copy-start | bytes 196
  6.2 21.2 %copy-start.12 = (bf16[4,64]{1,0:T(4,128)(2,1)S(1)}, bf16[4,64]{1,0:T(4,128)(2,1)}, u32[]{:S(2)}) copy-start(bf16[4,64]{1,0:T(4,128)(2,1)} %param.37) | copy-start | bytes 1540
  6.2 21.2 %copy-start.22 = (f32[16]{0:T(128)S(1)}, f32[16]{0:T(128)}, u32[]{:S(2)}) copy-start(f32[16]{0:T(128)} %param.36) | copy-start | bytes 196
  6.2 21.8 %copy-start.10 = (f32[2048]{0:T(1024)S(1)}, f32[2048]{0:T(1024)}, u32[]{:S(2)}) copy-start(f32[2048]{0:T(1024)} %param.44) | copy-start | bytes 24580
  6.2 23.4 %copy-start.5 = (bf16[16,2,3,512]{3,1,2,0:T(2,128)(2,1)S(1)}, bf16[16,2,3,512]{3,1,2,0:T(2,128)(2,1)}, u32[]{:S(2)}) copy-start(bf16[16,2,3,512]{3,1,2,0:T(2,128)(2,1)} %param.40) | copy-start | bytes 294916
  6.2 41.2 %all-to-all-start = ((bf16[16,72,192]{2,1,0:T(8,128)(2,1)}), bf16[16,72,192]{2,1,0:T(8,128)(2,1)S(1)}, u32[]{:S(2)}, u32[]{:S(2)}) async-start(bf16[16,72,192]{2,1,0:T(8,128)(2,1)} %broadcast_in_dim.247), calls=%async_computation | async-start | bytes 1179648 | tf_op jit(solution)/shard_map/all_to_all | solution.py:19
  22.1 52.3 %collective-permute-start.1 = (bf16[128,448]{0,1:T(8,128)(2,1)S(1)}, bf16[128,448]{0,1:T(8,128)(2,1)S(1)}, u32[]{:S(2)}, u32[]{:S(2)}) collective-permute-start(bf16[128,448]{0,1:T(8,128)(2,1)S(1)} %pad_maximum_fusion.3), channel_id=1, source_target_pairs={{0,16},{16,0},{32,48},{48,32},{64,80},{80,64},{96,112},{112,96},{1... | collective-permute-start | bytes 344072 | tf_op jit(solution)/shard_map/ppermute | solution.py:84
  28.9 90.2 %copy-start.23 = (s32[256]{0:T(256)}, s32[256]{0:T(256)S(1)}, u32[]{:S(2)}) copy-start(s32[256]{0:T(256)S(1)} %and_select_fusion.2) | copy-start | bytes 3076
  28.9 90.2 %copy-start.25 = (s32[64]{0:T(128)}, s32[64]{0:T(128)S(1)}, u32[]{:S(2)}) copy-start(s32[64]{0:T(128)S(1)} %get-tuple-element.56) | copy-start | bytes 772
  28.9 90.2 %copy-start.27 = (f32[64]{0:T(128)}, f32[64]{0:T(128)S(1)}, u32[]{:S(2)}) copy-start(f32[64]{0:T(128)S(1)} %get-tuple-element.57) | copy-start | bytes 772
  29.9 33.0 %copy-start.8 = (bf16[16,3,64]{2,0,1:T(8,128)(2,1)S(1)}, bf16[16,3,64]{2,0,1:T(8,128)(2,1)}, u32[]{:S(2)}) copy-start(bf16[16,3,64]{2,0,1:T(8,128)(2,1)} %param.39) | copy-start | bytes 18436
  29.9 37.2 %copy-start.1 = (f32[16,1,64,128]{3,2,1,0:T(8,128)S(1)}, f32[16,1,64,128]{3,2,1,0:T(8,128)}, u32[]{:S(2)}) copy-start(f32[16,1,64,128]{3,2,1,0:T(8,128)} %param.41) | copy-start | bytes 1572868
  47.4 9.9 %collective-permute-start = (bf16[16,72,192]{2,1,0:T(8,128)(2,1)S(1)}, bf16[16,72,192]{2,1,0:T(8,128)(2,1)S(1)}, u32[]{:S(2)}, u32[]{:S(2)}) collective-permute-start(bf16[16,72,192]{2,1,0:T(8,128)(2,1)S(1)} %all-to-all-done), channel_id=1, source_target_pairs={{0,16},{16,0},{32,48},{48,32},{64,80},{80,64},{96,112},{112,96},{1... | collective-permute-start | bytes 1327112 | tf_op jit(solution)/shard_map/ppermute | solution.py:84
  57.6 10.7 %copy-start.17 = (f32[64]{0:T(128)S(1)}, f32[64]{0:T(128)}, u32[]{:S(2)}) copy-start(f32[64]{0:T(128)} %param.42) | copy-start | bytes 772
  58.9 8.2 %all-to-all-start.1 = ((bf16[4,16,128]{2,1,0:T(8,128)(2,1)}), bf16[4,16,128]{2,1,0:T(8,128)(2,1)S(1)}, u32[]{:S(2)}, u32[]{:S(2)}) async-start(bf16[4,16,128]{2,1,0:T(8,128)(2,1)} %broadcast_in_dim.249), calls=%async_computation.1 | async-start | bytes 32768 | tf_op jit(solution)/shard_map/all_to_all | solution.py:19
  69.3 12.0 %all-to-all-start.2 = ((bf16[16,32,128]{2,1,0:T(8,128)(2,1)}), bf16[16,32,128]{2,1,0:T(8,128)(2,1)S(1)}, u32[]{:S(2)}, u32[]{:S(2)}) async-start(bf16[16,32,128]{2,1,0:T(8,128)(2,1)} %pad_maximum_fusion.2), calls=%async_computation.2 | async-start | bytes 262144 | tf_op jit(solution)/shard_map/all_to_all | solution.py:19
  82.0 18.7 %all-to-all-start.3 = ((bf16[16,16,128]{2,1,0:T(8,128)(2,1)}), bf16[16,16,128]{2,1,0:T(8,128)(2,1)S(1)}, u32[]{:S(2)}, u32[]{:S(2)}) async-start(bf16[16,16,128]{2,1,0:T(8,128)(2,1)} %broadcast_in_dim.253), calls=%async_computation.3 | async-start | bytes 131072 | tf_op jit(solution)/shard_map/all_to_all | solution.py:19
  89.3 29.8 %copy-start.13 = (f32[256,1]{0,1:T(1,128)}, f32[256,1]{0,1:T(1,128)S(1)}, u32[]{:S(2)}) copy-start(f32[256,1]{0,1:T(1,128)S(1)} %get-tuple-element.48) | copy-start | bytes 3076
  89.3 29.8 %copy-start.15 = (f32[256,1]{0,1:T(1,128)}, f32[256,1]{0,1:T(1,128)S(1)}, u32[]{:S(2)}) copy-start(f32[256,1]{0,1:T(1,128)S(1)} %get-tuple-element.49) | copy-start | bytes 3076
  102.5 10.3 %copy-start.2 = (bf16[1,2048,256]{2,1,0:T(8,128)(2,1)S(1)}, bf16[1,2048,256]{2,1,0:T(8,128)(2,1)}, u32[]{:S(2)}) copy-start(bf16[1,2048,256]{2,1,0:T(8,128)(2,1)} %param.47) | copy-start | bytes 3145732
  102.5 17.5 %all-to-all-start.4 = ((bf16[16,24,1024]{2,1,0:T(8,128)(2,1)}), bf16[16,24,1024]{2,1,0:T(8,128)(2,1)S(1)}, u32[]{:S(2)}, u32[]{:S(2)}) async-start(bf16[16,24,1024]{2,1,0:T(8,128)(2,1)} %pad_maximum_fusion), calls=%async_computation.4 | async-start | bytes 1572864 | tf_op jit(solution)/shard_map/all_to_all | solution.py:19
  106.2 15.4 %collective-permute-start.3 = (bf16[2048,256]{1,0:T(8,128)(2,1)}, bf16[2048,256]{1,0:T(8,128)(2,1)}, u32[]{:S(2)}, u32[]{:S(2)}) collective-permute-start(bf16[2048,256]{1,0:T(8,128)(2,1)} %bitcast.186), channel_id=1, source_target_pairs={{0,16},{16,0},{32,48},{48,32},{64,80},{80,64},{96,112},{112,96},{1... | collective-permute-start | bytes 3145736 | tf_op jit(solution)/shard_map/ppermute | solution.py:84
  112.8 12.4 %collective-permute-start.2 = (bf16[2048,256]{1,0:T(8,128)(2,1)S(1)}, bf16[2048,256]{1,0:T(8,128)(2,1)}, u32[]{:S(2)}, u32[]{:S(2)}) collective-permute-start(bf16[2048,256]{1,0:T(8,128)(2,1)S(1)} %bitcast.183), channel_id=1, source_target_pairs={{0,16},{16,0},{32,48},{48,32},{64,80},{80,64},{96,112},{112,96},{1... | collective-permute-start | bytes 3145736 | tf_op jit(solution)/shard_map/ppermute | solution.py:84
  114.7 10.4 %collective-permute-start.4 = (bf16[256,2048]{1,0:T(8,128)(2,1)}, bf16[256,2048]{1,0:T(8,128)(2,1)}, u32[]{:S(2)}, u32[]{:S(2)}) collective-permute-start(bf16[256,2048]{1,0:T(8,128)(2,1)} %bitcast.187), channel_id=1, source_target_pairs={{0,16},{16,0},{32,48},{48,32},{64,80},{80,64},{96,112},{112,96},{1... | collective-permute-start | bytes 3145736 | tf_op jit(solution)/shard_map/ppermute | solution.py:84
  117.1 29.4 %collective-permute-start.5 = (bf16[224,128]{1,0:T(8,128)(2,1)}, bf16[224,128]{1,0:T(8,128)(2,1)}, u32[]{:S(2)}, u32[]{:S(2)}) collective-permute-start(bf16[224,128]{1,0:T(8,128)(2,1)} %param.53), channel_id=1, source_target_pairs={{0,16},{16,0},{32,48},{48,32},{64,80},{80,64},{96,112},{112,96},{1... | collective-permute-start | bytes 172040 | tf_op jit(solution)/shard_map/ppermute | solution.py:84
  121.3 1.8 %copy-start.3 = (bf16[1,2048,256]{2,1,0:T(8,128)(2,1)S(1)}, bf16[1,2048,256]{2,1,0:T(8,128)(2,1)}, u32[]{:S(2)}) copy-start(bf16[1,2048,256]{2,1,0:T(8,128)(2,1)} %param.48) | copy-start | bytes 3145732
  127.6 7.8 %copy-start.11 = (f32[64,4]{0,1:T(4,128)S(1)}, f32[64,4]{0,1:T(4,128)}, u32[]{:S(2)}) copy-start(f32[64,4]{0,1:T(4,128)} %fusion.93) | copy-start | bytes 3076
  128.4 17.6 %copy-start.14 = (f32[256,1]{0,1:T(1,128)S(1)}, f32[256,1]{0,1:T(1,128)}, u32[]{:S(2)}) copy-start(f32[256,1]{0,1:T(1,128)} %copy-done.13) | copy-start | bytes 3076
  128.4 17.6 %copy-start.16 = (f32[256,1]{0,1:T(1,128)S(1)}, f32[256,1]{0,1:T(1,128)}, u32[]{:S(2)}) copy-start(f32[256,1]{0,1:T(1,128)} %copy-done.15) | copy-start | bytes 3076
  128.4 17.6 %copy-start.19 = (pred[64]{0:T(512)(128)(4,1)S(1)}, pred[64]{0:T(512)(128)(4,1)}, u32[]{:S(2)}) copy-start(pred[64]{0:T(512)(128)(4,1)} %copy-done.18) | copy-start | bytes 196
  128.4 17.6 %copy-start.24 = (s32[256]{0:T(256)S(1)}, s32[256]{0:T(256)}, u32[]{:S(2)}) copy-start(s32[256]{0:T(256)} %copy-done.23) | copy-start | bytes 3076
  128.4 17.6 %copy-start.26 = (s32[64]{0:T(128)S(1)}, s32[64]{0:T(128)}, u32[]{:S(2)}) copy-start(s32[64]{0:T(128)} %copy-done.25) | copy-start | bytes 772
  128.4 17.6 %copy-start.28 = (f32[64]{0:T(128)S(1)}, f32[64]{0:T(128)}, u32[]{:S(2)}) copy-start(f32[64]{0:T(128)} %copy-done.27) | copy-start | bytes 772
  128.5 17.5 %all-to-all-start.5 = ((bf16[16,128,128]{2,1,0:T(8,128)(2,1)}), bf16[16,128,128]{2,1,0:T(8,128)(2,1)S(1)}, u32[]{:S(2)}, u32[]{:S(2)}) async-start(bf16[16,128,128]{2,1,0:T(8,128)(2,1)} %pad_maximum_fusion.1), calls=%async_computation.5 | async-start | bytes 1048576 | tf_op jit(solution)/shard_map/all_to_all | solution.py:19
  146.3 5.4 %slice-start = ((bf16[16,2,3,512]{3,1,2,0:T(2,128)(2,1)}), bf16[16,2,2,512]{3,1,2,0:T(2,128)(2,1)S(1)}, s32[]{:S(2)}) async-start(bf16[16,2,3,512]{3,1,2,0:T(2,128)(2,1)} %param.40), calls=%async_computation.7 | async-start | bytes 131072 | tf_op jit(solution)/shard_map/slice | solution.py:211
  148.2 15.1 %all-to-all-start.6 = ((bf16[16,16,128]{2,1,0:T(8,128)(2,1)}), bf16[16,16,128]{2,1,0:T(8,128)(2,1)S(1)}, u32[]{:S(2)}, u32[]{:S(2)}) async-start(bf16[16,16,128]{2,1,0:T(8,128)(2,1)} %bitcast.48), calls=%async_computation.6 | async-start | bytes 131072 | tf_op jit(solution)/shard_map/all_to_all | solution.py:19

commit v4 on v3

--- a/solution.py
+++ b/solution.py
@@ -13,6 +13,7 @@
 BF = jnp.bfloat16
 F32 = jnp.float32
 CORES = 2
+CLASSES = 8
 
 
 def exchange(pieces, axis, groups=None):
@@ -75,7 +76,6 @@
     tp = lax.axis_index("tp")
     core = ep % CORES
     group = tp // PER_GROUP
-    member = tp % PER_GROUP
     rows_k = gate_weight.shape[0]
     cols = width // n_tp
     same_core = [[CORES * z + c for z in range(chips)] for c in range(CORES)]
@@ -83,14 +83,13 @@
     def from_other_core(shard):
         return lax.ppermute(shard, "ep", [(i, i ^ 1) for i in range(n_ep)])
 
-    same_group = [[PER_GROUP * g + m for m in range(PER_GROUP)] for g in range(GROUPS)]
-    part = 2 * STATE // PER_GROUP
+    per_class = n_ep // CLASSES
+    same_class = [[CLASSES * j + r for j in range(per_class)] for r in range(CLASSES)]
+    near = [[CLASSES * j + r for r in range(CLASSES)] for j in range(per_class)]
 
     write_own = slice_at(write_weight, group * STATE, STATE, 1)
     read_own = slice_at(read_weight, group * STATE, STATE, 1)
-    either = jnp.where(member < PER_GROUP // 2, write_own, read_own)
-    either = jnp.where(member % 2 == 0, either[:, :part], either[:, part:])
-    main = jnp.concatenate([gate_weight, inner_weight, either], axis=1)
+    main = jnp.concatenate([gate_weight, inner_weight, write_own, read_own], axis=1)
     pack_cols = main.shape[1]
     head_pick = (jnp.arange(HEADS) == tp).astype(BF)[None]
     step_row = lax.dot_general(
@@ -115,37 +114,46 @@
     extra = jnp.concatenate([step_row, route_row, jnp.zeros((6, rows_k), BF)], axis=0)
     extra = jnp.pad(extra, ((0, 0), (0, pack_cols - rows_k)))
     pack = jnp.concatenate([main, extra], axis=0)
-    own_pack = exchange(to_everyone(pack, chips), "ep", same_core)
-    other_pack = from_other_core(own_pack)
+    class_pack = exchange(to_everyone(pack, per_class), "ep", same_class)
 
     normed = rms_scale(tokens.astype(F32), mix_gain).astype(BF)
-    by_core = normed.reshape(seqs, chips, CORES, rows_k)
-    own_k = jnp.where(core == 0, by_core[:, :, 0], by_core[:, :, 1])
-    other_k = jnp.where(core == 0, by_core[:, :, 1], by_core[:, :, 0])
-
-    def projected_by(keys, packed):
-        padded = jnp.pad(keys, ((0, 0), (0, 0), (0, packed.shape[1] - rows_k)))
-        main_part = dot32(padded.reshape(seqs, -1), packed.reshape(-1, pack_cols))
-        weights = packed[:, rows_k, :rows_k].astype(F32)
-        step_part = jnp.sum(keys.astype(F32) * weights[None], axis=(1, 2))
-        return main_part, step_part
-
-    main_a, step_a = projected_by(own_k, own_pack)
-    main_b, step_b = projected_by(other_k, other_pack)
-    projected = main_a + main_b
-    step_raw = step_a + step_b
+    keys = normed.reshape(seqs, per_class, CLASSES, rows_k).transpose(2, 0, 1, 3)
+    keys = exchange(keys.reshape(CLASSES, seqs, per_class * rows_k), "ep", near)
+    keys = keys.reshape(CLASSES * seqs, per_class, rows_k)
+    padded = jnp.pad(keys, ((0, 0), (0, 0), (0, pack.shape[0] - rows_k)))
+    main_share = dot32(padded.reshape(CLASSES * seqs, -1), class_pack.reshape(-1, pack_cols))
+    step_rows = class_pack[:, rows_k, :rows_k].astype(F32)
+    step_share = jnp.sum(keys.astype(F32) * step_rows[None], axis=(1, 2)).reshape(CLASSES, seqs, 1)
+    route_rows = class_pack[:, rows_k + 1, : 4 * seqs].astype(F32)
+    route_rows = jnp.pad(route_rows, ((0, seqs - per_class), (0, 0)))
+    shares = exchange(
+        jnp.concatenate(
+            [
+                main_share.reshape(CLASSES, seqs, pack_cols),
+                step_share,
+                jnp.zeros((CLASSES, seqs, 63), F32),
+                to_everyone(route_rows, CLASSES),
+            ],
+            axis=2,
+        ),
+        "ep",
+        near,
+    )
+    projected = jnp.sum(shares[:, :, : pack_cols + 1], axis=0)
+    step_raw = projected[:, pack_cols]
+    own_routes = lax.dynamic_index_in_dim(
+        shares[:, :per_class, pack_cols + 64 :].reshape(
+            CLASSES // CORES, CORES, per_class, 4 * seqs
+        ),
+        core,
+        1,
+        False,
+    )
+    own_routes = own_routes.transpose(1, 0, 2).reshape(chips, 4 * seqs)
     gate_part = projected[:, :HEAD_DIM].astype(BF)
     inner_part = projected[:, HEAD_DIM : 2 * HEAD_DIM].astype(BF)
-    share_part = projected[:, 2 * HEAD_DIM :].astype(BF)
-    none = jnp.zeros_like(share_part)
-    placed = jnp.where(
-        member % 2 == 0,
-        jnp.concatenate([share_part, none], axis=1),
-        jnp.concatenate([none, share_part], axis=1),
-    )
-    quarters = exchange(to_everyone(placed, PER_GROUP), "tp", same_group)
-    write_part = quarters[0] + quarters[1]
-    read_part = quarters[2] + quarters[3]
+    write_part = projected[:, 2 * HEAD_DIM : 2 * HEAD_DIM + STATE].astype(BF)
+    read_part = projected[:, 2 * HEAD_DIM + STATE : pack_cols].astype(BF)
 
     inner_window = jnp.concatenate([inner_history, inner_part[:, None, :]], axis=1)
     inner_conv = jax.nn.silu(
@@ -177,7 +185,7 @@
     total = chips * seqs
     at = jnp.arange(total)[:, None]
     by_source = (at // seqs == jnp.arange(chips)[None]).astype(BF)
-    route_rows = dot32(by_source, own_pack[:, gate_weight.shape[0] + 1, : 4 * seqs])
+    route_rows = dot32(by_source, own_routes.astype(BF))
     route_lane = jnp.arange(4 * seqs)[None]
     class_routes = jnp.concatenate(
         [

time: 166 us -> 161 us (0.970)
  waiting for transfers between devices: 59.9 us -> 54.8 us
  other arithmetic: 12.4 us -> 14.8 us
    ppermute x6 -> x5, starting transfers between devices: 23.9 us -> 14.2 us  [from_other_core(): return lax.ppermute(shard, 'ep', [(i, i ^ 1) for i in range(n_ep)])]
    all_to_all x7 -> x8, starting transfers between devices: 46.2 us -> 55.3 us  [exchange(): lax.all_to_all(pieces, axis, split_axis=0, concat_axis=0, tiled=True, axi...]
    all_to_all x7 -> x8, waiting for transfers between devices: 58.3 us -> 54.8 us  [exchange(): lax.all_to_all(pieces, axis, split_axis=0, concat_axis=0, tiled=True, axi...]
    dot_general x12 -> x11, matrix products: 9.49 us -> 9.2 us  [dot32(): return jnp.dot(left, right, preferred_element_type=F32)]
where the time goes in v4:
time: 161 us; the launch traced here: 159 us
  starting transfers between devices  69.5 us (43%)
  waiting for transfers between devices  54.8 us (34%)
  other arithmetic  14.8 us (9%)
  matrix products  9.94 us (6%)
  local copies, waits for them, and re-layouts  8.18 us (5%)
  between operations  2.14 us (1%)
    all_to_all x8, starting transfers between devices, exchange(): lax.all_to_all(pieces, axis, split_axis=0, concat_axis=0, tiled=True, axi...  55.3 us
    all_to_all x8, waiting for transfers between devices, exchange(): lax.all_to_all(pieces, axis, split_axis=0, concat_axis=0, tiled=True, axi...  54.8 us
    ppermute x5, starting transfers between devices, from_other_core(): return lax.ppermute(shard, 'ep', [(i, i ^ 1) for i in range(n_ep)])  14.2 us
    dot_general x11, matrix products, dot32(): return jnp.dot(left, right, preferred_element_type=F32)  9.2 us
  transfers between devices with their start and end apart: 13, of which 7 were waited for; matrix products, arithmetic and copies ran while one was open for 13% of the time, Pallas kernels for 0%

profile of v4, /device:TPU:1, one launch (start us, length us, event | category | flops | bytes accessed | tf_op | source)
XLA Modules:
  0.0 159.4 jit_solution(7275826245721006210)
XLA Ops:
  0.7 1.0 fusion.18
  1.7 0.9 fusion.20
  2.7 0.2 reshape.437
  2.9 0.8 reshape.438
  3.7 10.1 %all-to-all-start = ((bf16[8,16,256]{2,1,0:T(8,128)(2,1)}), bf16[8,16,256]{2,1,0:T(8,128)(2,1)S(1)}, u32[]{:S(2)}, u32[]{:S(2)}) async-start(bf16[8,16,256]{2,1,0:T(8,128)(2,1)} %reshape.438), calls=%async_computation | async-start | bytes 131072 | tf_op jit(solution)/shard_map/all_to_all | solution.py:20
  13.8 0.9 pad_maximum_fusion.4
  14.6 2.0 %collective-permute-start = (bf16[128,448]{0,1:T(8,128)(2,1)S(1)}, bf16[128,448]{0,1:T(8,128)(2,1)S(1)}, u32[]{:S(2)}, u32[]{:S(2)}) collective-permute-start(bf16[128,448]{0,1:T(8,128)(2,1)S(1)} %pad_maximum_fusion.4), channel_id=1, source_target_pairs={{0,16},{16,0},{32,48},{48,32},{64,80},{80,64},{96,112},{112,96},{1... | collective-permute-start | bytes 344072 | tf_op jit(solution)/shard_map/ppermute | solution.py:84
  16.9 0.1 reduce-precision_reduce_fusion
  17.5 0.7 constant_dynamic-slice_fusion.2
  18.3 0.5 all-to-all-done
  18.9 0.7 broadcast_in_dim.246
  19.6 9.5 %all-to-all-start.1 = ((bf16[4,72,384]{2,1,0:T(8,128)(2,1)}), bf16[4,72,384]{2,1,0:T(8,128)(2,1)S(1)}, u32[]{:S(2)}, u32[]{:S(2)}) async-start(bf16[4,72,384]{2,1,0:T(8,128)(2,1)} %broadcast_in_dim.246), calls=%async_computation.1 | async-start | bytes 442368 | tf_op jit(solution)/shard_map/all_to_all | solution.py:20
  29.0 0.8 dynamic-slice_bitcast_fusion
  29.8 0.7 dynamic-slice_convert_fusion
  30.7 0.1 dot_general.50
  30.9 11.0 %all-to-all-done.1 = bf16[4,72,384]{2,1,0:T(8,128)(2,1)S(1)} async-done(((bf16[4,72,384]{2,1,0:T(8,128)(2,1)}), bf16[4,72,384]{2,1,0:T(8,128)(2,1)S(1)}, u32[]{:S(2)}, u32[]{:S(2)}) %all-to-all-start.1) | async-done | bytes 221216 | tf_op jit(solution)/shard_map/all_to_all | solution.py:20
  42.2 0.1 copy.84
  42.3 0.2 fusion.124
  42.5 0.8 pad_maximum_fusion.2
  43.3 10.1 %all-to-all-start.2 = ((f32[8,16,512]{2,1,0:T(8,128)}), f32[8,16,512]{2,1,0:T(8,128)S(1)}, u32[]{:S(2)}, u32[]{:S(2)}) async-start(f32[8,16,512]{2,1,0:T(8,128)} %pad_maximum_fusion.2), calls=%async_computation.2 | async-start | bytes 524288 | tf_op jit(solution)/shard_map/all_to_all | solution.py:20
  53.6 0.6 dynamic_slice.37
  54.2 0.6 dynamic_slice.38
  55.5 0.6 dynamic_slice.41
  56.2 0.3 concatenate.53
  56.4 5.7 %all-to-all-done.2 = f32[8,16,512]{2,1,0:T(8,128)S(1)} async-done(((f32[8,16,512]{2,1,0:T(8,128)}), f32[8,16,512]{2,1,0:T(8,128)S(1)}, u32[]{:S(2)}, u32[]{:S(2)}) %all-to-all-start.2) | async-done | bytes 262176 | tf_op jit(solution)/shard_map/all_to_all | solution.py:20
  62.2 0.8 fusion.81
  63.1 0.4 fusion.10
  63.6 0.8 multiply_reduce_fusion.4
  64.4 0.2 fusion.2
  64.7 0.7 pad_maximum_fusion.3
  65.3 6.8 %all-to-all-start.3 = ((bf16[16,32,128]{2,1,0:T(8,128)(2,1)}), bf16[16,32,128]{2,1,0:T(8,128)(2,1)S(1)}, u32[]{:S(2)}, u32[]{:S(2)}) async-start(bf16[16,32,128]{2,1,0:T(8,128)(2,1)} %pad_maximum_fusion.3), calls=%async_computation.3 | async-start | bytes 262144 | tf_op jit(solution)/shard_map/all_to_all | solution.py:20
  72.2 0.3 select_reduce_fusion
  72.5 6.5 %all-to-all-done.3 = bf16[16,32,128]{2,1,0:T(8,128)(2,1)S(1)} async-done(((bf16[16,32,128]{2,1,0:T(8,128)(2,1)}), bf16[16,32,128]{2,1,0:T(8,128)(2,1)S(1)}, u32[]{:S(2)}, u32[]{:S(2)}) %all-to-all-start.3) | async-done | bytes 131104 | tf_op jit(solution)/shard_map/all_to_all | solution.py:20
  79.0 0.7 multiply_convert_fusion.4
  79.7 0.6 broadcast_in_dim.252
  80.3 4.8 %all-to-all-start.4 = ((bf16[16,16,128]{2,1,0:T(8,128)(2,1)}), bf16[16,16,128]{2,1,0:T(8,128)(2,1)S(1)}, u32[]{:S(2)}, u32[]{:S(2)}) async-start(bf16[16,16,128]{2,1,0:T(8,128)(2,1)} %broadcast_in_dim.252), calls=%async_computation.4 | async-start | bytes 131072 | tf_op jit(solution)/shard_map/all_to_all | solution.py:20
  85.1 0.2 convolution_select_fusion.1
  85.3 11.3 %all-to-all-done.4 = bf16[16,16,128]{2,1,0:T(8,128)(2,1)S(1)} async-done(((bf16[16,16,128]{2,1,0:T(8,128)(2,1)}), bf16[16,16,128]{2,1,0:T(8,128)(2,1)S(1)}, u32[]{:S(2)}, u32[]{:S(2)}) %all-to-all-start.4) | async-done | bytes 65568 | tf_op jit(solution)/shard_map/all_to_all | solution.py:20
  96.9 0.3 fusion
  97.2 0.3 fusion.5
  97.6 0.9 pad_maximum_fusion
  98.5 3.7 %all-to-all-start.5 = ((bf16[16,24,1024]{2,1,0:T(8,128)(2,1)}), bf16[16,24,1024]{2,1,0:T(8,128)(2,1)S(1)}, u32[]{:S(2)}, u32[]{:S(2)}) async-start(bf16[16,24,1024]{2,1,0:T(8,128)(2,1)} %pad_maximum_fusion), calls=%async_computation.5 | async-start | bytes 1572864 | tf_op jit(solution)/shard_map/all_to_all | solution.py:20
  102.3 6.0 %collective-permute-start.2 = (bf16[2048,256]{1,0:T(8,128)(2,1)}, bf16[2048,256]{1,0:T(8,128)(2,1)}, u32[]{:S(2)}, u32[]{:S(2)}) collective-permute-start(bf16[2048,256]{1,0:T(8,128)(2,1)} %bitcast.174), channel_id=1, source_target_pairs={{0,16},{16,0},{32,48},{48,32},{64,80},{80,64},{96,112},{112,96},{1... | collective-permute-start | bytes 3145736 | tf_op jit(solution)/shard_map/ppermute | solution.py:84
  108.2 1.9 %collective-permute-start.1 = (bf16[2048,256]{1,0:T(8,128)(2,1)S(1)}, bf16[2048,256]{1,0:T(8,128)(2,1)}, u32[]{:S(2)}, u32[]{:S(2)}) collective-permute-start(bf16[2048,256]{1,0:T(8,128)(2,1)S(1)} %bitcast.171), channel_id=1, source_target_pairs={{0,16},{16,0},{32,48},{48,32},{64,80},{80,64},{96,112},{112,96},{1... | collective-permute-start | bytes 3145736 | tf_op jit(solution)/shard_map/ppermute | solution.py:84
  110.2 2.4 %collective-permute-start.3 = (bf16[256,2048]{1,0:T(8,128)(2,1)}, bf16[256,2048]{1,0:T(8,128)(2,1)}, u32[]{:S(2)}, u32[]{:S(2)}) collective-permute-start(bf16[256,2048]{1,0:T(8,128)(2,1)} %bitcast.175), channel_id=1, source_target_pairs={{0,16},{16,0},{32,48},{48,32},{64,80},{80,64},{96,112},{112,96},{1... | collective-permute-start | bytes 3145736 | tf_op jit(solution)/shard_map/ppermute | solution.py:84
  112.6 1.9 %collective-permute-start.4 = (bf16[224,128]{1,0:T(8,128)(2,1)}, bf16[224,128]{1,0:T(8,128)(2,1)}, u32[]{:S(2)}, u32[]{:S(2)}) collective-permute-start(bf16[224,128]{1,0:T(8,128)(2,1)} %param.53), channel_id=1, source_target_pairs={{0,16},{16,0},{32,48},{48,32},{64,80},{80,64},{96,112},{112,96},{1... | collective-permute-start | bytes 172040 | tf_op jit(solution)/shard_map/ppermute | solution.py:84
  114.6 0.3 fusion.88
  115.0 0.2 multiply_reduce_fusion
  115.4 0.2 fusion.79
  116.2 0.2 convolution_multiply_fusion.3
  116.5 1.5 convolution_multiply_fusion
  118.0 2.0 %convolution_convert_fusion.1 = bf16[32,2048]{1,0:T(8,128)(2,1)S(1)} fusion(bf16[4,8,16,128]{3,2,1,0:T(8,128)(2,1)S(1)} %copy.144, f32[32,256]{1,0:T(8,128)S(1)} %convolution_multiply_fusion.3, f32[32]{0:T(128)S(1)} %mul.373, bf16[1,256,2048]{2,1,0:T(8,128)(2,1)} %param.49, bf16[1,2048,256]{2,1,0:T(8,128)(2,1)S(1)} %copy-done.3), kind=kOutput, calls=%fused_computation.1 | convolution fusion | flops 67231744 | bytes 2392192 | tf_op jit(solution)/shard_map/dot_general | solution.py:35
  120.0 2.3 %convolution_convert_fusion = bf16[32,2048]{1,0:T(8,128)(2,1)S(1)} fusion(bf16[256,2048]{1,0:T(8,128)(2,1)} %collective-permute-done.3, f32[32,256]{1,0:T(8,128)S(1)} %convolution_multiply_fusion, bf16[2048,256]{1,0:T(8,128)(2,1)} %collective-permute-done.1, bf16[4,8,16,128]{3,2,1,0:T(8,128)(2,1)S(1)} %copy.143, f32[32]{0:T(128)S(1)} %mul.379), kind=kOutput, calls=%fused_computation | convolution fusion | flops 67231744 | bytes 2392192 | tf_op jit(solution)/shard_map/dot_general | solution.py:35
  122.4 0.8 pad_maximum_fusion.1
  123.2 6.9 %all-to-all-start.6 = ((bf16[16,128,128]{2,1,0:T(8,128)(2,1)}), bf16[16,128,128]{2,1,0:T(8,128)(2,1)S(1)}, u32[]{:S(2)}, u32[]{:S(2)}) async-start(bf16[16,128,128]{2,1,0:T(8,128)(2,1)} %pad_maximum_fusion.1), calls=%async_computation.6 | async-start | bytes 1048576 | tf_op jit(solution)/shard_map/all_to_all | solution.py:20
  130.1 0.6 fusion.66
  130.7 1.0 multiply_add_fusion
  131.7 9.0 %all-to-all-done.6 = bf16[16,128,128]{2,1,0:T(8,128)(2,1)S(1)} async-done(((bf16[16,128,128]{2,1,0:T(8,128)(2,1)}), bf16[16,128,128]{2,1,0:T(8,128)(2,1)S(1)}, u32[]{:S(2)}, u32[]{:S(2)}) %all-to-all-start.6) | async-done | bytes 524320 | tf_op jit(solution)/shard_map/all_to_all | solution.py:20
  140.8 0.3 fusion.60
  141.2 1.7 %fusion.1 = bf16[256,128]{1,0:T(8,128)(2,1)} fusion(f32[256,128]{1,0:T(8,128)S(1)} %fusion.60, bf16[32,8,4,128]{3,2,1,0:T(4,128)(2,1)S(1)} %bitcast.179, bf16[224,128]{1,0:T(8,128)(2,1)} %collective-permute-done.4, bf16[224,128]{1,0:T(8,128)(2,1)} %param.53), kind=kOutput, calls=%fused_computation.6 | convolution fusion | flops 34078720 | bytes 573440 | tf_op jit(solution)/shard_map/dot_general | solution.py:35
  142.9 3.5 %all-to-all-start.7 = ((bf16[16,16,128]{2,1,0:T(8,128)(2,1)}), bf16[16,16,128]{2,1,0:T(8,128)(2,1)S(1)}, u32[]{:S(2)}, u32[]{:S(2)}) async-start(bf16[16,16,128]{2,1,0:T(8,128)(2,1)} %bitcast.47), calls=%async_computation.7 | async-start | bytes 131072 | tf_op jit(solution)/shard_map/all_to_all | solution.py:20
  146.5 0.8 pad_maximum_fusion.5
  147.3 10.8 %all-to-all-done.7 = bf16[16,16,128]{2,1,0:T(8,128)(2,1)S(1)} async-done(((bf16[16,16,128]{2,1,0:T(8,128)(2,1)}), bf16[16,16,128]{2,1,0:T(8,128)(2,1)S(1)}, u32[]{:S(2)}, u32[]{:S(2)}) %all-to-all-start.7) | async-done | bytes 65568 | tf_op jit(solution)/shard_map/all_to_all | solution.py:20
  158.1 1.3 fusion.80
  (134 shorter events, 3.5 us)
Async XLA Ops:
  0.6 63.7 %copy-start = (bf16[64,2048]{1,0:T(8,128)(2,1)S(1)}, bf16[64,2048]{1,0:T(8,128)(2,1)}, u32[]{:S(2)}) copy-start(bf16[64,2048]{1,0:T(8,128)(2,1)} %param.43) | copy-start | bytes 786436
  0.6 16.1 %copy-start.13 = (f32[16,2]{0,1:T(2,128)S(1)}, f32[16,2]{0,1:T(2,128)}, u32[]{:S(2)}) copy-start(f32[16,2]{0,1:T(2,128)} %param.46) | copy-start | bytes 388
  0.7 16.3 %copy-start.14 = (s32[16,2]{0,1:T(2,128)S(1)}, s32[16,2]{0,1:T(2,128)}, u32[]{:S(2)}) copy-start(s32[16,2]{0,1:T(2,128)} %param.45) | copy-start | bytes 388
  0.7 16.4 %copy-start.11 = (bf16[64,16]{0,1:T(8,128)(2,1)S(1)}, bf16[64,16]{0,1:T(8,128)(2,1)}, u32[]{:S(2)}) copy-start(bf16[64,16]{0,1:T(8,128)(2,1)} %param.33) | copy-start | bytes 6148
  0.7 17.6 %copy-start.9 = (bf16[64,64]{1,0:T(8,128)(2,1)S(1)}, bf16[64,64]{1,0:T(8,128)(2,1)}, u32[]{:S(2)}) copy-start(bf16[64,64]{1,0:T(8,128)(2,1)} %param.29) | copy-start | bytes 24580
  0.7 17.6 %copy-start.8 = (bf16[64,64]{1,0:T(8,128)(2,1)S(1)}, bf16[64,64]{1,0:T(8,128)(2,1)}, u32[]{:S(2)}) copy-start(bf16[64,64]{1,0:T(8,128)(2,1)} %param.30) | copy-start | bytes 24580
  3.7 15.2 %all-to-all-start = ((bf16[8,16,256]{2,1,0:T(8,128)(2,1)}), bf16[8,16,256]{2,1,0:T(8,128)(2,1)S(1)}, u32[]{:S(2)}, u32[]{:S(2)}) async-start(bf16[8,16,256]{2,1,0:T(8,128)(2,1)} %reshape.438), calls=%async_computation | async-start | bytes 131072 | tf_op jit(solution)/shard_map/all_to_all | solution.py:20
  14.6 41.5 %collective-permute-start = (bf16[128,448]{0,1:T(8,128)(2,1)S(1)}, bf16[128,448]{0,1:T(8,128)(2,1)S(1)}, u32[]{:S(2)}, u32[]{:S(2)}) collective-permute-start(bf16[128,448]{0,1:T(8,128)(2,1)S(1)} %pad_maximum_fusion.4), channel_id=1, source_target_pairs={{0,16},{16,0},{32,48},{48,32},{64,80},{80,64},{96,112},{112,96},{1... | collective-permute-start | bytes 344072 | tf_op jit(solution)/shard_map/ppermute | solution.py:84
  19.6 22.4 %all-to-all-start.1 = ((bf16[4,72,384]{2,1,0:T(8,128)(2,1)}), bf16[4,72,384]{2,1,0:T(8,128)(2,1)S(1)}, u32[]{:S(2)}, u32[]{:S(2)}) async-start(bf16[4,72,384]{2,1,0:T(8,128)(2,1)} %broadcast_in_dim.246), calls=%async_computation.1 | async-start | bytes 442368 | tf_op jit(solution)/shard_map/all_to_all | solution.py:20
  30.7 22.8 %copy-start.4 = (bf16[16,2,3,512]{3,1,2,0:T(2,128)(2,1)S(1)}, bf16[16,2,3,512]{3,1,2,0:T(2,128)(2,1)}, u32[]{:S(2)}) copy-start(bf16[16,2,3,512]{3,1,2,0:T(2,128)(2,1)} %param.40) | copy-start | bytes 294916
  30.8 22.7 %copy-start.12 = (bf16[4,64]{1,0:T(4,128)(2,1)S(1)}, bf16[4,64]{1,0:T(4,128)(2,1)}, u32[]{:S(2)}) copy-start(bf16[4,64]{1,0:T(4,128)(2,1)} %param.37) | copy-start | bytes 1540
  30.9 22.7 %copy-start.16 = (f32[16]{0:T(128)S(1)}, f32[16]{0:T(128)}, u32[]{:S(2)}) copy-start(f32[16]{0:T(128)} %param.34) | copy-start | bytes 196
  30.9 23.3 %copy-start.17 = (f32[16]{0:T(128)S(1)}, f32[16]{0:T(128)}, u32[]{:S(2)}) copy-start(f32[16]{0:T(128)} %param.35) | copy-start | bytes 196
  30.9 24.6 %copy-start.18 = (f32[16]{0:T(128)S(1)}, f32[16]{0:T(128)}, u32[]{:S(2)}) copy-start(f32[16]{0:T(128)} %param.36) | copy-start | bytes 196
  30.9 25.1 %copy-start.10 = (f32[2048]{0:T(1024)S(1)}, f32[2048]{0:T(1024)}, u32[]{:S(2)}) copy-start(f32[2048]{0:T(1024)} %param.44) | copy-start | bytes 24580
  42.3 13.9 %copy-start.5 = (bf16[128,224]{0,1:T(8,128)(2,1)S(1)}, bf16[128,224]{0,1:T(8,128)(2,1)}, u32[]{:S(2)}) copy-start(bf16[128,224]{0,1:T(8,128)(2,1)} %param.51) | copy-start | bytes 172036
  42.3 13.9 %copy-start.6 = (bf16[128,224]{0,1:T(8,128)(2,1)S(1)}, bf16[128,224]{0,1:T(8,128)(2,1)}, u32[]{:S(2)}) copy-start(bf16[128,224]{0,1:T(8,128)(2,1)} %param.52) | copy-start | bytes 172036
  43.3 19.6 %copy-start.7 = (bf16[16,3,64]{2,0,1:T(8,128)(2,1)S(1)}, bf16[16,3,64]{2,0,1:T(8,128)(2,1)}, u32[]{:S(2)}) copy-start(bf16[16,3,64]{2,0,1:T(8,128)(2,1)} %param.39) | copy-start | bytes 18436
  43.3 19.8 %copy-start.1 = (f32[16,1,64,128]{3,2,1,0:T(8,128)S(1)}, f32[16,1,64,128]{3,2,1,0:T(8,128)}, u32[]{:S(2)}) copy-start(f32[16,1,64,128]{3,2,1,0:T(8,128)} %param.41) | copy-start | bytes 1572868
  43.3 18.8 %all-to-all-start.2 = ((f32[8,16,512]{2,1,0:T(8,128)}), f32[8,16,512]{2,1,0:T(8,128)S(1)}, u32[]{:S(2)}, u32[]{:S(2)}) async-start(f32[8,16,512]{2,1,0:T(8,128)} %pad_maximum_fusion.2), calls=%async_computation.2 | async-start | bytes 524288 | tf_op jit(solution)/shard_map/all_to_all | solution.py:20
  53.5 10.9 %copy-start.15 = (f32[64]{0:T(128)S(1)}, f32[64]{0:T(128)}, u32[]{:S(2)}) copy-start(f32[64]{0:T(128)} %param.42) | copy-start | bytes 772
  65.3 13.6 %all-to-all-start.3 = ((bf16[16,32,128]{2,1,0:T(8,128)(2,1)}), bf16[16,32,128]{2,1,0:T(8,128)(2,1)S(1)}, u32[]{:S(2)}, u32[]{:S(2)}) async-start(bf16[16,32,128]{2,1,0:T(8,128)(2,1)} %pad_maximum_fusion.3), calls=%async_computation.3 | async-start | bytes 262144 | tf_op jit(solution)/shard_map/all_to_all | solution.py:20
  80.3 16.4 %all-to-all-start.4 = ((bf16[16,16,128]{2,1,0:T(8,128)(2,1)}), bf16[16,16,128]{2,1,0:T(8,128)(2,1)S(1)}, u32[]{:S(2)}, u32[]{:S(2)}) async-start(bf16[16,16,128]{2,1,0:T(8,128)(2,1)} %broadcast_in_dim.252), calls=%async_computation.4 | async-start | bytes 131072 | tf_op jit(solution)/shard_map/all_to_all | solution.py:20
  98.5 9.7 %copy-start.2 = (bf16[1,2048,256]{2,1,0:T(8,128)(2,1)S(1)}, bf16[1,2048,256]{2,1,0:T(8,128)(2,1)}, u32[]{:S(2)}) copy-start(bf16[1,2048,256]{2,1,0:T(8,128)(2,1)} %param.47) | copy-start | bytes 3145732
  98.5 16.4 %all-to-all-start.5 = ((bf16[16,24,1024]{2,1,0:T(8,128)(2,1)}), bf16[16,24,1024]{2,1,0:T(8,128)(2,1)S(1)}, u32[]{:S(2)}, u32[]{:S(2)}) async-start(bf16[16,24,1024]{2,1,0:T(8,128)(2,1)} %pad_maximum_fusion), calls=%async_computation.5 | async-start | bytes 1572864 | tf_op jit(solution)/shard_map/all_to_all | solution.py:20
  102.3 14.2 %collective-permute-start.2 = (bf16[2048,256]{1,0:T(8,128)(2,1)}, bf16[2048,256]{1,0:T(8,128)(2,1)}, u32[]{:S(2)}, u32[]{:S(2)}) collective-permute-start(bf16[2048,256]{1,0:T(8,128)(2,1)} %bitcast.174), channel_id=1, source_target_pairs={{0,16},{16,0},{32,48},{48,32},{64,80},{80,64},{96,112},{112,96},{1... | collective-permute-start | bytes 3145736 | tf_op jit(solution)/shard_map/ppermute | solution.py:84
  108.2 11.7 %collective-permute-start.1 = (bf16[2048,256]{1,0:T(8,128)(2,1)S(1)}, bf16[2048,256]{1,0:T(8,128)(2,1)}, u32[]{:S(2)}, u32[]{:S(2)}) collective-permute-start(bf16[2048,256]{1,0:T(8,128)(2,1)S(1)} %bitcast.171), channel_id=1, source_target_pairs={{0,16},{16,0},{32,48},{48,32},{64,80},{80,64},{96,112},{112,96},{1... | collective-permute-start | bytes 3145736 | tf_op jit(solution)/shard_map/ppermute | solution.py:84
  110.2 9.8 %collective-permute-start.3 = (bf16[256,2048]{1,0:T(8,128)(2,1)}, bf16[256,2048]{1,0:T(8,128)(2,1)}, u32[]{:S(2)}, u32[]{:S(2)}) collective-permute-start(bf16[256,2048]{1,0:T(8,128)(2,1)} %bitcast.175), channel_id=1, source_target_pairs={{0,16},{16,0},{32,48},{48,32},{64,80},{80,64},{96,112},{112,96},{1... | collective-permute-start | bytes 3145736 | tf_op jit(solution)/shard_map/ppermute | solution.py:84
  112.6 28.6 %collective-permute-start.4 = (bf16[224,128]{1,0:T(8,128)(2,1)}, bf16[224,128]{1,0:T(8,128)(2,1)}, u32[]{:S(2)}, u32[]{:S(2)}) collective-permute-start(bf16[224,128]{1,0:T(8,128)(2,1)} %param.53), channel_id=1, source_target_pairs={{0,16},{16,0},{32,48},{48,32},{64,80},{80,64},{96,112},{112,96},{1... | collective-permute-start | bytes 172040 | tf_op jit(solution)/shard_map/ppermute | solution.py:84
  116.2 1.8 %copy-start.3 = (bf16[1,2048,256]{2,1,0:T(8,128)(2,1)S(1)}, bf16[1,2048,256]{2,1,0:T(8,128)(2,1)}, u32[]{:S(2)}) copy-start(bf16[1,2048,256]{2,1,0:T(8,128)(2,1)} %param.48) | copy-start | bytes 3145732
  123.2 17.5 %all-to-all-start.6 = ((bf16[16,128,128]{2,1,0:T(8,128)(2,1)}), bf16[16,128,128]{2,1,0:T(8,128)(2,1)S(1)}, u32[]{:S(2)}, u32[]{:S(2)}) async-start(bf16[16,128,128]{2,1,0:T(8,128)(2,1)} %pad_maximum_fusion.1), calls=%async_computation.6 | async-start | bytes 1048576 | tf_op jit(solution)/shard_map/all_to_all | solution.py:20
  141.1 5.4 %slice-start = ((bf16[16,2,3,512]{3,1,2,0:T(2,128)(2,1)}), bf16[16,2,2,512]{3,1,2,0:T(2,128)(2,1)S(1)}, s32[]{:S(2)}) async-start(bf16[16,2,3,512]{3,1,2,0:T(2,128)(2,1)} %param.40), calls=%async_computation.8 | async-start | bytes 131072 | tf_op jit(solution)/shard_map/slice | solution.py:219
  142.9 15.1 %all-to-all-start.7 = ((bf16[16,16,128]{2,1,0:T(8,128)(2,1)}), bf16[16,16,128]{2,1,0:T(8,128)(2,1)S(1)}, u32[]{:S(2)}, u32[]{:S(2)}) async-start(bf16[16,16,128]{2,1,0:T(8,128)(2,1)} %bitcast.47), calls=%async_computation.7 | async-start | bytes 131072 | tf_op jit(solution)/shard_map/all_to_all | solution.py:20

commit v5 on v4

--- a/solution.py
+++ b/solution.py
@@ -84,7 +84,7 @@
         return lax.ppermute(shard, "ep", [(i, i ^ 1) for i in range(n_ep)])
 
     per_class = n_ep // CLASSES
-    same_class = [[CLASSES * j + r for j in range(per_class)] for r in range(CLASSES)]
+    first_class = ep // CLASSES
     near = [[CLASSES * j + r for r in range(CLASSES)] for j in range(per_class)]
 
     write_own = slice_at(write_weight, group * STATE, STATE, 1)
@@ -114,10 +114,17 @@
     extra = jnp.concatenate([step_row, route_row, jnp.zeros((6, rows_k), BF)], axis=0)
     extra = jnp.pad(extra, ((0, 0), (0, pack_cols - rows_k)))
     pack = jnp.concatenate([main, extra], axis=0)
-    class_pack = exchange(to_everyone(pack, per_class), "ep", same_class)
+    class_pack = [pack]
+    for ahead in range(1, per_class):
+        hops = [(i, (i - CLASSES * ahead) % n_ep) for i in range(n_ep)]
+        class_pack.append(lax.ppermute(pack, "ep", hops))
+    class_pack = jnp.stack(class_pack)
 
     normed = rms_scale(tokens.astype(F32), mix_gain).astype(BF)
-    keys = normed.reshape(seqs, per_class, CLASSES, rows_k).transpose(2, 0, 1, 3)
+    rotated = slice_at(
+        jnp.concatenate([normed, normed], axis=1), first_class * CLASSES * rows_k, width, 1
+    )
+    keys = rotated.reshape(seqs, per_class, CLASSES, rows_k).transpose(2, 0, 1, 3)
     keys = exchange(keys.reshape(CLASSES, seqs, per_class * rows_k), "ep", near)
     keys = keys.reshape(CLASSES * seqs, per_class, rows_k)
     padded = jnp.pad(keys, ((0, 0), (0, 0), (0, pack.shape[0] - rows_k)))
@@ -184,7 +191,8 @@
 
     total = chips * seqs
     at = jnp.arange(total)[:, None]
-    by_source = (at // seqs == jnp.arange(chips)[None]).astype(BF)
+    source = (jnp.arange(chips)[None] + first_class * (CLASSES // CORES)) % chips
+    by_source = (at // seqs == source).astype(BF)
     route_rows = dot32(by_source, own_routes.astype(BF))
     route_lane = jnp.arange(4 * seqs)[None]
     class_routes = jnp.concatenate(

time: 161 us -> 157 us (0.975)
  waiting for transfers between devices: 54.8 us -> 44.4 us
  starting transfers between devices: 69.5 us -> 73.7 us
    ppermute x0 -> x3, starting transfers between devices: none -> 25.5 us  [local(): class_pack.append(lax.ppermute(pack, 'ep', hops))]
    all_to_all x8 -> x7, starting transfers between devices: 55.3 us -> 34.7 us  [exchange(): lax.all_to_all(pieces, axis, split_axis=0, concat_axis=0, tiled=True, axi...]
    all_to_all x8 -> x7, waiting for transfers between devices: 54.8 us -> 44.4 us  [exchange(): lax.all_to_all(pieces, axis, split_axis=0, concat_axis=0, tiled=True, axi...]
  transfers between devices with their start and end apart: 13 -> 15, of which waited for: 7 -> 6; matrix products, arithmetic and copies ran while one was open for 13% -> 13% of each run, Pallas kernels for 0% -> 0%
where the time goes in v5:
time: 157 us; the launch traced here: 155 us
  starting transfers between devices  73.7 us (47%)
  waiting for transfers between devices  44.4 us (28%)
  other arithmetic  15.7 us (10%)
  matrix products  10.6 us (7%)
  local copies, waits for them, and re-layouts  8.22 us (5%)
  between operations  2.2 us (1%)
    all_to_all x7, waiting for transfers between devices, exchange(): lax.all_to_all(pieces, axis, split_axis=0, concat_axis=0, tiled=True, axi...  44.4 us
    all_to_all x7, starting transfers between devices, exchange(): lax.all_to_all(pieces, axis, split_axis=0, concat_axis=0, tiled=True, axi...  34.7 us
    ppermute x3, starting transfers between devices, local(): class_pack.append(lax.ppermute(pack, 'ep', hops))  25.5 us
    ppermute x5, starting transfers between devices, from_other_core(): return lax.ppermute(shard, 'ep', [(i, i ^ 1) for i in range(n_ep)])  13.6 us
    dot_general x11, matrix products, dot32(): return jnp.dot(left, right, preferred_element_type=F32)  9.2 us
  transfers between devices with their start and end apart: 15, of which 6 were waited for; matrix products, arithmetic and copies ran while one was open for 13% of the time, Pallas kernels for 0%

profile of v5, /device:TPU:1, one launch (start us, length us, event | category | flops | bytes accessed | tf_op | source)
XLA Modules:
  0.0 154.8 jit_solution(5269077383501033319)
XLA Ops:
  0.8 0.8 fusion.127
  1.7 0.8 convert_bitcast_fusion.2
  2.4 0.8 fusion.7
  3.5 0.7 constant_dynamic-slice_fusion.2
  4.4 0.8 fusion.47
  5.2 9.6 %collective-permute-start.2 = (bf16[72,384]{1,0:T(8,128)(2,1)S(1)}, bf16[72,384]{1,0:T(8,128)(2,1)S(1)}, u32[]{:S(2)}, u32[]{:S(2)}) collective-permute-start(bf16[72,384]{1,0:T(8,128)(2,1)S(1)} %fusion.47), channel_id=1, source_target_pairs={{0,128},{16,144},{32,160},{48,176},{64,192},{80,208},{96,224},{112... | collective-permute-start | bytes 165896 | tf_op jit(solution)/shard_map/ppermute | solution.py:120
  14.8 5.6 %collective-permute-start = (bf16[72,384]{1,0:T(8,128)(2,1)S(1)}, bf16[72,384]{1,0:T(8,128)(2,1)S(1)}, u32[]{:S(2)}, u32[]{:S(2)}) collective-permute-start(bf16[72,384]{1,0:T(8,128)(2,1)S(1)} %fusion.47), channel_id=1, source_target_pairs={{0,384},{16,400},{32,416},{48,432},{64,448},{80,464},{96,480},{112... | collective-permute-start | bytes 165896 | tf_op jit(solution)/shard_map/ppermute | solution.py:120
  20.4 10.3 %collective-permute-start.1 = (bf16[72,384]{1,0:T(8,128)(2,1)S(1)}, bf16[72,384]{1,0:T(8,128)(2,1)S(1)}, u32[]{:S(2)}, u32[]{:S(2)}) collective-permute-start(bf16[72,384]{1,0:T(8,128)(2,1)S(1)} %fusion.47), channel_id=1, source_target_pairs={{0,256},{16,272},{32,288},{48,304},{64,320},{80,336},{96,352},{112... | collective-permute-start | bytes 165896 | tf_op jit(solution)/shard_map/ppermute | solution.py:120
  30.7 1.0 fusion.18
  31.7 0.9 fusion.20
  32.7 0.2 reshape.458
  33.0 0.8 reshape.459
  33.7 4.8 %all-to-all-start = ((bf16[8,16,256]{2,1,0:T(8,128)(2,1)}), bf16[8,16,256]{2,1,0:T(8,128)(2,1)S(1)}, u32[]{:S(2)}, u32[]{:S(2)}) async-start(bf16[8,16,256]{2,1,0:T(8,128)(2,1)} %reshape.459), calls=%async_computation | async-start | bytes 131072 | tf_op jit(solution)/shard_map/all_to_all | solution.py:20
  38.5 2.0 %collective-permute-start.3 = (bf16[128,448]{0,1:T(8,128)(2,1)S(1)}, bf16[128,448]{0,1:T(8,128)(2,1)S(1)}, u32[]{:S(2)}, u32[]{:S(2)}) collective-permute-start(bf16[128,448]{0,1:T(8,128)(2,1)S(1)} %pad_maximum_fusion.5), channel_id=1, source_target_pairs={{0,16},{16,0},{32,48},{48,32},{64,80},{80,64},{96,112},{112,96},{1... | collective-permute-start | bytes 344072 | tf_op jit(solution)/shard_map/ppermute | solution.py:84
  40.7 0.7 dynamic-slice_convert_fusion
  41.4 0.8 dynamic-slice_bitcast_fusion
  42.5 1.1 all-to-all-done
  44.2 0.2 fusion.128
  44.5 0.8 pad_maximum_fusion.2
  45.3 4.3 %all-to-all-start.1 = ((f32[8,16,512]{2,1,0:T(8,128)}), f32[8,16,512]{2,1,0:T(8,128)S(1)}, u32[]{:S(2)}, u32[]{:S(2)}) async-start(f32[8,16,512]{2,1,0:T(8,128)} %pad_maximum_fusion.2), calls=%async_computation.1 | async-start | bytes 524288 | tf_op jit(solution)/shard_map/all_to_all | solution.py:20
  49.7 0.6 dynamic_slice.41
  50.3 0.6 dynamic_slice.42
  51.6 0.6 dynamic_slice.45
  52.3 0.3 concatenate.57
  52.6 5.7 %all-to-all-done.1 = f32[8,16,512]{2,1,0:T(8,128)S(1)} async-done(((f32[8,16,512]{2,1,0:T(8,128)}), f32[8,16,512]{2,1,0:T(8,128)S(1)}, u32[]{:S(2)}, u32[]{:S(2)}) %all-to-all-start.1) | async-done | bytes 262176 | tf_op jit(solution)/shard_map/all_to_all | solution.py:20
  58.4 0.8 fusion.84
  59.3 0.4 fusion.10
  59.8 0.8 multiply_reduce_fusion.4
  60.6 0.2 fusion.2
  60.8 0.7 pad_maximum_fusion.4
  61.5 6.8 %all-to-all-start.2 = ((bf16[16,32,128]{2,1,0:T(8,128)(2,1)}), bf16[16,32,128]{2,1,0:T(8,128)(2,1)S(1)}, u32[]{:S(2)}, u32[]{:S(2)}) async-start(bf16[16,32,128]{2,1,0:T(8,128)(2,1)} %pad_maximum_fusion.4), calls=%async_computation.2 | async-start | bytes 262144 | tf_op jit(solution)/shard_map/all_to_all | solution.py:20
  68.4 0.3 select_reduce_fusion
  68.6 6.5 %all-to-all-done.2 = bf16[16,32,128]{2,1,0:T(8,128)(2,1)S(1)} async-done(((bf16[16,32,128]{2,1,0:T(8,128)(2,1)}), bf16[16,32,128]{2,1,0:T(8,128)(2,1)S(1)}, u32[]{:S(2)}, u32[]{:S(2)}) %all-to-all-start.2) | async-done | bytes 131104 | tf_op jit(solution)/shard_map/all_to_all | solution.py:20
  75.1 0.7 multiply_convert_fusion.4
  75.8 0.6 broadcast_in_dim.245
  76.5 4.8 %all-to-all-start.3 = ((bf16[16,16,128]{2,1,0:T(8,128)(2,1)}), bf16[16,16,128]{2,1,0:T(8,128)(2,1)S(1)}, u32[]{:S(2)}, u32[]{:S(2)}) async-start(bf16[16,16,128]{2,1,0:T(8,128)(2,1)} %broadcast_in_dim.245), calls=%async_computation.3 | async-start | bytes 131072 | tf_op jit(solution)/shard_map/all_to_all | solution.py:20
  81.2 0.2 convolution_select_fusion.1
  81.5 11.3 %all-to-all-done.3 = bf16[16,16,128]{2,1,0:T(8,128)(2,1)S(1)} async-done(((bf16[16,16,128]{2,1,0:T(8,128)(2,1)}), bf16[16,16,128]{2,1,0:T(8,128)(2,1)S(1)}, u32[]{:S(2)}, u32[]{:S(2)}) %all-to-all-start.3) | async-done | bytes 65568 | tf_op jit(solution)/shard_map/all_to_all | solution.py:20
  93.0 0.3 fusion
  93.4 0.3 fusion.5
  93.7 0.9 pad_maximum_fusion
  94.7 3.7 %all-to-all-start.4 = ((bf16[16,24,1024]{2,1,0:T(8,128)(2,1)}), bf16[16,24,1024]{2,1,0:T(8,128)(2,1)S(1)}, u32[]{:S(2)}, u32[]{:S(2)}) async-start(bf16[16,24,1024]{2,1,0:T(8,128)(2,1)} %pad_maximum_fusion), calls=%async_computation.4 | async-start | bytes 1572864 | tf_op jit(solution)/shard_map/all_to_all | solution.py:20
  98.4 5.3 %collective-permute-start.5 = (bf16[2048,256]{1,0:T(8,128)(2,1)}, bf16[2048,256]{1,0:T(8,128)(2,1)}, u32[]{:S(2)}, u32[]{:S(2)}) collective-permute-start(bf16[2048,256]{1,0:T(8,128)(2,1)} %bitcast.177), channel_id=1, source_target_pairs={{0,16},{16,0},{32,48},{48,32},{64,80},{80,64},{96,112},{112,96},{1... | collective-permute-start | bytes 3145736 | tf_op jit(solution)/shard_map/ppermute | solution.py:84
  103.7 1.9 %collective-permute-start.4 = (bf16[2048,256]{1,0:T(8,128)(2,1)S(1)}, bf16[2048,256]{1,0:T(8,128)(2,1)}, u32[]{:S(2)}, u32[]{:S(2)}) collective-permute-start(bf16[2048,256]{1,0:T(8,128)(2,1)S(1)} %bitcast.174), channel_id=1, source_target_pairs={{0,16},{16,0},{32,48},{48,32},{64,80},{80,64},{96,112},{112,96},{1... | collective-permute-start | bytes 3145736 | tf_op jit(solution)/shard_map/ppermute | solution.py:84
  105.6 2.4 %collective-permute-start.6 = (bf16[256,2048]{1,0:T(8,128)(2,1)}, bf16[256,2048]{1,0:T(8,128)(2,1)}, u32[]{:S(2)}, u32[]{:S(2)}) collective-permute-start(bf16[256,2048]{1,0:T(8,128)(2,1)} %bitcast.178), channel_id=1, source_target_pairs={{0,16},{16,0},{32,48},{48,32},{64,80},{80,64},{96,112},{112,96},{1... | collective-permute-start | bytes 3145736 | tf_op jit(solution)/shard_map/ppermute | solution.py:84
  108.1 1.9 %collective-permute-start.7 = (bf16[224,128]{1,0:T(8,128)(2,1)}, bf16[224,128]{1,0:T(8,128)(2,1)}, u32[]{:S(2)}, u32[]{:S(2)}) collective-permute-start(bf16[224,128]{1,0:T(8,128)(2,1)} %param.53), channel_id=1, source_target_pairs={{0,16},{16,0},{32,48},{48,32},{64,80},{80,64},{96,112},{112,96},{1... | collective-permute-start | bytes 172040 | tf_op jit(solution)/shard_map/ppermute | solution.py:84
  110.1 0.3 fusion.91
  110.4 0.2 multiply_reduce_fusion
  110.9 0.2 fusion.82
  111.7 0.2 convolution_multiply_fusion.3
  111.9 1.5 convolution_multiply_fusion
  113.5 2.0 %convolution_convert_fusion.1 = bf16[32,2048]{1,0:T(8,128)(2,1)S(1)} fusion(bf16[4,8,16,128]{3,2,1,0:T(8,128)(2,1)S(1)} %copy.140, f32[32,256]{1,0:T(8,128)S(1)} %convolution_multiply_fusion.3, f32[32]{0:T(128)S(1)} %mul.382, bf16[1,256,2048]{2,1,0:T(8,128)(2,1)} %param.49, bf16[1,2048,256]{2,1,0:T(8,128)(2,1)S(1)} %copy-done.3), kind=kOutput, calls=%fused_computation.1 | convolution fusion | flops 67231744 | bytes 2392192 | tf_op jit(solution)/shard_map/dot_general | solution.py:35
  115.5 2.3 %convolution_convert_fusion = bf16[32,2048]{1,0:T(8,128)(2,1)S(1)} fusion(bf16[256,2048]{1,0:T(8,128)(2,1)} %collective-permute-done.6, f32[32,256]{1,0:T(8,128)S(1)} %convolution_multiply_fusion, bf16[2048,256]{1,0:T(8,128)(2,1)} %collective-permute-done.4, bf16[4,8,16,128]{3,2,1,0:T(8,128)(2,1)S(1)} %copy.139, f32[32]{0:T(128)S(1)} %mul.388), kind=kOutput, calls=%fused_computation | convolution fusion | flops 67231744 | bytes 2392192 | tf_op jit(solution)/shard_map/dot_general | solution.py:35
  117.9 0.8 pad_maximum_fusion.1
  118.7 6.9 %all-to-all-start.5 = ((bf16[16,128,128]{2,1,0:T(8,128)(2,1)}), bf16[16,128,128]{2,1,0:T(8,128)(2,1)S(1)}, u32[]{:S(2)}, u32[]{:S(2)}) async-start(bf16[16,128,128]{2,1,0:T(8,128)(2,1)} %pad_maximum_fusion.1), calls=%async_computation.5 | async-start | bytes 1048576 | tf_op jit(solution)/shard_map/all_to_all | solution.py:20
  125.6 0.6 fusion.69
  126.2 1.0 multiply_add_fusion
  127.2 9.0 %all-to-all-done.5 = bf16[16,128,128]{2,1,0:T(8,128)(2,1)S(1)} async-done(((bf16[16,128,128]{2,1,0:T(8,128)(2,1)}), bf16[16,128,128]{2,1,0:T(8,128)(2,1)S(1)}, u32[]{:S(2)}, u32[]{:S(2)}) %all-to-all-start.5) | async-done | bytes 524320 | tf_op jit(solution)/shard_map/all_to_all | solution.py:20
  136.2 0.3 fusion.63
  136.7 1.7 %fusion.1 = bf16[256,128]{1,0:T(8,128)(2,1)} fusion(f32[256,128]{1,0:T(8,128)S(1)} %fusion.63, bf16[32,8,4,128]{3,2,1,0:T(4,128)(2,1)S(1)} %bitcast.182, bf16[224,128]{1,0:T(8,128)(2,1)} %collective-permute-done.7, bf16[224,128]{1,0:T(8,128)(2,1)} %param.53), kind=kOutput, calls=%fused_computation.6 | convolution fusion | flops 34078720 | bytes 573440 | tf_op jit(solution)/shard_map/dot_general | solution.py:35
  138.4 3.5 %all-to-all-start.6 = ((bf16[16,16,128]{2,1,0:T(8,128)(2,1)}), bf16[16,16,128]{2,1,0:T(8,128)(2,1)S(1)}, u32[]{:S(2)}, u32[]{:S(2)}) async-start(bf16[16,16,128]{2,1,0:T(8,128)(2,1)} %bitcast.51), calls=%async_computation.6 | async-start | bytes 131072 | tf_op jit(solution)/shard_map/all_to_all | solution.py:20
  142.0 0.8 pad_maximum_fusion.6
  142.7 10.8 %all-to-all-done.6 = bf16[16,16,128]{2,1,0:T(8,128)(2,1)S(1)} async-done(((bf16[16,16,128]{2,1,0:T(8,128)(2,1)}), bf16[16,16,128]{2,1,0:T(8,128)(2,1)S(1)}, u32[]{:S(2)}, u32[]{:S(2)}) %all-to-all-start.6) | async-done | bytes 65568 | tf_op jit(solution)/shard_map/all_to_all | solution.py:20
  153.6 1.3 fusion.83
  (135 shorter events, 3.9 us)
Async XLA Ops:
  0.6 59.9 %copy-start = (bf16[64,2048]{1,0:T(8,128)(2,1)S(1)}, bf16[64,2048]{1,0:T(8,128)(2,1)}, u32[]{:S(2)}) copy-start(bf16[64,2048]{1,0:T(8,128)(2,1)} %param.43) | copy-start | bytes 786436
  0.6 39.9 %copy-start.8 = (bf16[64,64]{1,0:T(8,128)(2,1)S(1)}, bf16[64,64]{1,0:T(8,128)(2,1)}, u32[]{:S(2)}) copy-start(bf16[64,64]{1,0:T(8,128)(2,1)} %param.29) | copy-start | bytes 24580
  0.7 39.9 %copy-start.7 = (bf16[64,64]{1,0:T(8,128)(2,1)S(1)}, bf16[64,64]{1,0:T(8,128)(2,1)}, u32[]{:S(2)}) copy-start(bf16[64,64]{1,0:T(8,128)(2,1)} %param.30) | copy-start | bytes 24580
  0.7 37.8 %copy-start.5 = (bf16[128,224]{0,1:T(8,128)(2,1)S(1)}, bf16[128,224]{0,1:T(8,128)(2,1)}, u32[]{:S(2)}) copy-start(bf16[128,224]{0,1:T(8,128)(2,1)} %param.51) | copy-start | bytes 172036
  0.7 37.8 %copy-start.6 = (bf16[128,224]{0,1:T(8,128)(2,1)S(1)}, bf16[128,224]{0,1:T(8,128)(2,1)}, u32[]{:S(2)}) copy-start(bf16[128,224]{0,1:T(8,128)(2,1)} %param.52) | copy-start | bytes 172036
  5.2 37.1 %collective-permute-start.2 = (bf16[72,384]{1,0:T(8,128)(2,1)S(1)}, bf16[72,384]{1,0:T(8,128)(2,1)S(1)}, u32[]{:S(2)}, u32[]{:S(2)}) collective-permute-start(bf16[72,384]{1,0:T(8,128)(2,1)S(1)} %fusion.47), channel_id=1, source_target_pairs={{0,128},{16,144},{32,160},{48,176},{64,192},{80,208},{96,224},{112... | collective-permute-start | bytes 165896 | tf_op jit(solution)/shard_map/ppermute | solution.py:120
  14.8 27.5 %collective-permute-start = (bf16[72,384]{1,0:T(8,128)(2,1)S(1)}, bf16[72,384]{1,0:T(8,128)(2,1)S(1)}, u32[]{:S(2)}, u32[]{:S(2)}) collective-permute-start(bf16[72,384]{1,0:T(8,128)(2,1)S(1)} %fusion.47), channel_id=1, source_target_pairs={{0,384},{16,400},{32,416},{48,432},{64,448},{80,464},{96,480},{112... | collective-permute-start | bytes 165896 | tf_op jit(solution)/shard_map/ppermute | solution.py:120
  20.4 21.9 %collective-permute-start.1 = (bf16[72,384]{1,0:T(8,128)(2,1)S(1)}, bf16[72,384]{1,0:T(8,128)(2,1)S(1)}, u32[]{:S(2)}, u32[]{:S(2)}) collective-permute-start(bf16[72,384]{1,0:T(8,128)(2,1)S(1)} %fusion.47), channel_id=1, source_target_pairs={{0,256},{16,272},{32,288},{48,304},{64,320},{80,336},{96,352},{112... | collective-permute-start | bytes 165896 | tf_op jit(solution)/shard_map/ppermute | solution.py:120
  33.7 9.9 %all-to-all-start = ((bf16[8,16,256]{2,1,0:T(8,128)(2,1)}), bf16[8,16,256]{2,1,0:T(8,128)(2,1)S(1)}, u32[]{:S(2)}, u32[]{:S(2)}) async-start(bf16[8,16,256]{2,1,0:T(8,128)(2,1)} %reshape.459), calls=%async_computation | async-start | bytes 131072 | tf_op jit(solution)/shard_map/all_to_all | solution.py:20
  38.5 13.8 %collective-permute-start.3 = (bf16[128,448]{0,1:T(8,128)(2,1)S(1)}, bf16[128,448]{0,1:T(8,128)(2,1)S(1)}, u32[]{:S(2)}, u32[]{:S(2)}) collective-permute-start(bf16[128,448]{0,1:T(8,128)(2,1)S(1)} %pad_maximum_fusion.5), channel_id=1, source_target_pairs={{0,16},{16,0},{32,48},{48,32},{64,80},{80,64},{96,112},{112,96},{1... | collective-permute-start | bytes 344072 | tf_op jit(solution)/shard_map/ppermute | solution.py:84
  43.8 5.8 %copy-start.4 = (bf16[16,2,3,512]{3,1,2,0:T(2,128)(2,1)S(1)}, bf16[16,2,3,512]{3,1,2,0:T(2,128)(2,1)}, u32[]{:S(2)}) copy-start(bf16[16,2,3,512]{3,1,2,0:T(2,128)(2,1)} %param.40) | copy-start | bytes 294916
  44.0 5.8 %copy-start.11 = (bf16[4,64]{1,0:T(4,128)(2,1)S(1)}, bf16[4,64]{1,0:T(4,128)(2,1)}, u32[]{:S(2)}) copy-start(bf16[4,64]{1,0:T(4,128)(2,1)} %param.37) | copy-start | bytes 1540
  44.0 5.8 %copy-start.13 = (f32[16]{0:T(128)S(1)}, f32[16]{0:T(128)}, u32[]{:S(2)}) copy-start(f32[16]{0:T(128)} %param.34) | copy-start | bytes 196
  44.0 6.3 %copy-start.14 = (f32[16]{0:T(128)S(1)}, f32[16]{0:T(128)}, u32[]{:S(2)}) copy-start(f32[16]{0:T(128)} %param.35) | copy-start | bytes 196
  44.0 7.6 %copy-start.15 = (f32[16]{0:T(128)S(1)}, f32[16]{0:T(128)}, u32[]{:S(2)}) copy-start(f32[16]{0:T(128)} %param.36) | copy-start | bytes 196
  44.0 8.2 %copy-start.10 = (f32[2048]{0:T(1024)S(1)}, f32[2048]{0:T(1024)}, u32[]{:S(2)}) copy-start(f32[2048]{0:T(1024)} %param.44) | copy-start | bytes 24580
  45.3 13.9 %copy-start.9 = (bf16[16,3,64]{2,0,1:T(8,128)(2,1)S(1)}, bf16[16,3,64]{2,0,1:T(8,128)(2,1)}, u32[]{:S(2)}) copy-start(bf16[16,3,64]{2,0,1:T(8,128)(2,1)} %param.39) | copy-start | bytes 18436
  45.3 14.0 %copy-start.1 = (f32[16,1,64,128]{3,2,1,0:T(8,128)S(1)}, f32[16,1,64,128]{3,2,1,0:T(8,128)}, u32[]{:S(2)}) copy-start(f32[16,1,64,128]{3,2,1,0:T(8,128)} %param.41) | copy-start | bytes 1572868
  45.3 13.0 %all-to-all-start.1 = ((f32[8,16,512]{2,1,0:T(8,128)}), f32[8,16,512]{2,1,0:T(8,128)S(1)}, u32[]{:S(2)}, u32[]{:S(2)}) async-start(f32[8,16,512]{2,1,0:T(8,128)} %pad_maximum_fusion.2), calls=%async_computation.1 | async-start | bytes 524288 | tf_op jit(solution)/shard_map/all_to_all | solution.py:20
  49.6 10.9 %copy-start.12 = (f32[64]{0:T(128)S(1)}, f32[64]{0:T(128)}, u32[]{:S(2)}) copy-start(f32[64]{0:T(128)} %param.42) | copy-start | bytes 772
  61.5 13.6 %all-to-all-start.2 = ((bf16[16,32,128]{2,1,0:T(8,128)(2,1)}), bf16[16,32,128]{2,1,0:T(8,128)(2,1)S(1)}, u32[]{:S(2)}, u32[]{:S(2)}) async-start(bf16[16,32,128]{2,1,0:T(8,128)(2,1)} %pad_maximum_fusion.4), calls=%async_computation.2 | async-start | bytes 262144 | tf_op jit(solution)/shard_map/all_to_all | solution.py:20
  76.5 16.4 %all-to-all-start.3 = ((bf16[16,16,128]{2,1,0:T(8,128)(2,1)}), bf16[16,16,128]{2,1,0:T(8,128)(2,1)S(1)}, u32[]{:S(2)}, u32[]{:S(2)}) async-start(bf16[16,16,128]{2,1,0:T(8,128)(2,1)} %broadcast_in_dim.245), calls=%async_computation.3 | async-start | bytes 131072 | tf_op jit(solution)/shard_map/all_to_all | solution.py:20
  94.7 9.0 %copy-start.2 = (bf16[1,2048,256]{2,1,0:T(8,128)(2,1)S(1)}, bf16[1,2048,256]{2,1,0:T(8,128)(2,1)}, u32[]{:S(2)}) copy-start(bf16[1,2048,256]{2,1,0:T(8,128)(2,1)} %param.47) | copy-start | bytes 3145732
  94.7 15.7 %all-to-all-start.4 = ((bf16[16,24,1024]{2,1,0:T(8,128)(2,1)}), bf16[16,24,1024]{2,1,0:T(8,128)(2,1)S(1)}, u32[]{:S(2)}, u32[]{:S(2)}) async-start(bf16[16,24,1024]{2,1,0:T(8,128)(2,1)} %pad_maximum_fusion), calls=%async_computation.4 | async-start | bytes 1572864 | tf_op jit(solution)/shard_map/all_to_all | solution.py:20
  98.4 13.5 %collective-permute-start.5 = (bf16[2048,256]{1,0:T(8,128)(2,1)}, bf16[2048,256]{1,0:T(8,128)(2,1)}, u32[]{:S(2)}, u32[]{:S(2)}) collective-permute-start(bf16[2048,256]{1,0:T(8,128)(2,1)} %bitcast.177), channel_id=1, source_target_pairs={{0,16},{16,0},{32,48},{48,32},{64,80},{80,64},{96,112},{112,96},{1... | collective-permute-start | bytes 3145736 | tf_op jit(solution)/shard_map/ppermute | solution.py:84
  103.7 11.7 %collective-permute-start.4 = (bf16[2048,256]{1,0:T(8,128)(2,1)S(1)}, bf16[2048,256]{1,0:T(8,128)(2,1)}, u32[]{:S(2)}, u32[]{:S(2)}) collective-permute-start(bf16[2048,256]{1,0:T(8,128)(2,1)S(1)} %bitcast.174), channel_id=1, source_target_pairs={{0,16},{16,0},{32,48},{48,32},{64,80},{80,64},{96,112},{112,96},{1... | collective-permute-start | bytes 3145736 | tf_op jit(solution)/shard_map/ppermute | solution.py:84
  105.6 9.8 %collective-permute-start.6 = (bf16[256,2048]{1,0:T(8,128)(2,1)}, bf16[256,2048]{1,0:T(8,128)(2,1)}, u32[]{:S(2)}, u32[]{:S(2)}) collective-permute-start(bf16[256,2048]{1,0:T(8,128)(2,1)} %bitcast.178), channel_id=1, source_target_pairs={{0,16},{16,0},{32,48},{48,32},{64,80},{80,64},{96,112},{112,96},{1... | collective-permute-start | bytes 3145736 | tf_op jit(solution)/shard_map/ppermute | solution.py:84
  108.1 28.6 %collective-permute-start.7 = (bf16[224,128]{1,0:T(8,128)(2,1)}, bf16[224,128]{1,0:T(8,128)(2,1)}, u32[]{:S(2)}, u32[]{:S(2)}) collective-permute-start(bf16[224,128]{1,0:T(8,128)(2,1)} %param.53), channel_id=1, source_target_pairs={{0,16},{16,0},{32,48},{48,32},{64,80},{80,64},{96,112},{112,96},{1... | collective-permute-start | bytes 172040 | tf_op jit(solution)/shard_map/ppermute | solution.py:84
  111.7 1.8 %copy-start.3 = (bf16[1,2048,256]{2,1,0:T(8,128)(2,1)S(1)}, bf16[1,2048,256]{2,1,0:T(8,128)(2,1)}, u32[]{:S(2)}) copy-start(bf16[1,2048,256]{2,1,0:T(8,128)(2,1)} %param.48) | copy-start | bytes 3145732
  118.7 17.5 %all-to-all-start.5 = ((bf16[16,128,128]{2,1,0:T(8,128)(2,1)}), bf16[16,128,128]{2,1,0:T(8,128)(2,1)S(1)}, u32[]{:S(2)}, u32[]{:S(2)}) async-start(bf16[16,128,128]{2,1,0:T(8,128)(2,1)} %pad_maximum_fusion.1), calls=%async_computation.5 | async-start | bytes 1048576 | tf_op jit(solution)/shard_map/all_to_all | solution.py:20
  136.5 5.4 %slice-start = ((bf16[16,2,3,512]{3,1,2,0:T(2,128)(2,1)}), bf16[16,2,2,512]{3,1,2,0:T(2,128)(2,1)S(1)}, s32[]{:S(2)}) async-start(bf16[16,2,3,512]{3,1,2,0:T(2,128)(2,1)} %param.40), calls=%async_computation.7 | async-start | bytes 131072 | tf_op jit(solution)/shard_map/slice | solution.py:227
  138.4 15.1 %all-to-all-start.6 = ((bf16[16,16,128]{2,1,0:T(8,128)(2,1)}), bf16[16,16,128]{2,1,0:T(8,128)(2,1)S(1)}, u32[]{:S(2)}, u32[]{:S(2)}) async-start(bf16[16,16,128]{2,1,0:T(8,128)(2,1)} %bitcast.51), calls=%async_computation.6 | async-start | bytes 131072 | tf_op jit(solution)/shard_map/all_to_all | solution.py:20

commit v6 on v5

--- a/solution.py
+++ b/solution.py
@@ -133,7 +133,7 @@
     step_share = jnp.sum(keys.astype(F32) * step_rows[None], axis=(1, 2)).reshape(CLASSES, seqs, 1)
     route_rows = class_pack[:, rows_k + 1, : 4 * seqs].astype(F32)
     route_rows = jnp.pad(route_rows, ((0, seqs - per_class), (0, 0)))
-    shares = exchange(
+    outgoing = (
         jnp.concatenate(
             [
                 main_share.reshape(CLASSES, seqs, pack_cols),
@@ -142,10 +142,9 @@
                 to_everyone(route_rows, CLASSES),
             ],
             axis=2,
-        ),
-        "ep",
-        near,
-    )
+        )
+    )
+    shares = exchange(outgoing, "ep", near)
     projected = jnp.sum(shares[:, :, : pack_cols + 1], axis=0)
     step_raw = projected[:, pack_cols]
     own_routes = lax.dynamic_index_in_dim(
@@ -376,4 +375,6 @@
         P("ep", None, "tp"),
         P("ep", None, None, None),
     )
-    return jax.shard_map(local, mesh=mesh, in_specs=in_specs, out_specs=out_specs, check_vma=False)
+    return jax.shard_map(
+        local, mesh=mesh, in_specs=in_specs, out_specs=out_specs, check_vma=False
+    )

time: 157 us -> 157 us (level)
  no operation moved by 1% of the time
where the time goes in v6:
time: 157 us; the launch traced here: 155 us
  starting transfers between devices  73.7 us (47%)
  waiting for transfers between devices  44.4 us (28%)
  other arithmetic  15.7 us (10%)
  matrix products  10.6 us (7%)
  local copies, waits for them, and re-layouts  8.22 us (5%)
  between operations  2.2 us (1%)
    all_to_all x7, waiting for transfers between devices, exchange(): lax.all_to_all(pieces, axis, split_axis=0, concat_axis=0, tiled=True, axi...  44.4 us
    all_to_all x7, starting transfers between devices, exchange(): lax.all_to_all(pieces, axis, split_axis=0, concat_axis=0, tiled=True, axi...  34.7 us
    ppermute x3, starting transfers between devices, local(): class_pack.append(lax.ppermute(pack, 'ep', hops))  25.5 us
    ppermute x5, starting transfers between devices, from_other_core(): return lax.ppermute(shard, 'ep', [(i, i ^ 1) for i in range(n_ep)])  13.6 us
    dot_general x11, matrix products, dot32(): return jnp.dot(left, right, preferred_element_type=F32)  9.2 us
  transfers between devices with their start and end apart: 15, of which 6 were waited for; matrix products, arithmetic and copies ran while one was open for 13% of the time, Pallas kernels for 0%

profile of v6, /device:TPU:1, one launch (start us, length us, event | category | flops | bytes accessed | tf_op | source)
XLA Modules:
  0.0 154.8 jit_solution(5269077383501033319)
XLA Ops:
  0.8 0.8 fusion.127
  1.7 0.8 convert_bitcast_fusion.2
  2.4 0.8 fusion.7
  3.5 0.7 constant_dynamic-slice_fusion.2
  4.4 0.8 fusion.47
  5.2 9.6 %collective-permute-start.2 = (bf16[72,384]{1,0:T(8,128)(2,1)S(1)}, bf16[72,384]{1,0:T(8,128)(2,1)S(1)}, u32[]{:S(2)}, u32[]{:S(2)}) collective-permute-start(bf16[72,384]{1,0:T(8,128)(2,1)S(1)} %fusion.47), channel_id=1, source_target_pairs={{0,128},{16,144},{32,160},{48,176},{64,192},{80,208},{96,224},{112... | collective-permute-start | bytes 165896 | tf_op jit(solution)/shard_map/ppermute | solution.py:120
  14.8 5.6 %collective-permute-start = (bf16[72,384]{1,0:T(8,128)(2,1)S(1)}, bf16[72,384]{1,0:T(8,128)(2,1)S(1)}, u32[]{:S(2)}, u32[]{:S(2)}) collective-permute-start(bf16[72,384]{1,0:T(8,128)(2,1)S(1)} %fusion.47), channel_id=1, source_target_pairs={{0,384},{16,400},{32,416},{48,432},{64,448},{80,464},{96,480},{112... | collective-permute-start | bytes 165896 | tf_op jit(solution)/shard_map/ppermute | solution.py:120
  20.4 10.3 %collective-permute-start.1 = (bf16[72,384]{1,0:T(8,128)(2,1)S(1)}, bf16[72,384]{1,0:T(8,128)(2,1)S(1)}, u32[]{:S(2)}, u32[]{:S(2)}) collective-permute-start(bf16[72,384]{1,0:T(8,128)(2,1)S(1)} %fusion.47), channel_id=1, source_target_pairs={{0,256},{16,272},{32,288},{48,304},{64,320},{80,336},{96,352},{112... | collective-permute-start | bytes 165896 | tf_op jit(solution)/shard_map/ppermute | solution.py:120
  30.7 1.0 fusion.18
  31.7 0.9 fusion.20
  32.7 0.2 reshape.458
  33.0 0.8 reshape.459
  33.7 4.8 %all-to-all-start = ((bf16[8,16,256]{2,1,0:T(8,128)(2,1)}), bf16[8,16,256]{2,1,0:T(8,128)(2,1)S(1)}, u32[]{:S(2)}, u32[]{:S(2)}) async-start(bf16[8,16,256]{2,1,0:T(8,128)(2,1)} %reshape.459), calls=%async_computation | async-start | bytes 131072 | tf_op jit(solution)/shard_map/all_to_all | solution.py:20
  38.5 2.0 %collective-permute-start.3 = (bf16[128,448]{0,1:T(8,128)(2,1)S(1)}, bf16[128,448]{0,1:T(8,128)(2,1)S(1)}, u32[]{:S(2)}, u32[]{:S(2)}) collective-permute-start(bf16[128,448]{0,1:T(8,128)(2,1)S(1)} %pad_maximum_fusion.5), channel_id=1, source_target_pairs={{0,16},{16,0},{32,48},{48,32},{64,80},{80,64},{96,112},{112,96},{1... | collective-permute-start | bytes 344072 | tf_op jit(solution)/shard_map/ppermute | solution.py:84
  40.7 0.7 dynamic-slice_convert_fusion
  41.4 0.8 dynamic-slice_bitcast_fusion
  42.5 1.1 all-to-all-done
  44.2 0.2 fusion.128
  44.5 0.8 pad_maximum_fusion.2
  45.3 4.3 %all-to-all-start.1 = ((f32[8,16,512]{2,1,0:T(8,128)}), f32[8,16,512]{2,1,0:T(8,128)S(1)}, u32[]{:S(2)}, u32[]{:S(2)}) async-start(f32[8,16,512]{2,1,0:T(8,128)} %pad_maximum_fusion.2), calls=%async_computation.1 | async-start | bytes 524288 | tf_op jit(solution)/shard_map/all_to_all | solution.py:20
  49.7 0.6 dynamic_slice.41
  50.3 0.6 dynamic_slice.42
  51.6 0.6 dynamic_slice.45
  52.3 0.3 concatenate.57
  52.6 5.7 %all-to-all-done.1 = f32[8,16,512]{2,1,0:T(8,128)S(1)} async-done(((f32[8,16,512]{2,1,0:T(8,128)}), f32[8,16,512]{2,1,0:T(8,128)S(1)}, u32[]{:S(2)}, u32[]{:S(2)}) %all-to-all-start.1) | async-done | bytes 262176 | tf_op jit(solution)/shard_map/all_to_all | solution.py:20
  58.4 0.8 fusion.84
  59.3 0.4 fusion.10
  59.8 0.8 multiply_reduce_fusion.4
  60.6 0.2 fusion.2
  60.8 0.7 pad_maximum_fusion.4
  61.5 6.8 %all-to-all-start.2 = ((bf16[16,32,128]{2,1,0:T(8,128)(2,1)}), bf16[16,32,128]{2,1,0:T(8,128)(2,1)S(1)}, u32[]{:S(2)}, u32[]{:S(2)}) async-start(bf16[16,32,128]{2,1,0:T(8,128)(2,1)} %pad_maximum_fusion.4), calls=%async_computation.2 | async-start | bytes 262144 | tf_op jit(solution)/shard_map/all_to_all | solution.py:20
  68.4 0.3 select_reduce_fusion
  68.6 6.5 %all-to-all-done.2 = bf16[16,32,128]{2,1,0:T(8,128)(2,1)S(1)} async-done(((bf16[16,32,128]{2,1,0:T(8,128)(2,1)}), bf16[16,32,128]{2,1,0:T(8,128)(2,1)S(1)}, u32[]{:S(2)}, u32[]{:S(2)}) %all-to-all-start.2) | async-done | bytes 131104 | tf_op jit(solution)/shard_map/all_to_all | solution.py:20
  75.1 0.7 multiply_convert_fusion.4
  75.8 0.6 broadcast_in_dim.245
  76.5 4.8 %all-to-all-start.3 = ((bf16[16,16,128]{2,1,0:T(8,128)(2,1)}), bf16[16,16,128]{2,1,0:T(8,128)(2,1)S(1)}, u32[]{:S(2)}, u32[]{:S(2)}) async-start(bf16[16,16,128]{2,1,0:T(8,128)(2,1)} %broadcast_in_dim.245), calls=%async_computation.3 | async-start | bytes 131072 | tf_op jit(solution)/shard_map/all_to_all | solution.py:20
  81.2 0.2 convolution_select_fusion.1
  81.5 11.3 %all-to-all-done.3 = bf16[16,16,128]{2,1,0:T(8,128)(2,1)S(1)} async-done(((bf16[16,16,128]{2,1,0:T(8,128)(2,1)}), bf16[16,16,128]{2,1,0:T(8,128)(2,1)S(1)}, u32[]{:S(2)}, u32[]{:S(2)}) %all-to-all-start.3) | async-done | bytes 65568 | tf_op jit(solution)/shard_map/all_to_all | solution.py:20
  93.0 0.3 fusion
  93.4 0.3 fusion.5
  93.7 0.9 pad_maximum_fusion
  94.7 3.7 %all-to-all-start.4 = ((bf16[16,24,1024]{2,1,0:T(8,128)(2,1)}), bf16[16,24,1024]{2,1,0:T(8,128)(2,1)S(1)}, u32[]{:S(2)}, u32[]{:S(2)}) async-start(bf16[16,24,1024]{2,1,0:T(8,128)(2,1)} %pad_maximum_fusion), calls=%async_computation.4 | async-start | bytes 1572864 | tf_op jit(solution)/shard_map/all_to_all | solution.py:20
  98.4 5.3 %collective-permute-start.5 = (bf16[2048,256]{1,0:T(8,128)(2,1)}, bf16[2048,256]{1,0:T(8,128)(2,1)}, u32[]{:S(2)}, u32[]{:S(2)}) collective-permute-start(bf16[2048,256]{1,0:T(8,128)(2,1)} %bitcast.177), channel_id=1, source_target_pairs={{0,16},{16,0},{32,48},{48,32},{64,80},{80,64},{96,112},{112,96},{1... | collective-permute-start | bytes 3145736 | tf_op jit(solution)/shard_map/ppermute | solution.py:84
  103.7 1.9 %collective-permute-start.4 = (bf16[2048,256]{1,0:T(8,128)(2,1)S(1)}, bf16[2048,256]{1,0:T(8,128)(2,1)}, u32[]{:S(2)}, u32[]{:S(2)}) collective-permute-start(bf16[2048,256]{1,0:T(8,128)(2,1)S(1)} %bitcast.174), channel_id=1, source_target_pairs={{0,16},{16,0},{32,48},{48,32},{64,80},{80,64},{96,112},{112,96},{1... | collective-permute-start | bytes 3145736 | tf_op jit(solution)/shard_map/ppermute | solution.py:84
  105.6 2.4 %collective-permute-start.6 = (bf16[256,2048]{1,0:T(8,128)(2,1)}, bf16[256,2048]{1,0:T(8,128)(2,1)}, u32[]{:S(2)}, u32[]{:S(2)}) collective-permute-start(bf16[256,2048]{1,0:T(8,128)(2,1)} %bitcast.178), channel_id=1, source_target_pairs={{0,16},{16,0},{32,48},{48,32},{64,80},{80,64},{96,112},{112,96},{1... | collective-permute-start | bytes 3145736 | tf_op jit(solution)/shard_map/ppermute | solution.py:84
  108.1 1.9 %collective-permute-start.7 = (bf16[224,128]{1,0:T(8,128)(2,1)}, bf16[224,128]{1,0:T(8,128)(2,1)}, u32[]{:S(2)}, u32[]{:S(2)}) collective-permute-start(bf16[224,128]{1,0:T(8,128)(2,1)} %param.53), channel_id=1, source_target_pairs={{0,16},{16,0},{32,48},{48,32},{64,80},{80,64},{96,112},{112,96},{1... | collective-permute-start | bytes 172040 | tf_op jit(solution)/shard_map/ppermute | solution.py:84
  110.1 0.3 fusion.91
  110.4 0.2 multiply_reduce_fusion
  110.9 0.2 fusion.82
  111.7 0.2 convolution_multiply_fusion.3
  111.9 1.5 convolution_multiply_fusion
  113.5 2.0 %convolution_convert_fusion.1 = bf16[32,2048]{1,0:T(8,128)(2,1)S(1)} fusion(bf16[4,8,16,128]{3,2,1,0:T(8,128)(2,1)S(1)} %copy.140, f32[32,256]{1,0:T(8,128)S(1)} %convolution_multiply_fusion.3, f32[32]{0:T(128)S(1)} %mul.382, bf16[1,256,2048]{2,1,0:T(8,128)(2,1)} %param.49, bf16[1,2048,256]{2,1,0:T(8,128)(2,1)S(1)} %copy-done.3), kind=kOutput, calls=%fused_computation.1 | convolution fusion | flops 67231744 | bytes 2392192 | tf_op jit(solution)/shard_map/dot_general | solution.py:35
  115.5 2.3 %convolution_convert_fusion = bf16[32,2048]{1,0:T(8,128)(2,1)S(1)} fusion(bf16[256,2048]{1,0:T(8,128)(2,1)} %collective-permute-done.6, f32[32,256]{1,0:T(8,128)S(1)} %convolution_multiply_fusion, bf16[2048,256]{1,0:T(8,128)(2,1)} %collective-permute-done.4, bf16[4,8,16,128]{3,2,1,0:T(8,128)(2,1)S(1)} %copy.139, f32[32]{0:T(128)S(1)} %mul.388), kind=kOutput, calls=%fused_computation | convolution fusion | flops 67231744 | bytes 2392192 | tf_op jit(solution)/shard_map/dot_general | solution.py:35
  117.9 0.8 pad_maximum_fusion.1
  118.7 6.9 %all-to-all-start.5 = ((bf16[16,128,128]{2,1,0:T(8,128)(2,1)}), bf16[16,128,128]{2,1,0:T(8,128)(2,1)S(1)}, u32[]{:S(2)}, u32[]{:S(2)}) async-start(bf16[16,128,128]{2,1,0:T(8,128)(2,1)} %pad_maximum_fusion.1), calls=%async_computation.5 | async-start | bytes 1048576 | tf_op jit(solution)/shard_map/all_to_all | solution.py:20
  125.6 0.6 fusion.69
  126.2 1.0 multiply_add_fusion
  127.2 9.0 %all-to-all-done.5 = bf16[16,128,128]{2,1,0:T(8,128)(2,1)S(1)} async-done(((bf16[16,128,128]{2,1,0:T(8,128)(2,1)}), bf16[16,128,128]{2,1,0:T(8,128)(2,1)S(1)}, u32[]{:S(2)}, u32[]{:S(2)}) %all-to-all-start.5) | async-done | bytes 524320 | tf_op jit(solution)/shard_map/all_to_all | solution.py:20
  136.2 0.3 fusion.63
  136.7 1.7 %fusion.1 = bf16[256,128]{1,0:T(8,128)(2,1)} fusion(f32[256,128]{1,0:T(8,128)S(1)} %fusion.63, bf16[32,8,4,128]{3,2,1,0:T(4,128)(2,1)S(1)} %bitcast.182, bf16[224,128]{1,0:T(8,128)(2,1)} %collective-permute-done.7, bf16[224,128]{1,0:T(8,128)(2,1)} %param.53), kind=kOutput, calls=%fused_computation.6 | convolution fusion | flops 34078720 | bytes 573440 | tf_op jit(solution)/shard_map/dot_general | solution.py:35
  138.4 3.5 %all-to-all-start.6 = ((bf16[16,16,128]{2,1,0:T(8,128)(2,1)}), bf16[16,16,128]{2,1,0:T(8,128)(2,1)S(1)}, u32[]{:S(2)}, u32[]{:S(2)}) async-start(bf16[16,16,128]{2,1,0:T(8,128)(2,1)} %bitcast.51), calls=%async_computation.6 | async-start | bytes 131072 | tf_op jit(solution)/shard_map/all_to_all | solution.py:20
  142.0 0.8 pad_maximum_fusion.6
  142.7 10.8 %all-to-all-done.6 = bf16[16,16,128]{2,1,0:T(8,128)(2,1)S(1)} async-done(((bf16[16,16,128]{2,1,0:T(8,128)(2,1)}), bf16[16,16,128]{2,1,0:T(8,128)(2,1)S(1)}, u32[]{:S(2)}, u32[]{:S(2)}) %all-to-all-start.6) | async-done | bytes 65568 | tf_op jit(solution)/shard_map/all_to_all | solution.py:20
  153.6 1.3 fusion.83
  (135 shorter events, 3.9 us)
Async XLA Ops:
  0.6 59.9 %copy-start = (bf16[64,2048]{1,0:T(8,128)(2,1)S(1)}, bf16[64,2048]{1,0:T(8,128)(2,1)}, u32[]{:S(2)}) copy-start(bf16[64,2048]{1,0:T(8,128)(2,1)} %param.43) | copy-start | bytes 786436
  0.6 39.9 %copy-start.8 = (bf16[64,64]{1,0:T(8,128)(2,1)S(1)}, bf16[64,64]{1,0:T(8,128)(2,1)}, u32[]{:S(2)}) copy-start(bf16[64,64]{1,0:T(8,128)(2,1)} %param.29) | copy-start | bytes 24580
  0.7 39.9 %copy-start.7 = (bf16[64,64]{1,0:T(8,128)(2,1)S(1)}, bf16[64,64]{1,0:T(8,128)(2,1)}, u32[]{:S(2)}) copy-start(bf16[64,64]{1,0:T(8,128)(2,1)} %param.30) | copy-start | bytes 24580
  0.7 37.8 %copy-start.5 = (bf16[128,224]{0,1:T(8,128)(2,1)S(1)}, bf16[128,224]{0,1:T(8,128)(2,1)}, u32[]{:S(2)}) copy-start(bf16[128,224]{0,1:T(8,128)(2,1)} %param.51) | copy-start | bytes 172036
  0.7 37.8 %copy-start.6 = (bf16[128,224]{0,1:T(8,128)(2,1)S(1)}, bf16[128,224]{0,1:T(8,128)(2,1)}, u32[]{:S(2)}) copy-start(bf16[128,224]{0,1:T(8,128)(2,1)} %param.52) | copy-start | bytes 172036
  5.2 37.1 %collective-permute-start.2 = (bf16[72,384]{1,0:T(8,128)(2,1)S(1)}, bf16[72,384]{1,0:T(8,128)(2,1)S(1)}, u32[]{:S(2)}, u32[]{:S(2)}) collective-permute-start(bf16[72,384]{1,0:T(8,128)(2,1)S(1)} %fusion.47), channel_id=1, source_target_pairs={{0,128},{16,144},{32,160},{48,176},{64,192},{80,208},{96,224},{112... | collective-permute-start | bytes 165896 | tf_op jit(solution)/shard_map/ppermute | solution.py:120
  14.8 27.5 %collective-permute-start = (bf16[72,384]{1,0:T(8,128)(2,1)S(1)}, bf16[72,384]{1,0:T(8,128)(2,1)S(1)}, u32[]{:S(2)}, u32[]{:S(2)}) collective-permute-start(bf16[72,384]{1,0:T(8,128)(2,1)S(1)} %fusion.47), channel_id=1, source_target_pairs={{0,384},{16,400},{32,416},{48,432},{64,448},{80,464},{96,480},{112... | collective-permute-start | bytes 165896 | tf_op jit(solution)/shard_map/ppermute | solution.py:120
  20.4 21.9 %collective-permute-start.1 = (bf16[72,384]{1,0:T(8,128)(2,1)S(1)}, bf16[72,384]{1,0:T(8,128)(2,1)S(1)}, u32[]{:S(2)}, u32[]{:S(2)}) collective-permute-start(bf16[72,384]{1,0:T(8,128)(2,1)S(1)} %fusion.47), channel_id=1, source_target_pairs={{0,256},{16,272},{32,288},{48,304},{64,320},{80,336},{96,352},{112... | collective-permute-start | bytes 165896 | tf_op jit(solution)/shard_map/ppermute | solution.py:120
  33.7 9.9 %all-to-all-start = ((bf16[8,16,256]{2,1,0:T(8,128)(2,1)}), bf16[8,16,256]{2,1,0:T(8,128)(2,1)S(1)}, u32[]{:S(2)}, u32[]{:S(2)}) async-start(bf16[8,16,256]{2,1,0:T(8,128)(2,1)} %reshape.459), calls=%async_computation | async-start | bytes 131072 | tf_op jit(solution)/shard_map/all_to_all | solution.py:20
  38.5 13.8 %collective-permute-start.3 = (bf16[128,448]{0,1:T(8,128)(2,1)S(1)}, bf16[128,448]{0,1:T(8,128)(2,1)S(1)}, u32[]{:S(2)}, u32[]{:S(2)}) collective-permute-start(bf16[128,448]{0,1:T(8,128)(2,1)S(1)} %pad_maximum_fusion.5), channel_id=1, source_target_pairs={{0,16},{16,0},{32,48},{48,32},{64,80},{80,64},{96,112},{112,96},{1... | collective-permute-start | bytes 344072 | tf_op jit(solution)/shard_map/ppermute | solution.py:84
  43.8 5.8 %copy-start.4 = (bf16[16,2,3,512]{3,1,2,0:T(2,128)(2,1)S(1)}, bf16[16,2,3,512]{3,1,2,0:T(2,128)(2,1)}, u32[]{:S(2)}) copy-start(bf16[16,2,3,512]{3,1,2,0:T(2,128)(2,1)} %param.40) | copy-start | bytes 294916
  44.0 5.8 %copy-start.11 = (bf16[4,64]{1,0:T(4,128)(2,1)S(1)}, bf16[4,64]{1,0:T(4,128)(2,1)}, u32[]{:S(2)}) copy-start(bf16[4,64]{1,0:T(4,128)(2,1)} %param.37) | copy-start | bytes 1540
  44.0 5.8 %copy-start.13 = (f32[16]{0:T(128)S(1)}, f32[16]{0:T(128)}, u32[]{:S(2)}) copy-start(f32[16]{0:T(128)} %param.34) | copy-start | bytes 196
  44.0 6.3 %copy-start.14 = (f32[16]{0:T(128)S(1)}, f32[16]{0:T(128)}, u32[]{:S(2)}) copy-start(f32[16]{0:T(128)} %param.35) | copy-start | bytes 196
  44.0 7.6 %copy-start.15 = (f32[16]{0:T(128)S(1)}, f32[16]{0:T(128)}, u32[]{:S(2)}) copy-start(f32[16]{0:T(128)} %param.36) | copy-start | bytes 196
  44.0 8.2 %copy-start.10 = (f32[2048]{0:T(1024)S(1)}, f32[2048]{0:T(1024)}, u32[]{:S(2)}) copy-start(f32[2048]{0:T(1024)} %param.44) | copy-start | bytes 24580
  45.3 13.9 %copy-start.9 = (bf16[16,3,64]{2,0,1:T(8,128)(2,1)S(1)}, bf16[16,3,64]{2,0,1:T(8,128)(2,1)}, u32[]{:S(2)}) copy-start(bf16[16,3,64]{2,0,1:T(8,128)(2,1)} %param.39) | copy-start | bytes 18436
  45.3 14.0 %copy-start.1 = (f32[16,1,64,128]{3,2,1,0:T(8,128)S(1)}, f32[16,1,64,128]{3,2,1,0:T(8,128)}, u32[]{:S(2)}) copy-start(f32[16,1,64,128]{3,2,1,0:T(8,128)} %param.41) | copy-start | bytes 1572868
  45.3 13.0 %all-to-all-start.1 = ((f32[8,16,512]{2,1,0:T(8,128)}), f32[8,16,512]{2,1,0:T(8,128)S(1)}, u32[]{:S(2)}, u32[]{:S(2)}) async-start(f32[8,16,512]{2,1,0:T(8,128)} %pad_maximum_fusion.2), calls=%async_computation.1 | async-start | bytes 524288 | tf_op jit(solution)/shard_map/all_to_all | solution.py:20
  49.6 10.9 %copy-start.12 = (f32[64]{0:T(128)S(1)}, f32[64]{0:T(128)}, u32[]{:S(2)}) copy-start(f32[64]{0:T(128)} %param.42) | copy-start | bytes 772
  61.5 13.6 %all-to-all-start.2 = ((bf16[16,32,128]{2,1,0:T(8,128)(2,1)}), bf16[16,32,128]{2,1,0:T(8,128)(2,1)S(1)}, u32[]{:S(2)}, u32[]{:S(2)}) async-start(bf16[16,32,128]{2,1,0:T(8,128)(2,1)} %pad_maximum_fusion.4), calls=%async_computation.2 | async-start | bytes 262144 | tf_op jit(solution)/shard_map/all_to_all | solution.py:20
  76.5 16.4 %all-to-all-start.3 = ((bf16[16,16,128]{2,1,0:T(8,128)(2,1)}), bf16[16,16,128]{2,1,0:T(8,128)(2,1)S(1)}, u32[]{:S(2)}, u32[]{:S(2)}) async-start(bf16[16,16,128]{2,1,0:T(8,128)(2,1)} %broadcast_in_dim.245), calls=%async_computation.3 | async-start | bytes 131072 | tf_op jit(solution)/shard_map/all_to_all | solution.py:20
  94.7 9.0 %copy-start.2 = (bf16[1,2048,256]{2,1,0:T(8,128)(2,1)S(1)}, bf16[1,2048,256]{2,1,0:T(8,128)(2,1)}, u32[]{:S(2)}) copy-start(bf16[1,2048,256]{2,1,0:T(8,128)(2,1)} %param.47) | copy-start | bytes 3145732
  94.7 15.7 %all-to-all-start.4 = ((bf16[16,24,1024]{2,1,0:T(8,128)(2,1)}), bf16[16,24,1024]{2,1,0:T(8,128)(2,1)S(1)}, u32[]{:S(2)}, u32[]{:S(2)}) async-start(bf16[16,24,1024]{2,1,0:T(8,128)(2,1)} %pad_maximum_fusion), calls=%async_computation.4 | async-start | bytes 1572864 | tf_op jit(solution)/shard_map/all_to_all | solution.py:20
  98.4 13.5 %collective-permute-start.5 = (bf16[2048,256]{1,0:T(8,128)(2,1)}, bf16[2048,256]{1,0:T(8,128)(2,1)}, u32[]{:S(2)}, u32[]{:S(2)}) collective-permute-start(bf16[2048,256]{1,0:T(8,128)(2,1)} %bitcast.177), channel_id=1, source_target_pairs={{0,16},{16,0},{32,48},{48,32},{64,80},{80,64},{96,112},{112,96},{1... | collective-permute-start | bytes 3145736 | tf_op jit(solution)/shard_map/ppermute | solution.py:84
  103.7 11.7 %collective-permute-start.4 = (bf16[2048,256]{1,0:T(8,128)(2,1)S(1)}, bf16[2048,256]{1,0:T(8,128)(2,1)}, u32[]{:S(2)}, u32[]{:S(2)}) collective-permute-start(bf16[2048,256]{1,0:T(8,128)(2,1)S(1)} %bitcast.174), channel_id=1, source_target_pairs={{0,16},{16,0},{32,48},{48,32},{64,80},{80,64},{96,112},{112,96},{1... | collective-permute-start | bytes 3145736 | tf_op jit(solution)/shard_map/ppermute | solution.py:84
  105.6 9.8 %collective-permute-start.6 = (bf16[256,2048]{1,0:T(8,128)(2,1)}, bf16[256,2048]{1,0:T(8,128)(2,1)}, u32[]{:S(2)}, u32[]{:S(2)}) collective-permute-start(bf16[256,2048]{1,0:T(8,128)(2,1)} %bitcast.178), channel_id=1, source_target_pairs={{0,16},{16,0},{32,48},{48,32},{64,80},{80,64},{96,112},{112,96},{1... | collective-permute-start | bytes 3145736 | tf_op jit(solution)/shard_map/ppermute | solution.py:84
  108.1 28.6 %collective-permute-start.7 = (bf16[224,128]{1,0:T(8,128)(2,1)}, bf16[224,128]{1,0:T(8,128)(2,1)}, u32[]{:S(2)}, u32[]{:S(2)}) collective-permute-start(bf16[224,128]{1,0:T(8,128)(2,1)} %param.53), channel_id=1, source_target_pairs={{0,16},{16,0},{32,48},{48,32},{64,80},{80,64},{96,112},{112,96},{1... | collective-permute-start | bytes 172040 | tf_op jit(solution)/shard_map/ppermute | solution.py:84
  111.7 1.8 %copy-start.3 = (bf16[1,2048,256]{2,1,0:T(8,128)(2,1)S(1)}, bf16[1,2048,256]{2,1,0:T(8,128)(2,1)}, u32[]{:S(2)}) copy-start(bf16[1,2048,256]{2,1,0:T(8,128)(2,1)} %param.48) | copy-start | bytes 3145732
  118.7 17.5 %all-to-all-start.5 = ((bf16[16,128,128]{2,1,0:T(8,128)(2,1)}), bf16[16,128,128]{2,1,0:T(8,128)(2,1)S(1)}, u32[]{:S(2)}, u32[]{:S(2)}) async-start(bf16[16,128,128]{2,1,0:T(8,128)(2,1)} %pad_maximum_fusion.1), calls=%async_computation.5 | async-start | bytes 1048576 | tf_op jit(solution)/shard_map/all_to_all | solution.py:20
  136.5 5.4 %slice-start = ((bf16[16,2,3,512]{3,1,2,0:T(2,128)(2,1)}), bf16[16,2,2,512]{3,1,2,0:T(2,128)(2,1)S(1)}, s32[]{:S(2)}) async-start(bf16[16,2,3,512]{3,1,2,0:T(2,128)(2,1)} %param.40), calls=%async_computation.7 | async-start | bytes 131072 | tf_op jit(solution)/shard_map/slice | solution.py:226
  138.4 15.1 %all-to-all-start.6 = ((bf16[16,16,128]{2,1,0:T(8,128)(2,1)}), bf16[16,16,128]{2,1,0:T(8,128)(2,1)S(1)}, u32[]{:S(2)}, u32[]{:S(2)}) async-start(bf16[16,16,128]{2,1,0:T(8,128)(2,1)} %bitcast.51), calls=%async_computation.6 | async-start | bytes 131072 | tf_op jit(solution)/shard_map/all_to_all | solution.py:20

commit v7 on v5

--- a/solution.py
+++ b/solution.py
@@ -114,10 +114,14 @@
     extra = jnp.concatenate([step_row, route_row, jnp.zeros((6, rows_k), BF)], axis=0)
     extra = jnp.pad(extra, ((0, 0), (0, pack_cols - rows_k)))
     pack = jnp.concatenate([main, extra], axis=0)
-    class_pack = [pack]
-    for ahead in range(1, per_class):
-        hops = [(i, (i - CLASSES * ahead) % n_ep) for i in range(n_ep)]
-        class_pack.append(lax.ppermute(pack, "ep", hops))
+    def from_ahead(shard, classes_on):
+        hops = [(i, (i - CLASSES * classes_on) % n_ep) for i in range(n_ep)]
+        return lax.ppermute(shard, "ep", hops)
+
+    class_pack = [pack, from_ahead(pack, 1)]
+    for ahead in range(2, per_class - 1):
+        class_pack.append(from_ahead(class_pack[-1], 1))
+    class_pack.append(from_ahead(pack, -1))
     class_pack = jnp.stack(class_pack)
 
     normed = rms_scale(tokens.astype(F32), mix_gain).astype(BF)

time: 157 us -> 163 us (1.038)
  starting transfers between devices: 73.7 us -> 80.2 us
    all_to_all x7, starting transfers between devices: 34.7 us -> 43.6 us  [exchange(): lax.all_to_all(pieces, axis, split_axis=0, concat_axis=0, tiled=True, axi...]
    ppermute x3, starting transfers between devices: 25.5 us -> 22.3 us  [from_ahead(): return lax.ppermute(shard, 'ep', hops)]
where the time goes in v7:
time: 163 us; the launch traced here: 161 us
  starting transfers between devices  80.2 us (49%)
  waiting for transfers between devices  44.1 us (27%)
  other arithmetic  15.7 us (10%)
  matrix products  10.6 us (7%)
  local copies, waits for them, and re-layouts  8.23 us (5%)
  between operations  2.21 us (1%)
    all_to_all x7, starting transfers between devices, exchange(): lax.all_to_all(pieces, axis, split_axis=0, concat_axis=0, tiled=True, axi...  43.6 us
    all_to_all x7, waiting for transfers between devices, exchange(): lax.all_to_all(pieces, axis, split_axis=0, concat_axis=0, tiled=True, axi...  43.2 us
    ppermute x3, starting transfers between devices, from_ahead(): return lax.ppermute(shard, 'ep', hops)  22.3 us
    ppermute x5, starting transfers between devices, from_other_core(): return lax.ppermute(shard, 'ep', [(i, i ^ 1) for i in range(n_ep)])  14.2 us
    dot_general x11, matrix products, dot32(): return jnp.dot(left, right, preferred_element_type=F32)  9.2 us
  transfers between devices with their start and end apart: 15, of which 6 were waited for; matrix products, arithmetic and copies ran while one was open for 13% of the time, Pallas kernels for 0%

profile of v7, /device:TPU:1, one launch (start us, length us, event | category | flops | bytes accessed | tf_op | source)
XLA Modules:
  0.0 161.0 jit_solution(16213593040220955911)
XLA Ops:
  0.8 0.8 fusion.127
  1.7 0.8 convert_bitcast_fusion.2
  2.4 0.8 fusion.7
  3.5 0.7 constant_dynamic-slice_fusion.2
  4.4 0.8 fusion.47
  5.2 13.3 %collective-permute-start = (bf16[72,384]{1,0:T(8,128)(2,1)S(1)}, bf16[72,384]{1,0:T(8,128)(2,1)S(1)}, u32[]{:S(2)}, u32[]{:S(2)}) collective-permute-start(bf16[72,384]{1,0:T(8,128)(2,1)S(1)} %fusion.47), channel_id=1, source_target_pairs={{0,384},{16,400},{32,416},{48,432},{64,448},{80,464},{96,480},{112... | collective-permute-start | bytes 165896 | tf_op jit(solution)/shard_map/ppermute | solution.py:119
  18.5 1.9 %collective-permute-start.2 = (bf16[72,384]{1,0:T(8,128)(2,1)S(1)}, bf16[72,384]{1,0:T(8,128)(2,1)S(1)}, u32[]{:S(2)}, u32[]{:S(2)}) collective-permute-start(bf16[72,384]{1,0:T(8,128)(2,1)S(1)} %fusion.47), channel_id=1, source_target_pairs={{0,128},{16,144},{32,160},{48,176},{64,192},{80,208},{96,224},{112... | collective-permute-start | bytes 165896 | tf_op jit(solution)/shard_map/ppermute | solution.py:119
  20.4 1.0 fusion.18
  21.4 0.9 fusion.20
  22.5 0.2 reshape.458
  22.7 0.8 reshape.459
  23.5 4.6 %all-to-all-start = ((bf16[8,16,256]{2,1,0:T(8,128)(2,1)}), bf16[8,16,256]{2,1,0:T(8,128)(2,1)S(1)}, u32[]{:S(2)}, u32[]{:S(2)}) async-start(bf16[8,16,256]{2,1,0:T(8,128)(2,1)} %reshape.459), calls=%async_computation | async-start | bytes 131072 | tf_op jit(solution)/shard_map/all_to_all | solution.py:20
  28.2 2.0 %collective-permute-start.3 = (bf16[128,448]{0,1:T(8,128)(2,1)S(1)}, bf16[128,448]{0,1:T(8,128)(2,1)S(1)}, u32[]{:S(2)}, u32[]{:S(2)}) collective-permute-start(bf16[128,448]{0,1:T(8,128)(2,1)S(1)} %pad_maximum_fusion.5), channel_id=1, source_target_pairs={{0,16},{16,0},{32,48},{48,32},{64,80},{80,64},{96,112},{112,96},{1... | collective-permute-start | bytes 344072 | tf_op jit(solution)/shard_map/ppermute | solution.py:84
  30.3 0.7 dynamic-slice_convert_fusion
  31.1 7.1 %collective-permute-start.1 = (bf16[72,384]{1,0:T(8,128)(2,1)S(1)}, bf16[72,384]{1,0:T(8,128)(2,1)S(1)}, u32[]{:S(2)}, u32[]{:S(2)}) collective-permute-start(bf16[72,384]{1,0:T(8,128)(2,1)S(1)} %collective-permute-done), channel_id=1, source_target_pairs={{0,384},{16,400},{32,416},{48,432},{64,448},{80,464},{96,480},{112... | collective-permute-start | bytes 165896 | tf_op jit(solution)/shard_map/ppermute | solution.py:119
  38.2 0.8 dynamic-slice_bitcast_fusion
  39.0 0.8 collective-permute-done.1
  40.7 0.2 fusion.128
  40.9 0.8 pad_maximum_fusion.2
  41.7 9.8 %all-to-all-start.1 = ((f32[8,16,512]{2,1,0:T(8,128)}), f32[8,16,512]{2,1,0:T(8,128)S(1)}, u32[]{:S(2)}, u32[]{:S(2)}) async-start(f32[8,16,512]{2,1,0:T(8,128)} %pad_maximum_fusion.2), calls=%async_computation.1 | async-start | bytes 524288 | tf_op jit(solution)/shard_map/all_to_all | solution.py:20
  51.7 0.6 dynamic_slice.41
  52.3 0.6 dynamic_slice.42
  53.6 0.6 dynamic_slice.45
  54.3 0.3 concatenate.57
  54.5 5.7 %all-to-all-done.1 = f32[8,16,512]{2,1,0:T(8,128)S(1)} async-done(((f32[8,16,512]{2,1,0:T(8,128)}), f32[8,16,512]{2,1,0:T(8,128)S(1)}, u32[]{:S(2)}, u32[]{:S(2)}) %all-to-all-start.1) | async-done | bytes 262176 | tf_op jit(solution)/shard_map/all_to_all | solution.py:20
  60.3 0.8 fusion.84
  61.2 0.4 fusion.10
  61.7 0.8 multiply_reduce_fusion.4
  62.5 0.2 fusion.2
  62.7 0.7 pad_maximum_fusion.4
  63.4 5.5 %all-to-all-start.2 = ((bf16[16,32,128]{2,1,0:T(8,128)(2,1)}), bf16[16,32,128]{2,1,0:T(8,128)(2,1)S(1)}, u32[]{:S(2)}, u32[]{:S(2)}) async-start(bf16[16,32,128]{2,1,0:T(8,128)(2,1)} %pad_maximum_fusion.4), calls=%async_computation.2 | async-start | bytes 262144 | tf_op jit(solution)/shard_map/all_to_all | solution.py:20
  69.0 0.3 select_reduce_fusion
  69.3 6.5 %all-to-all-done.2 = bf16[16,32,128]{2,1,0:T(8,128)(2,1)S(1)} async-done(((bf16[16,32,128]{2,1,0:T(8,128)(2,1)}), bf16[16,32,128]{2,1,0:T(8,128)(2,1)S(1)}, u32[]{:S(2)}, u32[]{:S(2)}) %all-to-all-start.2) | async-done | bytes 131104 | tf_op jit(solution)/shard_map/all_to_all | solution.py:20
  75.8 0.7 multiply_convert_fusion.4
  76.5 0.6 broadcast_in_dim.245
  77.1 9.6 %all-to-all-start.3 = ((bf16[16,16,128]{2,1,0:T(8,128)(2,1)}), bf16[16,16,128]{2,1,0:T(8,128)(2,1)S(1)}, u32[]{:S(2)}, u32[]{:S(2)}) async-start(bf16[16,16,128]{2,1,0:T(8,128)(2,1)} %broadcast_in_dim.245), calls=%async_computation.3 | async-start | bytes 131072 | tf_op jit(solution)/shard_map/all_to_all | solution.py:20
  86.7 0.2 convolution_select_fusion.1
  87.0 11.3 %all-to-all-done.3 = bf16[16,16,128]{2,1,0:T(8,128)(2,1)S(1)} async-done(((bf16[16,16,128]{2,1,0:T(8,128)(2,1)}), bf16[16,16,128]{2,1,0:T(8,128)(2,1)S(1)}, u32[]{:S(2)}, u32[]{:S(2)}) %all-to-all-start.3) | async-done | bytes 65568 | tf_op jit(solution)/shard_map/all_to_all | solution.py:20
  98.5 0.3 fusion
  98.8 0.3 fusion.5
  99.2 0.9 pad_maximum_fusion
  100.1 3.7 %all-to-all-start.4 = ((bf16[16,24,1024]{2,1,0:T(8,128)(2,1)}), bf16[16,24,1024]{2,1,0:T(8,128)(2,1)S(1)}, u32[]{:S(2)}, u32[]{:S(2)}) async-start(bf16[16,24,1024]{2,1,0:T(8,128)(2,1)} %pad_maximum_fusion), calls=%async_computation.4 | async-start | bytes 1572864 | tf_op jit(solution)/shard_map/all_to_all | solution.py:20
  103.9 6.0 %collective-permute-start.5 = (bf16[2048,256]{1,0:T(8,128)(2,1)}, bf16[2048,256]{1,0:T(8,128)(2,1)}, u32[]{:S(2)}, u32[]{:S(2)}) collective-permute-start(bf16[2048,256]{1,0:T(8,128)(2,1)} %bitcast.177), channel_id=1, source_target_pairs={{0,16},{16,0},{32,48},{48,32},{64,80},{80,64},{96,112},{112,96},{1... | collective-permute-start | bytes 3145736 | tf_op jit(solution)/shard_map/ppermute | solution.py:84
  109.8 1.9 %collective-permute-start.4 = (bf16[2048,256]{1,0:T(8,128)(2,1)S(1)}, bf16[2048,256]{1,0:T(8,128)(2,1)}, u32[]{:S(2)}, u32[]{:S(2)}) collective-permute-start(bf16[2048,256]{1,0:T(8,128)(2,1)S(1)} %bitcast.174), channel_id=1, source_target_pairs={{0,16},{16,0},{32,48},{48,32},{64,80},{80,64},{96,112},{112,96},{1... | collective-permute-start | bytes 3145736 | tf_op jit(solution)/shard_map/ppermute | solution.py:84
  111.8 2.4 %collective-permute-start.6 = (bf16[256,2048]{1,0:T(8,128)(2,1)}, bf16[256,2048]{1,0:T(8,128)(2,1)}, u32[]{:S(2)}, u32[]{:S(2)}) collective-permute-start(bf16[256,2048]{1,0:T(8,128)(2,1)} %bitcast.178), channel_id=1, source_target_pairs={{0,16},{16,0},{32,48},{48,32},{64,80},{80,64},{96,112},{112,96},{1... | collective-permute-start | bytes 3145736 | tf_op jit(solution)/shard_map/ppermute | solution.py:84
  114.2 1.9 %collective-permute-start.7 = (bf16[224,128]{1,0:T(8,128)(2,1)}, bf16[224,128]{1,0:T(8,128)(2,1)}, u32[]{:S(2)}, u32[]{:S(2)}) collective-permute-start(bf16[224,128]{1,0:T(8,128)(2,1)} %param.53), channel_id=1, source_target_pairs={{0,16},{16,0},{32,48},{48,32},{64,80},{80,64},{96,112},{112,96},{1... | collective-permute-start | bytes 172040 | tf_op jit(solution)/shard_map/ppermute | solution.py:84
  116.2 0.3 fusion.91
  116.6 0.2 multiply_reduce_fusion
  117.0 0.2 fusion.82
  117.8 0.2 convolution_multiply_fusion.3
  118.1 1.5 convolution_multiply_fusion
  119.6 2.0 %convolution_convert_fusion.1 = bf16[32,2048]{1,0:T(8,128)(2,1)S(1)} fusion(bf16[4,8,16,128]{3,2,1,0:T(8,128)(2,1)S(1)} %copy.140, f32[32,256]{1,0:T(8,128)S(1)} %convolution_multiply_fusion.3, f32[32]{0:T(128)S(1)} %mul.382, bf16[1,256,2048]{2,1,0:T(8,128)(2,1)} %param.49, bf16[1,2048,256]{2,1,0:T(8,128)(2,1)S(1)} %copy-done.3), kind=kOutput, calls=%fused_computation.1 | convolution fusion | flops 67231744 | bytes 2392192 | tf_op jit(solution)/shard_map/dot_general | solution.py:35
  121.6 2.3 %convolution_convert_fusion = bf16[32,2048]{1,0:T(8,128)(2,1)S(1)} fusion(bf16[256,2048]{1,0:T(8,128)(2,1)} %collective-permute-done.6, f32[32,256]{1,0:T(8,128)S(1)} %convolution_multiply_fusion, bf16[2048,256]{1,0:T(8,128)(2,1)} %collective-permute-done.4, bf16[4,8,16,128]{3,2,1,0:T(8,128)(2,1)S(1)} %copy.139, f32[32]{0:T(128)S(1)} %mul.388), kind=kOutput, calls=%fused_computation | convolution fusion | flops 67231744 | bytes 2392192 | tf_op jit(solution)/shard_map/dot_general | solution.py:35
  124.0 0.8 pad_maximum_fusion.1
  124.9 6.9 %all-to-all-start.5 = ((bf16[16,128,128]{2,1,0:T(8,128)(2,1)}), bf16[16,128,128]{2,1,0:T(8,128)(2,1)S(1)}, u32[]{:S(2)}, u32[]{:S(2)}) async-start(bf16[16,128,128]{2,1,0:T(8,128)(2,1)} %pad_maximum_fusion.1), calls=%async_computation.5 | async-start | bytes 1048576 | tf_op jit(solution)/shard_map/all_to_all | solution.py:20
  131.7 0.6 fusion.69
  132.3 1.0 multiply_add_fusion
  133.4 9.0 %all-to-all-done.5 = bf16[16,128,128]{2,1,0:T(8,128)(2,1)S(1)} async-done(((bf16[16,128,128]{2,1,0:T(8,128)(2,1)}), bf16[16,128,128]{2,1,0:T(8,128)(2,1)S(1)}, u32[]{:S(2)}, u32[]{:S(2)}) %all-to-all-start.5) | async-done | bytes 524320 | tf_op jit(solution)/shard_map/all_to_all | solution.py:20
  142.4 0.3 fusion.63
  142.8 1.7 %fusion.1 = bf16[256,128]{1,0:T(8,128)(2,1)} fusion(f32[256,128]{1,0:T(8,128)S(1)} %fusion.63, bf16[32,8,4,128]{3,2,1,0:T(4,128)(2,1)S(1)} %bitcast.182, bf16[224,128]{1,0:T(8,128)(2,1)} %collective-permute-done.7, bf16[224,128]{1,0:T(8,128)(2,1)} %param.53), kind=kOutput, calls=%fused_computation.6 | convolution fusion | flops 34078720 | bytes 573440 | tf_op jit(solution)/shard_map/dot_general | solution.py:35
  144.5 3.5 %all-to-all-start.6 = ((bf16[16,16,128]{2,1,0:T(8,128)(2,1)}), bf16[16,16,128]{2,1,0:T(8,128)(2,1)S(1)}, u32[]{:S(2)}, u32[]{:S(2)}) async-start(bf16[16,16,128]{2,1,0:T(8,128)(2,1)} %bitcast.51), calls=%async_computation.6 | async-start | bytes 131072 | tf_op jit(solution)/shard_map/all_to_all | solution.py:20
  148.1 0.8 pad_maximum_fusion.6
  148.9 10.8 %all-to-all-done.6 = bf16[16,16,128]{2,1,0:T(8,128)(2,1)S(1)} async-done(((bf16[16,16,128]{2,1,0:T(8,128)(2,1)}), bf16[16,16,128]{2,1,0:T(8,128)(2,1)S(1)}, u32[]{:S(2)}, u32[]{:S(2)}) %all-to-all-start.6) | async-done | bytes 65568 | tf_op jit(solution)/shard_map/all_to_all | solution.py:20
  159.7 1.3 fusion.83
  (135 shorter events, 3.9 us)
Async XLA Ops:
  0.6 61.8 %copy-start = (bf16[64,2048]{1,0:T(8,128)(2,1)S(1)}, bf16[64,2048]{1,0:T(8,128)(2,1)}, u32[]{:S(2)}) copy-start(bf16[64,2048]{1,0:T(8,128)(2,1)} %param.43) | copy-start | bytes 786436
  0.6 29.5 %copy-start.8 = (bf16[64,64]{1,0:T(8,128)(2,1)S(1)}, bf16[64,64]{1,0:T(8,128)(2,1)}, u32[]{:S(2)}) copy-start(bf16[64,64]{1,0:T(8,128)(2,1)} %param.29) | copy-start | bytes 24580
  0.7 29.5 %copy-start.7 = (bf16[64,64]{1,0:T(8,128)(2,1)S(1)}, bf16[64,64]{1,0:T(8,128)(2,1)}, u32[]{:S(2)}) copy-start(bf16[64,64]{1,0:T(8,128)(2,1)} %param.30) | copy-start | bytes 24580
  0.7 27.5 %copy-start.5 = (bf16[128,224]{0,1:T(8,128)(2,1)S(1)}, bf16[128,224]{0,1:T(8,128)(2,1)}, u32[]{:S(2)}) copy-start(bf16[128,224]{0,1:T(8,128)(2,1)} %param.51) | copy-start | bytes 172036
  0.7 27.5 %copy-start.6 = (bf16[128,224]{0,1:T(8,128)(2,1)S(1)}, bf16[128,224]{0,1:T(8,128)(2,1)}, u32[]{:S(2)}) copy-start(bf16[128,224]{0,1:T(8,128)(2,1)} %param.52) | copy-start | bytes 172036
  5.2 25.9 %collective-permute-start = (bf16[72,384]{1,0:T(8,128)(2,1)S(1)}, bf16[72,384]{1,0:T(8,128)(2,1)S(1)}, u32[]{:S(2)}, u32[]{:S(2)}) collective-permute-start(bf16[72,384]{1,0:T(8,128)(2,1)S(1)} %fusion.47), channel_id=1, source_target_pairs={{0,384},{16,400},{32,416},{48,432},{64,448},{80,464},{96,480},{112... | collective-permute-start | bytes 165896 | tf_op jit(solution)/shard_map/ppermute | solution.py:119
  18.5 20.6 %collective-permute-start.2 = (bf16[72,384]{1,0:T(8,128)(2,1)S(1)}, bf16[72,384]{1,0:T(8,128)(2,1)S(1)}, u32[]{:S(2)}, u32[]{:S(2)}) collective-permute-start(bf16[72,384]{1,0:T(8,128)(2,1)S(1)} %fusion.47), channel_id=1, source_target_pairs={{0,128},{16,144},{32,160},{48,176},{64,192},{80,208},{96,224},{112... | collective-permute-start | bytes 165896 | tf_op jit(solution)/shard_map/ppermute | solution.py:119
  23.5 16.6 %all-to-all-start = ((bf16[8,16,256]{2,1,0:T(8,128)(2,1)}), bf16[8,16,256]{2,1,0:T(8,128)(2,1)S(1)}, u32[]{:S(2)}, u32[]{:S(2)}) async-start(bf16[8,16,256]{2,1,0:T(8,128)(2,1)} %reshape.459), calls=%async_computation | async-start | bytes 131072 | tf_op jit(solution)/shard_map/all_to_all | solution.py:20
  28.2 26.1 %collective-permute-start.3 = (bf16[128,448]{0,1:T(8,128)(2,1)S(1)}, bf16[128,448]{0,1:T(8,128)(2,1)S(1)}, u32[]{:S(2)}, u32[]{:S(2)}) collective-permute-start(bf16[128,448]{0,1:T(8,128)(2,1)S(1)} %pad_maximum_fusion.5), channel_id=1, source_target_pairs={{0,16},{16,0},{32,48},{48,32},{64,80},{80,64},{96,112},{112,96},{1... | collective-permute-start | bytes 344072 | tf_op jit(solution)/shard_map/ppermute | solution.py:84
  31.1 8.8 %collective-permute-start.1 = (bf16[72,384]{1,0:T(8,128)(2,1)S(1)}, bf16[72,384]{1,0:T(8,128)(2,1)S(1)}, u32[]{:S(2)}, u32[]{:S(2)}) collective-permute-start(bf16[72,384]{1,0:T(8,128)(2,1)S(1)} %collective-permute-done), channel_id=1, source_target_pairs={{0,384},{16,400},{32,416},{48,432},{64,448},{80,464},{96,480},{112... | collective-permute-start | bytes 165896 | tf_op jit(solution)/shard_map/ppermute | solution.py:119
  40.3 11.3 %copy-start.4 = (bf16[16,2,3,512]{3,1,2,0:T(2,128)(2,1)S(1)}, bf16[16,2,3,512]{3,1,2,0:T(2,128)(2,1)}, u32[]{:S(2)}) copy-start(bf16[16,2,3,512]{3,1,2,0:T(2,128)(2,1)} %param.40) | copy-start | bytes 294916
  40.4 11.2 %copy-start.11 = (bf16[4,64]{1,0:T(4,128)(2,1)S(1)}, bf16[4,64]{1,0:T(4,128)(2,1)}, u32[]{:S(2)}) copy-start(bf16[4,64]{1,0:T(4,128)(2,1)} %param.37) | copy-start | bytes 1540
  40.4 11.3 %copy-start.13 = (f32[16]{0:T(128)S(1)}, f32[16]{0:T(128)}, u32[]{:S(2)}) copy-start(f32[16]{0:T(128)} %param.34) | copy-start | bytes 196
  40.4 11.8 %copy-start.14 = (f32[16]{0:T(128)S(1)}, f32[16]{0:T(128)}, u32[]{:S(2)}) copy-start(f32[16]{0:T(128)} %param.35) | copy-start | bytes 196
  40.4 13.1 %copy-start.15 = (f32[16]{0:T(128)S(1)}, f32[16]{0:T(128)}, u32[]{:S(2)}) copy-start(f32[16]{0:T(128)} %param.36) | copy-start | bytes 196
  40.5 13.7 %copy-start.10 = (f32[2048]{0:T(1024)S(1)}, f32[2048]{0:T(1024)}, u32[]{:S(2)}) copy-start(f32[2048]{0:T(1024)} %param.44) | copy-start | bytes 24580
  41.7 19.4 %copy-start.9 = (bf16[16,3,64]{2,0,1:T(8,128)(2,1)S(1)}, bf16[16,3,64]{2,0,1:T(8,128)(2,1)}, u32[]{:S(2)}) copy-start(bf16[16,3,64]{2,0,1:T(8,128)(2,1)} %param.39) | copy-start | bytes 18436
  41.7 19.5 %copy-start.1 = (f32[16,1,64,128]{3,2,1,0:T(8,128)S(1)}, f32[16,1,64,128]{3,2,1,0:T(8,128)}, u32[]{:S(2)}) copy-start(f32[16,1,64,128]{3,2,1,0:T(8,128)} %param.41) | copy-start | bytes 1572868
  41.7 18.5 %all-to-all-start.1 = ((f32[8,16,512]{2,1,0:T(8,128)}), f32[8,16,512]{2,1,0:T(8,128)S(1)}, u32[]{:S(2)}, u32[]{:S(2)}) async-start(f32[8,16,512]{2,1,0:T(8,128)} %pad_maximum_fusion.2), calls=%async_computation.1 | async-start | bytes 524288 | tf_op jit(solution)/shard_map/all_to_all | solution.py:20
  51.6 10.9 %copy-start.12 = (f32[64]{0:T(128)S(1)}, f32[64]{0:T(128)}, u32[]{:S(2)}) copy-start(f32[64]{0:T(128)} %param.42) | copy-start | bytes 772
  63.4 12.3 %all-to-all-start.2 = ((bf16[16,32,128]{2,1,0:T(8,128)(2,1)}), bf16[16,32,128]{2,1,0:T(8,128)(2,1)S(1)}, u32[]{:S(2)}, u32[]{:S(2)}) async-start(bf16[16,32,128]{2,1,0:T(8,128)(2,1)} %pad_maximum_fusion.4), calls=%async_computation.2 | async-start | bytes 262144 | tf_op jit(solution)/shard_map/all_to_all | solution.py:20
  77.1 21.2 %all-to-all-start.3 = ((bf16[16,16,128]{2,1,0:T(8,128)(2,1)}), bf16[16,16,128]{2,1,0:T(8,128)(2,1)S(1)}, u32[]{:S(2)}, u32[]{:S(2)}) async-start(bf16[16,16,128]{2,1,0:T(8,128)(2,1)} %broadcast_in_dim.245), calls=%async_computation.3 | async-start | bytes 131072 | tf_op jit(solution)/shard_map/all_to_all | solution.py:20
  100.1 9.7 %copy-start.2 = (bf16[1,2048,256]{2,1,0:T(8,128)(2,1)S(1)}, bf16[1,2048,256]{2,1,0:T(8,128)(2,1)}, u32[]{:S(2)}) copy-start(bf16[1,2048,256]{2,1,0:T(8,128)(2,1)} %param.47) | copy-start | bytes 3145732
  100.1 16.4 %all-to-all-start.4 = ((bf16[16,24,1024]{2,1,0:T(8,128)(2,1)}), bf16[16,24,1024]{2,1,0:T(8,128)(2,1)S(1)}, u32[]{:S(2)}, u32[]{:S(2)}) async-start(bf16[16,24,1024]{2,1,0:T(8,128)(2,1)} %pad_maximum_fusion), calls=%async_computation.4 | async-start | bytes 1572864 | tf_op jit(solution)/shard_map/all_to_all | solution.py:20
  103.9 14.2 %collective-permute-start.5 = (bf16[2048,256]{1,0:T(8,128)(2,1)}, bf16[2048,256]{1,0:T(8,128)(2,1)}, u32[]{:S(2)}, u32[]{:S(2)}) collective-permute-start(bf16[2048,256]{1,0:T(8,128)(2,1)} %bitcast.177), channel_id=1, source_target_pairs={{0,16},{16,0},{32,48},{48,32},{64,80},{80,64},{96,112},{112,96},{1... | collective-permute-start | bytes 3145736 | tf_op jit(solution)/shard_map/ppermute | solution.py:84
  109.8 11.7 %collective-permute-start.4 = (bf16[2048,256]{1,0:T(8,128)(2,1)S(1)}, bf16[2048,256]{1,0:T(8,128)(2,1)}, u32[]{:S(2)}, u32[]{:S(2)}) collective-permute-start(bf16[2048,256]{1,0:T(8,128)(2,1)S(1)} %bitcast.174), channel_id=1, source_target_pairs={{0,16},{16,0},{32,48},{48,32},{64,80},{80,64},{96,112},{112,96},{1... | collective-permute-start | bytes 3145736 | tf_op jit(solution)/shard_map/ppermute | solution.py:84
  111.8 9.8 %collective-permute-start.6 = (bf16[256,2048]{1,0:T(8,128)(2,1)}, bf16[256,2048]{1,0:T(8,128)(2,1)}, u32[]{:S(2)}, u32[]{:S(2)}) collective-permute-start(bf16[256,2048]{1,0:T(8,128)(2,1)} %bitcast.178), channel_id=1, source_target_pairs={{0,16},{16,0},{32,48},{48,32},{64,80},{80,64},{96,112},{112,96},{1... | collective-permute-start | bytes 3145736 | tf_op jit(solution)/shard_map/ppermute | solution.py:84
  114.2 28.6 %collective-permute-start.7 = (bf16[224,128]{1,0:T(8,128)(2,1)}, bf16[224,128]{1,0:T(8,128)(2,1)}, u32[]{:S(2)}, u32[]{:S(2)}) collective-permute-start(bf16[224,128]{1,0:T(8,128)(2,1)} %param.53), channel_id=1, source_target_pairs={{0,16},{16,0},{32,48},{48,32},{64,80},{80,64},{96,112},{112,96},{1... | collective-permute-start | bytes 172040 | tf_op jit(solution)/shard_map/ppermute | solution.py:84
  117.8 1.8 %copy-start.3 = (bf16[1,2048,256]{2,1,0:T(8,128)(2,1)S(1)}, bf16[1,2048,256]{2,1,0:T(8,128)(2,1)}, u32[]{:S(2)}) copy-start(bf16[1,2048,256]{2,1,0:T(8,128)(2,1)} %param.48) | copy-start | bytes 3145732
  124.9 17.5 %all-to-all-start.5 = ((bf16[16,128,128]{2,1,0:T(8,128)(2,1)}), bf16[16,128,128]{2,1,0:T(8,128)(2,1)S(1)}, u32[]{:S(2)}, u32[]{:S(2)}) async-start(bf16[16,128,128]{2,1,0:T(8,128)(2,1)} %pad_maximum_fusion.1), calls=%async_computation.5 | async-start | bytes 1048576 | tf_op jit(solution)/shard_map/all_to_all | solution.py:20
  142.7 5.4 %slice-start = ((bf16[16,2,3,512]{3,1,2,0:T(2,128)(2,1)}), bf16[16,2,2,512]{3,1,2,0:T(2,128)(2,1)S(1)}, s32[]{:S(2)}) async-start(bf16[16,2,3,512]{3,1,2,0:T(2,128)(2,1)} %param.40), calls=%async_computation.7 | async-start | bytes 131072 | tf_op jit(solution)/shard_map/slice | solution.py:231
  144.5 15.1 %all-to-all-start.6 = ((bf16[16,16,128]{2,1,0:T(8,128)(2,1)}), bf16[16,16,128]{2,1,0:T(8,128)(2,1)S(1)}, u32[]{:S(2)}, u32[]{:S(2)}) async-start(bf16[16,16,128]{2,1,0:T(8,128)(2,1)} %bitcast.51), calls=%async_computation.6 | async-start | bytes 131072 | tf_op jit(solution)/shard_map/all_to_all | solution.py:20
